TPU v7x, 512 devices: a whole 4x4x16 slice. The times are simulated.
512 devices in a mesh: sp: 16 (over z), dp: 32 (over y, x, core).
Axes of the slice: x: 4, y: 4, z: 16, core: 2. Of those that a mesh axis runs over, the one named last changes fastest.
Arguments:
- inputs: bfloat16 [32, 2176, 2048], P('dp', 'sp'), may hold values from -6 to 6
- query_vectors: bfloat16 [32, 2176, 1024], P('dp', 'sp'), may hold values from -6 to 6
- key_vectors: bfloat16 [32, 2176, 1024], P('dp', 'sp'), may hold values from -6 to 6
- value_vectors: bfloat16 [32, 2176, 1024], P('dp', 'sp'), may hold values from -6 to 6
- cotangent: bfloat16 [32, 2176, 1024], P('dp', 'sp'), may hold values from -6 to 6
- gate_prefix: float32 [32, 16, 2176], P('dp', 'sp'), may hold values from -2176 to 0, as said below
- value_weight: bfloat16 [2048, 1024], P('sp', 'dp'), may hold values from -0.125 to 0.125
Outputs:
- query_grad: bfloat16 [32, 2176, 1024], P('dp', 'sp')
- key_grad: bfloat16 [32, 2176, 1024], P('dp', 'sp')
- input_grad: bfloat16 [32, 2176, 2048], P('dp', 'sp')
- weight_grad: float32 [2048, 1024], P('sp', 'dp')
Inputs may be any that keep to these rules, and one draw needn't show every extreme that they name: `gate_prefix`: non-increasing along the positions of each sequence and head.
All inputs are finite; a program needn't handle non-finite values.
Results may differ from a plain program's by a relative error of at most 0.015.
Values may be sent and summed in bfloat16 or wider, within the bound.
No kernel may reach another device: no remote copies, remote signals or barrier semaphores. Data moves between devices by JAX's collectives and lax.ppermute only.
A program may use at most 128 MiB of HBM per device.

v0:
```python
import jax
import jax.numpy as jnp
from jax import lax
from jax.experimental import pallas as pl
from jax.experimental.pallas import tpu as pltpu
from jax.sharding import Mesh, PartitionSpec as P

HEAD_DIM = 64
LANES = 128
TILE = 256
FLOOR = -1e30


def rolled(x):
    return pltpu.roll(x, HEAD_DIM, 1)


def low_lanes(shape):
    return lax.broadcasted_iota(jnp.int32, shape, 1) < HEAD_DIM


def pack_kernel(q_ref, k_ref, v_ref, g_ref, out_ref):
    heads, tokens, _ = out_ref.shape
    low = low_lanes((tokens, LANES))
    for pair in range(heads // 2):
        cols = slice(pair * LANES, (pair + 1) * LANES)
        for first_ref, second_ref, lane in ((q_ref, k_ref, 0), (v_ref, g_ref, LANES)):
            first = first_ref[:, cols].astype(jnp.float32)
            second = second_ref[:, cols].astype(jnp.float32)
            out_ref[2 * pair, :, lane : lane + LANES] = jnp.where(
                low, first, rolled(second)
            ).astype(jnp.bfloat16)
            out_ref[2 * pair + 1, :, lane : lane + LANES] = jnp.where(
                low, rolled(first), second
            ).astype(jnp.bfloat16)


def dot_nt(a, b):
    return lax.dot_general(a, b, (((1,), (1,)), ((), ())), preferred_element_type=jnp.float32)


def dot_nn(a, b):
    return lax.dot_general(a, b, (((1,), (0,)), ((), ())), preferred_element_type=jnp.float32)


def folded(x, op):
    return op(x.reshape(x.shape[0] // 8, 8, x.shape[1]), axis=0)


def attention_kernel(
    x_ref, p_ref, qk_ref, v_out_ref, kq_ref, kt_ref, pc_ref, acc_ref, dq_ref, s_ref, d_ref
):
    length = x_ref.shape[0]
    scale = HEAD_DIM**-0.5
    blocks = [(b, min(TILE, length - b)) for b in range(0, length, TILE)]
    for base, rows in blocks:
        here = slice(base, base + rows)
        wide = x_ref[here, :LANES].astype(jnp.float32)
        swapped = rolled(wide)
        kq_ref[here] = swapped.astype(jnp.bfloat16)
        kt_ref[:, here] = swapped.T[:HEAD_DIM].astype(jnp.bfloat16)
        pc_ref[here] = jnp.broadcast_to(p_ref[:, here], (LANES, rows)).T
        acc_ref[here] = jnp.zeros((rows, LANES), jnp.float32)
    for index, (q_base, q_rows) in enumerate(blocks):
        q_here = slice(q_base, q_base + q_rows)
        low = low_lanes((q_rows, LANES))
        query_wide = x_ref[q_here, :LANES].astype(jnp.float32)
        grad_wide = rolled(x_ref[q_here, LANES:].astype(jnp.float32))
        query_low = jnp.where(low, query_wide * scale, 0.0).astype(jnp.bfloat16)
        query_high = jnp.where(low, 0.0, rolled(query_wide)).astype(jnp.bfloat16)
        grad_low = jnp.where(low, grad_wide, 0.0).astype(jnp.bfloat16)
        pivot = pc_ref[q_base : q_base + 1, :]
        peak = jnp.full((8, q_rows), FLOOR, jnp.float32)
        for u_base, u_rows in blocks[: index + 1]:
            u_here = slice(u_base, u_base + u_rows)
            shift = pivot - pc_ref[u_here]
            shift = jnp.concatenate([shift] * (q_rows // LANES), axis=1)
            scores = dot_nt(kq_ref[u_here], query_low) + shift
            if u_base == q_base:
                seen = lax.broadcasted_iota(jnp.int32, scores.shape, 0) <= lax.broadcasted_iota(
                    jnp.int32, scores.shape, 1
                )
                scores = jnp.where(seen, scores, FLOOR)
            s_ref[u_here, :q_rows] = scores
            peak = jnp.maximum(peak, folded(scores, jnp.max))
        peak = jnp.max(peak, axis=0, keepdims=True)
        total = jnp.zeros((8, q_rows), jnp.float32)
        for u_base, u_rows in blocks[: index + 1]:
            u_here = slice(u_base, u_base + u_rows)
            raised = jnp.exp(s_ref[u_here, :q_rows] - peak)
            s_ref[u_here, :q_rows] = raised
            total = total + folded(raised, jnp.sum)
        share = 1.0 / jnp.sum(total, axis=0, keepdims=True)
        term = jnp.zeros((8, q_rows), jnp.float32)
        for u_base, u_rows in blocks[: index + 1]:
            u_here = slice(u_base, u_base + u_rows)
            soft = s_ref[u_here, :q_rows] * share
            s_ref[u_here, :q_rows] = soft
            acc_ref[u_here] += dot_nn(soft.astype(jnp.bfloat16), grad_low)
            soft_grad = dot_nt(x_ref[u_here, LANES:], grad_low)
            d_ref[u_here, :q_rows] = soft_grad
            term = term + folded(soft * soft_grad, jnp.sum)
        term = jnp.sum(term, axis=0, keepdims=True)
        query_grad = jnp.zeros((HEAD_DIM, q_rows), jnp.float32)
        for u_base, u_rows in blocks[: index + 1]:
            u_here = slice(u_base, u_base + u_rows)
            score_low = (s_ref[u_here, :q_rows] * (d_ref[u_here, :q_rows] - term)).astype(
                jnp.bfloat16
            )
            acc_ref[u_here] += dot_nn(score_low, query_high)
            query_grad = query_grad + dot_nn(kt_ref[:, u_here], score_low)
        query_grad = jnp.concatenate([query_grad, jnp.zeros_like(query_grad)], axis=0)
        dq_ref[q_here] = query_grad.T
    for base, rows in blocks:
        here = slice(base, base + rows)
        qk_ref[here] = (
            jnp.where(low_lanes((rows, LANES)), dq_ref[here], acc_ref[here]) * scale
        ).astype(jnp.bfloat16)
    planes, kept, _ = v_out_ref.shape
    tokens = length // planes
    for plane in range(planes):
        base = plane * tokens
        first = acc_ref[base : base + kept]
        second = acc_ref[base + kept : base + tokens]
        second = jnp.concatenate([second, first[: 2 * kept - tokens]], axis=0)
        v_out_ref[plane] = jnp.where(low_lanes(first.shape), first, rolled(second)).astype(
            jnp.bfloat16
        )


def unpack_value_kernel(x_ref, rows_ref, parts_ref):
    heads, kept, _ = x_ref.shape
    cores, columns, tokens, _ = parts_ref.shape
    rest = tokens - kept
    quarter = LANES // heads * columns
    lane = lax.broadcasted_iota(jnp.int32, (tokens, LANES), 1)
    for column in range(columns):
        parts = [jnp.zeros((tokens, LANES), jnp.float32)] * cores
        for group in range(heads // columns):
            block = x_ref[group * columns + column].astype(jnp.float32)
            for core in range(cores):
                home = group * quarter
                top = pltpu.roll(block, (home - core * quarter) % LANES, 1)
                bottom = pltpu.roll(block, (home - core * quarter - HEAD_DIM) % LANES, 1)[:rest]
                moved = jnp.concatenate([top, bottom], axis=0)
                inside = (lane >= home) & (lane < home + quarter)
                parts[core] = jnp.where(inside, moved, parts[core])
        for core in range(cores):
            part = parts[core].astype(jnp.bfloat16)
            parts_ref[core, column] = part
            rows_ref[core, :, column * LANES : (column + 1) * LANES] = part


def unpack_pair_kernel(x_ref, q_ref, k_ref):
    heads, tokens, _ = x_ref.shape
    low = low_lanes((tokens, LANES))
    for pair in range(heads // 2):
        first = x_ref[2 * pair].astype(jnp.float32)
        second = x_ref[2 * pair + 1].astype(jnp.float32)
        cols = slice(pair * LANES, (pair + 1) * LANES)
        q_ref[:, cols] = jnp.where(low, first, rolled(second)).astype(jnp.bfloat16)
        k_ref[:, cols] = jnp.where(low, rolled(first), second).astype(jnp.bfloat16)


def exchanged(x, axis):
    return lax.all_to_all(x, axis, split_axis=0, concat_axis=0, tiled=True)


def shifted(x, axis, step):
    count = lax.axis_size(axis)
    return lax.ppermute(x, axis, [(place, (place + step) % count) for place in range(count)])


def block_of(x, index):
    return lax.dynamic_index_in_dim(x, index, 0, keepdims=False)


def from_all(x, axis):
    return [x] + [shifted(x, axis, step) for step in range(1, lax.axis_size(axis))]


def sent_blocks(blocks, axis):
    count = lax.axis_size(axis)
    here = lax.axis_index(axis)
    own = block_of(blocks, here)
    return [own] + [
        shifted(block_of(blocks, (here + step) % count), axis, step) for step in range(1, count)
    ]


def placed(parts, axis):
    count = lax.axis_size(axis)
    here = lax.axis_index(axis)
    whole = jnp.zeros((count, *parts[0].shape), parts[0].dtype)
    for step, part in enumerate(parts):
        whole = lax.dynamic_update_index_in_dim(whole, part, (here - step) % count, 0)
    return whole.reshape(count * parts[0].shape[0], *parts[0].shape[1:])


def shaped(*shape, dtype=jnp.bfloat16):
    return jax.ShapeDtypeStruct(shape, dtype)


def shards(inputs, query_vectors, key_vectors, value_vectors, cotangent, gate_prefix, value_weight):
    planes = lax.axis_size("sp")
    cores, columns, lines = lax.axis_size("core"), lax.axis_size("x"), lax.axis_size("y")
    core = lax.axis_index("core")
    tokens, model = inputs.shape[1:]
    width = query_vectors.shape[2]
    heads = width // HEAD_DIM
    length = planes * tokens
    w_cols = value_weight.shape[1]
    weight_block = jnp.broadcast_to(value_weight.T, (planes, w_cols, model // planes))
    weight_block = exchanged(weight_block, "sp")
    weight_block = jnp.moveaxis(weight_block, 0, 1).reshape(w_cols, model)
    packed = pl.pallas_call(pack_kernel, out_shape=shaped(heads, tokens, 2 * LANES))(
        query_vectors[0], key_vectors[0], value_vectors[0], cotangent[0]
    )
    arrived = exchanged(packed, "sp")
    input_rows = jnp.concatenate(from_all(inputs[0], "x"), axis=0)
    input_rows = jnp.concatenate(from_all(input_rows, "core"), axis=0)
    weight_line = placed(from_all(weight_block, "y"), "y")
    weight_half = placed(from_all(weight_line, "x"), "x")
    weight_halves = from_all(weight_half, "core")
    kept = (tokens // 2 + 7) // 8 * 8
    pair_grad, value_grad = pl.pallas_call(
        attention_kernel,
        out_shape=(shaped(length, LANES), shaped(planes, kept, LANES)),
        scratch_shapes=[
            pltpu.VMEM((length, LANES), jnp.bfloat16),
            pltpu.VMEM((HEAD_DIM, length), jnp.bfloat16),
            pltpu.VMEM((length, LANES), jnp.float32),
            pltpu.VMEM((length, LANES), jnp.float32),
            pltpu.VMEM((length, LANES), jnp.float32),
            pltpu.VMEM((length, TILE), jnp.float32),
            pltpu.VMEM((length, TILE), jnp.float32),
        ],
    )(arrived.reshape(length, 2 * LANES), gate_prefix[0])
    value_back = exchanged(value_grad, "sp")
    pair_back = exchanged(pair_grad.reshape(planes, tokens, LANES), "sp")
    value_rows, value_parts = pl.pallas_call(
        unpack_value_kernel,
        out_shape=(shaped(cores, tokens, width // cores), shaped(cores, columns, tokens, LANES)),
    )(value_back)
    away = shifted(block_of(value_parts, 1 - core), "core", 1)
    both = jnp.concatenate([block_of(value_parts, core), away], axis=1)
    pieces = sent_blocks(both, "x")
    value_cols = jnp.concatenate(
        [piece[:tokens] for piece in pieces] + [piece[tokens:] for piece in pieces], axis=0
    )
    partial = lax.dot_general(
        value_cols, input_rows, (((0,), (0,)), ((), ())), preferred_element_type=jnp.float32
    ).astype(jnp.bfloat16)
    partial = sent_blocks(partial.reshape(lines, w_cols, model), "y")
    partial = sum(part.astype(jnp.float32) for part in partial).astype(jnp.bfloat16)
    partial = jnp.moveaxis(partial.reshape(w_cols, planes, model // planes), 1, 0)
    partial = exchanged(partial, "sp")
    weight_grad = partial.astype(jnp.float32).sum(axis=0).T
    query_grad, key_grad = pl.pallas_call(
        unpack_pair_kernel, out_shape=(shaped(tokens, width), shaped(tokens, width))
    )(pair_back)
    input_grad = sum(
        lax.dot_general(
            block_of(value_rows, place),
            half,
            (((1,), (0,)), ((), ())),
            preferred_element_type=jnp.float32,
        )
        for place, half in zip((core, 1 - core), weight_halves)
    ).astype(jnp.bfloat16)
    return (query_grad[None], key_grad[None], input_grad[None], weight_grad)


def solution(mesh):
    grid = Mesh(mesh.devices.reshape(-1, 4, 4, 2), ("sp", "y", "x", "core"))
    rows = P(("y", "x", "core"), "sp", None)
    weight = P("sp", ("y", "x", "core"))

    return jax.shard_map(
        shards,
        mesh=grid,
        in_specs=(rows,) * 6 + (weight,),
        out_specs=(rows, rows, rows, weight),
        check_vma=False,
    )
```

profile of v0, /device:TPU:38, one launch (start us, length us, event | category | flops | bytes accessed | tf_op | source)
XLA Modules:
  0.0 228.2 jit_solution(1439758260722696136)
XLA Ops:
  2.0 15.2 %all-to-all-start.3 = ((bf16[16,32,128]{2,1,0:T(8,128)(2,1)}), bf16[16,32,128]{2,1,0:T(8,128)(2,1)S(1)}, u32[]{:S(2)}, u32[]{:S(2)}) async-start(bf16[16,32,128]{2,1,0:T(8,128)(2,1)} %broadcast_in_dim.48), calls=%async_computation.3 | async-start | bytes 262144 | tf_op jit(solution)/shard_map/all_to_all | solution.py:166
  17.2 2.7 %shard_map.102 = bf16[16,136,256]{2,1,0:T(8,128)(2,1)} custom-call(bf16[136,1024]{1,0:T(8,128)(2,1)} %bitcast.92, bf16[136,1024]{1,0:T(8,128)(2,1)} %bitcast.93, bf16[136,1024]{1,0:T(8,128)(2,1)} %bitcast.94, bf16[136,1024]{1,0:T(8,128)(2,1)} %bitcast.95), custom_call_target="tpu_custom_call" | custom-call | tf_op jit(solution)/shard_map/pallas_call | solution.py:216
  20.0 11.5 %all-to-all-done.3 = bf16[16,32,128]{2,1,0:T(8,128)(2,1)S(1)} async-done(((bf16[16,32,128]{2,1,0:T(8,128)(2,1)}), bf16[16,32,128]{2,1,0:T(8,128)(2,1)S(1)}, u32[]{:S(2)}, u32[]{:S(2)}) %all-to-all-start.3) | async-done | bytes 131104 | tf_op jit(solution)/shard_map/all_to_all | solution.py:166
  31.4 4.3 %all-to-all-start = ((bf16[16,136,256]{2,1,0:T(8,128)(2,1)}), bf16[16,136,256]{2,1,0:T(8,128)(2,1)S(1)}, u32[]{:S(2)}, u32[]{:S(2)}) async-start(bf16[16,136,256]{2,1,0:T(8,128)(2,1)} %shard_map.102), calls=%async_computation | async-start | bytes 2228224 | tf_op jit(solution)/shard_map/all_to_all | solution.py:166
  38.2 4.3 %collective-permute-start.12 = (bf16[136,2048]{1,0:T(8,128)(2,1)S(1)}, bf16[136,2048]{1,0:T(8,128)(2,1)S(1)}, u32[]{:S(2)}, u32[]{:S(2)}) collective-permute-start(bf16[136,2048]{1,0:T(8,128)(2,1)S(1)} %bitcast.85), channel_id=1, source_target_pairs={{0,4},{2,6},{4,0},{6,2},{1,5},{3,7},{5,1},{7,3},{8,12},{10,14},{12... | collective-permute-start | bytes 1671176 | tf_op jit(solution)/shard_map/ppermute | solution.py:171
  46.2 3.5 %collective-permute-start = (bf16[32,2048]{1,0:T(8,128)(2,1)}, bf16[32,2048]{1,0:T(8,128)(2,1)}, u32[]{:S(2)}, u32[]{:S(2)}) collective-permute-start(bf16[32,2048]{1,0:T(8,128)(2,1)} %copy_bitcast_fusion), channel_id=1, source_target_pairs={{0,8},{8,16},{16,24},{24,0},{1,9},{9,17},{17,25},{25,1},{2,10},{10... | collective-permute-start | bytes 393224 | tf_op jit(solution)/shard_map/ppermute | solution.py:171
  49.6 4.8 %collective-permute-start.1 = (bf16[32,2048]{1,0:T(8,128)(2,1)}, bf16[32,2048]{1,0:T(8,128)(2,1)}, u32[]{:S(2)}, u32[]{:S(2)}) collective-permute-start(bf16[32,2048]{1,0:T(8,128)(2,1)} %copy_bitcast_fusion), channel_id=1, source_target_pairs={{0,16},{8,24},{16,0},{24,8},{1,17},{9,25},{17,1},{25,9},{2,18},{10... | collective-permute-start | bytes 393224 | tf_op jit(solution)/shard_map/ppermute | solution.py:171
  57.7 3.2 %collective-permute-start.2 = (bf16[32,2048]{1,0:T(8,128)(2,1)}, bf16[32,2048]{1,0:T(8,128)(2,1)S(1)}, u32[]{:S(2)}, u32[]{:S(2)}) collective-permute-start(bf16[32,2048]{1,0:T(8,128)(2,1)} %copy_bitcast_fusion), channel_id=1, source_target_pairs={{0,24},{8,0},{16,8},{24,16},{1,25},{9,1},{17,9},{25,17},{2,26},{10... | collective-permute-start | bytes 393224 | tf_op jit(solution)/shard_map/ppermute | solution.py:171
  60.9 5.5 %collective-permute-done.13 = bf16[136,2048]{1,0:T(8,128)(2,1)S(1)} collective-permute-done((bf16[136,2048]{1,0:T(8,128)(2,1)S(1)}, bf16[136,2048]{1,0:T(8,128)(2,1)S(1)}, u32[]{:S(2)}, u32[]{:S(2)}) %collective-permute-start.13) | collective-permute-done | bytes 557088 | tf_op jit(solution)/shard_map/ppermute | solution.py:171
  79.0 4.3 %collective-permute-start.4 = (bf16[128,2048]{1,0:T(8,128)(2,1)}, bf16[128,2048]{1,0:T(8,128)(2,1)}, u32[]{:S(2)}, u32[]{:S(2)}) collective-permute-start(bf16[128,2048]{1,0:T(8,128)(2,1)} %bitcast.16), channel_id=1, source_target_pairs={{0,4},{2,6},{4,0},{6,2},{1,5},{3,7},{5,1},{7,3},{8,12},{10,14},{12... | collective-permute-start | bytes 1572872 | tf_op jit(solution)/shard_map/ppermute | solution.py:171
  83.3 2.9 %collective-permute-start.5 = (bf16[128,2048]{1,0:T(8,128)(2,1)}, bf16[128,2048]{1,0:T(8,128)(2,1)S(1)}, u32[]{:S(2)}, u32[]{:S(2)}) collective-permute-start(bf16[128,2048]{1,0:T(8,128)(2,1)} %bitcast.16), channel_id=1, source_target_pairs={{0,6},{2,0},{4,2},{6,4},{1,7},{3,1},{5,3},{7,5},{8,14},{10,8},{12,... | collective-permute-start | bytes 1572872 | tf_op jit(solution)/shard_map/ppermute | solution.py:171
  87.9 13.0 %shard_map.103 = (bf16[2176,128]{1,0:T(8,128)(2,1)}, bf16[16,72,128]{2,1,0:T(8,128)(2,1)}) custom-call(bf16[2176,256]{1,0:T(8,128)(2,1)} %bitcast.83, f32[1,2176]{1,0:T(1,128)} %bitcast.97), custom_call_target="tpu_custom_call" | custom-call | tf_op jit(solution)/shard_map/pallas_call | solution.py:226
  100.9 11.3 %all-to-all-start.2 = ((bf16[16,72,128]{2,1,0:T(8,128)(2,1)}), bf16[16,72,128]{2,1,0:T(8,128)(2,1)S(1)}, u32[]{:S(2)}, u32[]{:S(2)}) async-start(bf16[16,72,128]{2,1,0:T(8,128)(2,1)} %get-tuple-element.13), calls=%async_computation.2 | async-start | bytes 589824 | tf_op jit(solution)/shard_map/all_to_all | solution.py:166
  115.8 14.9 %all-to-all-done.2.x_ref = bf16[16,72,128]{2,1,0:T(8,128)(2,1)S(1)} async-done(((bf16[16,72,128]{2,1,0:T(8,128)(2,1)}), bf16[16,72,128]{2,1,0:T(8,128)(2,1)S(1)}, u32[]{:S(2)}, u32[]{:S(2)}) %all-to-all-start.2) | async-done | bytes 294944 | tf_op jit(solution)/shard_map/all_to_all | solution.py:166
  136.5 3.3 %constant_dynamic-update-slice_fusion = bf16[1088,2048]{1,0:T(8,128)(2,1)} fusion(bf16[1088,2048]{1,0:T(8,128)(2,1)} %constant_dynamic-update-slice_fusion.1, bf16[544,2048]{1,0:T(8,128)(2,1)} %collective-permute-done.14), kind=kLoop, calls=%fused_computation.54 | loop fusion | bytes 4456448 | tf_op jit(solution)/shard_map/concatenate | solution.py:221
  139.8 4.5 %collective-permute-start.8 = (bf16[272,128]{1,0:T(8,128)(2,1)S(1)}, bf16[272,128]{1,0:T(8,128)(2,1)S(1)}, u32[]{:S(2)}, u32[]{:S(2)}) collective-permute-start(bf16[272,128]{1,0:T(8,128)(2,1)S(1)} %get-tuple-element.21), channel_id=1, source_target_pairs={{0,2},{2,4},{4,6},{6,0},{1,3},{3,5},{5,7},{7,1},{8,10},{10,12},{12... | collective-permute-start | bytes 208904 | tf_op jit(solution)/shard_map/ppermute | solution.py:171
  146.3 3.2 %collective-permute-start.10 = (bf16[272,128]{1,0:T(8,128)(2,1)S(1)}, bf16[272,128]{1,0:T(8,128)(2,1)S(1)}, u32[]{:S(2)}, u32[]{:S(2)}) collective-permute-start(bf16[272,128]{1,0:T(8,128)(2,1)S(1)} %get-tuple-element.19), channel_id=1, source_target_pairs={{0,6},{2,0},{4,2},{6,4},{1,7},{3,1},{5,3},{7,5},{8,14},{10,8},{12,... | collective-permute-start | bytes 208904 | tf_op jit(solution)/shard_map/ppermute | solution.py:171
  153.8 3.1 %convolution_convert_fusion = bf16[128,2048]{1,0:T(8,128)(2,1)S(1)} fusion(bf16[1088,128]{1,0:T(8,128)(2,1)S(1)} %slice_dynamic-update-slice_fusion, bf16[1088,2048]{1,0:T(8,128)(2,1)} %constant_dynamic-update-slice_fusion), kind=kOutput, calls=%fused_computation.2 | convolution fusion | flops 570687488 | bytes 5259264 | tf_op jit(solution)/shard_map/dot_general | solution.py:251
  156.9 4.9 %collective-permute-start.17 = (bf16[32,2048]{1,0:T(8,128)(2,1)S(1)}, bf16[32,2048]{1,0:T(8,128)(2,1)S(1)}, u32[]{:S(2)}, u32[]{:S(2)}) collective-permute-start(bf16[32,2048]{1,0:T(8,128)(2,1)S(1)} %get-tuple-element.17), channel_id=1, source_target_pairs={{0,24},{8,0},{16,8},{24,16},{1,25},{9,1},{17,9},{25,17},{2,26},{10... | collective-permute-start | bytes 393224 | tf_op jit(solution)/shard_map/ppermute | solution.py:171
  161.9 2.5 %collective-permute-start.16 = (bf16[32,2048]{1,0:T(8,128)(2,1)S(1)}, bf16[32,2048]{1,0:T(8,128)(2,1)S(1)}, u32[]{:S(2)}, u32[]{:S(2)}) collective-permute-start(bf16[32,2048]{1,0:T(8,128)(2,1)S(1)} %get-tuple-element.18), channel_id=1, source_target_pairs={{0,16},{8,24},{16,0},{24,8},{1,17},{9,25},{17,1},{25,9},{2,18},{10... | collective-permute-start | bytes 393224 | tf_op jit(solution)/shard_map/ppermute | solution.py:171
  164.4 2.9 %collective-permute-start.15 = (bf16[32,2048]{1,0:T(8,128)(2,1)S(1)}, bf16[32,2048]{1,0:T(8,128)(2,1)S(1)}, u32[]{:S(2)}, u32[]{:S(2)}) collective-permute-start(bf16[32,2048]{1,0:T(8,128)(2,1)S(1)} %get-tuple-element.16), channel_id=1, source_target_pairs={{0,8},{8,16},{16,24},{24,0},{1,9},{9,17},{17,25},{25,1},{2,10},{10... | collective-permute-start | bytes 393224 | tf_op jit(solution)/shard_map/ppermute | solution.py:171
  173.0 19.5 %all_to_all.25 = bf16[16,32,128]{2,1,0:T(8,128)(2,1)S(1)} all-to-all(bf16[16,32,128]{2,1,0:T(8,128)(2,1)S(1)} %copy.13), channel_id=1, replica_groups=mesh['sp'=16,'y'=4,'x'=4,'core'=2] {'sp'}, dimensions={0} | all-to-all | bytes 262144 | tf_op jit(solution)/shard_map/all_to_all | solution.py:166
  192.4 5.3 %all-to-all-start.1 = ((bf16[16,136,128]{2,1,0:T(8,128)(2,1)}), bf16[16,136,128]{2,1,0:T(8,128)(2,1)}, u32[]{:S(2)}, u32[]{:S(2)}) async-start(bf16[16,136,128]{2,1,0:T(8,128)(2,1)} %bitcast.6), calls=%async_computation.1 | async-start | bytes 1114112 | tf_op jit(solution)/shard_map/all_to_all | solution.py:166
  201.9 24.2 %all-to-all-done.1.x_ref = bf16[16,136,128]{2,1,0:T(8,128)(2,1)} async-done(((bf16[16,136,128]{2,1,0:T(8,128)(2,1)}), bf16[16,136,128]{2,1,0:T(8,128)(2,1)}, u32[]{:S(2)}, u32[]{:S(2)}) %all-to-all-start.1) | async-done | bytes 557088 | tf_op jit(solution)/shard_map/all_to_all | solution.py:166
  (71 shorter events, 51.8 us)
Async XLA Ops:
  2.0 29.4 %all-to-all-start.3 = ((bf16[16,32,128]{2,1,0:T(8,128)(2,1)}), bf16[16,32,128]{2,1,0:T(8,128)(2,1)S(1)}, u32[]{:S(2)}, u32[]{:S(2)}) async-start(bf16[16,32,128]{2,1,0:T(8,128)(2,1)} %broadcast_in_dim.48), calls=%async_computation.3 | async-start | bytes 262144 | tf_op jit(solution)/shard_map/all_to_all | solution.py:166
  17.2 18.5 %copy-start.1 = (bf16[1,136,2048]{2,1,0:T(8,128)(2,1)S(1)}, bf16[1,136,2048]{2,1,0:T(8,128)(2,1)}, u32[]{:S(2)}) copy-start(bf16[1,136,2048]{2,1,0:T(8,128)(2,1)} %param.7) | copy-start | bytes 1671172
  31.4 55.5 %all-to-all-start = ((bf16[16,136,256]{2,1,0:T(8,128)(2,1)}), bf16[16,136,256]{2,1,0:T(8,128)(2,1)S(1)}, u32[]{:S(2)}, u32[]{:S(2)}) async-start(bf16[16,136,256]{2,1,0:T(8,128)(2,1)} %shard_map.102), calls=%async_computation | async-start | bytes 2228224 | tf_op jit(solution)/shard_map/all_to_all | solution.py:166
  35.8 21.9 %collective-permute-start.11 = (bf16[136,2048]{1,0:T(8,128)(2,1)S(1)}, bf16[136,2048]{1,0:T(8,128)(2,1)S(1)}, u32[]{:S(2)}, u32[]{:S(2)}) collective-permute-start(bf16[136,2048]{1,0:T(8,128)(2,1)S(1)} %bitcast.84), channel_id=1, source_target_pairs={{0,2},{2,4},{4,6},{6,0},{1,3},{3,5},{5,7},{7,1},{8,10},{10,12},{12... | collective-permute-start | bytes 1671176 | tf_op jit(solution)/shard_map/ppermute | solution.py:171
  38.2 22.8 %collective-permute-start.12 = (bf16[136,2048]{1,0:T(8,128)(2,1)S(1)}, bf16[136,2048]{1,0:T(8,128)(2,1)S(1)}, u32[]{:S(2)}, u32[]{:S(2)}) collective-permute-start(bf16[136,2048]{1,0:T(8,128)(2,1)S(1)} %bitcast.85), channel_id=1, source_target_pairs={{0,4},{2,6},{4,0},{6,2},{1,5},{3,7},{5,1},{7,3},{8,12},{10,14},{12... | collective-permute-start | bytes 1671176 | tf_op jit(solution)/shard_map/ppermute | solution.py:171
  42.5 24.0 %collective-permute-start.13 = (bf16[136,2048]{1,0:T(8,128)(2,1)S(1)}, bf16[136,2048]{1,0:T(8,128)(2,1)S(1)}, u32[]{:S(2)}, u32[]{:S(2)}) collective-permute-start(bf16[136,2048]{1,0:T(8,128)(2,1)S(1)} %bitcast.86), channel_id=1, source_target_pairs={{0,6},{2,0},{4,2},{6,4},{1,7},{3,1},{5,3},{7,5},{8,14},{10,8},{12,... | collective-permute-start | bytes 1671176 | tf_op jit(solution)/shard_map/ppermute | solution.py:171
  46.2 24.8 %collective-permute-start = (bf16[32,2048]{1,0:T(8,128)(2,1)}, bf16[32,2048]{1,0:T(8,128)(2,1)}, u32[]{:S(2)}, u32[]{:S(2)}) collective-permute-start(bf16[32,2048]{1,0:T(8,128)(2,1)} %copy_bitcast_fusion), channel_id=1, source_target_pairs={{0,8},{8,16},{16,24},{24,0},{1,9},{9,17},{17,25},{25,1},{2,10},{10... | collective-permute-start | bytes 393224 | tf_op jit(solution)/shard_map/ppermute | solution.py:171
  49.6 22.9 %collective-permute-start.1 = (bf16[32,2048]{1,0:T(8,128)(2,1)}, bf16[32,2048]{1,0:T(8,128)(2,1)}, u32[]{:S(2)}, u32[]{:S(2)}) collective-permute-start(bf16[32,2048]{1,0:T(8,128)(2,1)} %copy_bitcast_fusion), channel_id=1, source_target_pairs={{0,16},{8,24},{16,0},{24,8},{1,17},{9,25},{17,1},{25,9},{2,18},{10... | collective-permute-start | bytes 393224 | tf_op jit(solution)/shard_map/ppermute | solution.py:171
  57.7 16.4 %collective-permute-start.2 = (bf16[32,2048]{1,0:T(8,128)(2,1)}, bf16[32,2048]{1,0:T(8,128)(2,1)S(1)}, u32[]{:S(2)}, u32[]{:S(2)}) collective-permute-start(bf16[32,2048]{1,0:T(8,128)(2,1)} %copy_bitcast_fusion), channel_id=1, source_target_pairs={{0,24},{8,0},{16,8},{24,16},{1,25},{9,1},{17,9},{25,17},{2,26},{10... | collective-permute-start | bytes 393224 | tf_op jit(solution)/shard_map/ppermute | solution.py:171
  68.1 68.3 %collective-permute-start.14 = (bf16[544,2048]{1,0:T(8,128)(2,1)}, bf16[544,2048]{1,0:T(8,128)(2,1)}, u32[]{:S(2)}, u32[]{:S(2)}) collective-permute-start(bf16[544,2048]{1,0:T(8,128)(2,1)} %pad_maximum_fusion), channel_id=1, source_target_pairs={{0,1},{1,0},{2,3},{3,2},{4,5},{5,4},{6,7},{7,6},{8,9},{9,8},{10,11... | collective-permute-start | bytes 6684680 | tf_op jit(solution)/shard_map/ppermute | solution.py:171
  74.7 38.9 %collective-permute-start.3 = (bf16[128,2048]{1,0:T(8,128)(2,1)}, bf16[128,2048]{1,0:T(8,128)(2,1)}, u32[]{:S(2)}, u32[]{:S(2)}) collective-permute-start(bf16[128,2048]{1,0:T(8,128)(2,1)} %bitcast.16), channel_id=1, source_target_pairs={{0,2},{2,4},{4,6},{6,0},{1,3},{3,5},{5,7},{7,1},{8,10},{10,12},{12... | collective-permute-start | bytes 1572872 | tf_op jit(solution)/shard_map/ppermute | solution.py:171
  79.0 35.7 %collective-permute-start.4 = (bf16[128,2048]{1,0:T(8,128)(2,1)}, bf16[128,2048]{1,0:T(8,128)(2,1)}, u32[]{:S(2)}, u32[]{:S(2)}) collective-permute-start(bf16[128,2048]{1,0:T(8,128)(2,1)} %bitcast.16), channel_id=1, source_target_pairs={{0,4},{2,6},{4,0},{6,2},{1,5},{3,7},{5,1},{7,3},{8,12},{10,14},{12... | collective-permute-start | bytes 1572872 | tf_op jit(solution)/shard_map/ppermute | solution.py:171
  83.3 84.0 %collective-permute-start.5 = (bf16[128,2048]{1,0:T(8,128)(2,1)}, bf16[128,2048]{1,0:T(8,128)(2,1)S(1)}, u32[]{:S(2)}, u32[]{:S(2)}) collective-permute-start(bf16[128,2048]{1,0:T(8,128)(2,1)} %bitcast.16), channel_id=1, source_target_pairs={{0,6},{2,0},{4,2},{6,4},{1,7},{3,1},{5,3},{7,5},{8,14},{10,8},{12,... | collective-permute-start | bytes 1572872 | tf_op jit(solution)/shard_map/ppermute | solution.py:171
  100.9 29.8 %all-to-all-start.2 = ((bf16[16,72,128]{2,1,0:T(8,128)(2,1)}), bf16[16,72,128]{2,1,0:T(8,128)(2,1)S(1)}, u32[]{:S(2)}, u32[]{:S(2)}) async-start(bf16[16,72,128]{2,1,0:T(8,128)(2,1)} %get-tuple-element.13), calls=%async_computation.2 | async-start | bytes 589824 | tf_op jit(solution)/shard_map/all_to_all | solution.py:166
  134.5 5.2 %collective-permute-start.7 = (bf16[4,136,128]{2,1,0:T(8,128)(2,1)S(1)}, bf16[4,136,128]{2,1,0:T(8,128)(2,1)S(1)}, u32[]{:S(2)}, u32[]{:S(2)}) collective-permute-start(bf16[4,136,128]{2,1,0:T(8,128)(2,1)S(1)} %get-tuple-element.23), channel_id=1, source_target_pairs={{0,1},{1,0},{2,3},{3,2},{4,5},{5,4},{6,7},{7,6},{8,9},{9,8},{10,11... | collective-permute-start | bytes 417800 | tf_op jit(solution)/shard_map/ppermute | solution.py:171
  139.8 9.7 %collective-permute-start.8 = (bf16[272,128]{1,0:T(8,128)(2,1)S(1)}, bf16[272,128]{1,0:T(8,128)(2,1)S(1)}, u32[]{:S(2)}, u32[]{:S(2)}) collective-permute-start(bf16[272,128]{1,0:T(8,128)(2,1)S(1)} %get-tuple-element.21), channel_id=1, source_target_pairs={{0,2},{2,4},{4,6},{6,0},{1,3},{3,5},{5,7},{7,1},{8,10},{10,12},{12... | collective-permute-start | bytes 208904 | tf_op jit(solution)/shard_map/ppermute | solution.py:171
  144.3 7.7 %collective-permute-start.9 = (bf16[272,128]{1,0:T(8,128)(2,1)S(1)}, bf16[272,128]{1,0:T(8,128)(2,1)S(1)}, u32[]{:S(2)}, u32[]{:S(2)}) collective-permute-start(bf16[272,128]{1,0:T(8,128)(2,1)S(1)} %get-tuple-element.22), channel_id=1, source_target_pairs={{0,4},{2,6},{4,0},{6,2},{1,5},{3,7},{5,1},{7,3},{8,12},{10,14},{12... | collective-permute-start | bytes 208904 | tf_op jit(solution)/shard_map/ppermute | solution.py:171
  146.3 7.4 %collective-permute-start.10 = (bf16[272,128]{1,0:T(8,128)(2,1)S(1)}, bf16[272,128]{1,0:T(8,128)(2,1)S(1)}, u32[]{:S(2)}, u32[]{:S(2)}) collective-permute-start(bf16[272,128]{1,0:T(8,128)(2,1)S(1)} %get-tuple-element.19), channel_id=1, source_target_pairs={{0,6},{2,0},{4,2},{6,4},{1,7},{3,1},{5,3},{7,5},{8,14},{10,8},{12,... | collective-permute-start | bytes 208904 | tf_op jit(solution)/shard_map/ppermute | solution.py:171
  156.9 12.4 %collective-permute-start.17 = (bf16[32,2048]{1,0:T(8,128)(2,1)S(1)}, bf16[32,2048]{1,0:T(8,128)(2,1)S(1)}, u32[]{:S(2)}, u32[]{:S(2)}) collective-permute-start(bf16[32,2048]{1,0:T(8,128)(2,1)S(1)} %get-tuple-element.17), channel_id=1, source_target_pairs={{0,24},{8,0},{16,8},{24,16},{1,25},{9,1},{17,9},{25,17},{2,26},{10... | collective-permute-start | bytes 393224 | tf_op jit(solution)/shard_map/ppermute | solution.py:171
  161.9 9.6 %collective-permute-start.16 = (bf16[32,2048]{1,0:T(8,128)(2,1)S(1)}, bf16[32,2048]{1,0:T(8,128)(2,1)S(1)}, u32[]{:S(2)}, u32[]{:S(2)}) collective-permute-start(bf16[32,2048]{1,0:T(8,128)(2,1)S(1)} %get-tuple-element.18), channel_id=1, source_target_pairs={{0,16},{8,24},{16,0},{24,8},{1,17},{9,25},{17,1},{25,9},{2,18},{10... | collective-permute-start | bytes 393224 | tf_op jit(solution)/shard_map/ppermute | solution.py:171
  164.4 8.4 %collective-permute-start.15 = (bf16[32,2048]{1,0:T(8,128)(2,1)S(1)}, bf16[32,2048]{1,0:T(8,128)(2,1)S(1)}, u32[]{:S(2)}, u32[]{:S(2)}) collective-permute-start(bf16[32,2048]{1,0:T(8,128)(2,1)S(1)} %get-tuple-element.16), channel_id=1, source_target_pairs={{0,8},{8,16},{16,24},{24,0},{1,9},{9,17},{17,25},{25,1},{2,10},{10... | collective-permute-start | bytes 393224 | tf_op jit(solution)/shard_map/ppermute | solution.py:171
  167.4 30.4 %collective-permute-start.6 = (bf16[512,2048]{1,0:T(8,128)(2,1)S(1)}, bf16[512,2048]{1,0:T(8,128)(2,1)}, u32[]{:S(2)}, u32[]{:S(2)}) collective-permute-start(bf16[512,2048]{1,0:T(8,128)(2,1)S(1)} %bitcast.81), channel_id=1, source_target_pairs={{0,1},{1,0},{2,3},{3,2},{4,5},{5,4},{6,7},{7,6},{8,9},{9,8},{10,11... | collective-permute-start | bytes 6291464 | tf_op jit(solution)/shard_map/ppermute | solution.py:171
  192.4 33.6 %all-to-all-start.1 = ((bf16[16,136,128]{2,1,0:T(8,128)(2,1)}), bf16[16,136,128]{2,1,0:T(8,128)(2,1)}, u32[]{:S(2)}, u32[]{:S(2)}) async-start(bf16[16,136,128]{2,1,0:T(8,128)(2,1)} %bitcast.6), calls=%async_computation.1 | async-start | bytes 1114112 | tf_op jit(solution)/shard_map/all_to_all | solution.py:166
  197.7 2.2 copy-start.3
  (2 other events, 1.7 us)
where the time goes:
time: 230 us; the launch traced here: 228 us
  starting transfers between devices  91.8 us (40%)
  waiting for transfers between devices  64.6 us (28%)
  local copies, waits for them, and re-layouts  22.1 us (10%)
  Pallas kernels  19.9 us (9%)
  blocking collectives  19.5 us (8%)
  matrix products  6.59 us (3%)
  other arithmetic  2.41 us (1%)
    ppermute x18, starting transfers between devices, shifted(): lax.ppermute(x, axis, [(place, (place + step) % count) for place in range...  55.7 us
    all_to_all x4, waiting for transfers between devices, exchanged(): return lax.all_to_all(x, axis, split_axis=0, concat_axis=0, tiled=True)  51.4 us
    all_to_all x4, starting transfers between devices, exchanged(): return lax.all_to_all(x, axis, split_axis=0, concat_axis=0, tiled=True)  36.1 us
    all_to_all x1, blocking collectives, exchanged(): return lax.all_to_all(x, axis, split_axis=0, concat_axis=0, tiled=True)  19.5 us
    ppermute x18, waiting for transfers between devices, shifted(): lax.ppermute(x, axis, [(place, (place + step) % count) for place in range...  13.2 us
    pallas_call x1, Pallas kernels, shards(): pl.pallas_call(attention_kernel, out_shape=(shaped(length, LANES), shaped...  13 us
    dynamic_update_slice x8, local copies, waits for them, and re-layouts, placed(): lax.dynamic_update_index_in_dim(whole, part, (here - step) % count, 0)  7.78 us
    unnamed x20, local copies, waits for them, and re-layouts  5.22 us
  transfers between devices with their start and end apart: 22, of which 9 were waited for; matrix products, arithmetic and copies ran while one was open for 12% of the time, Pallas kernels for 8%

commit v1 on v0

--- a/solution.py
+++ b/solution.py
@@ -47,41 +47,57 @@
     return op(x.reshape(x.shape[0] // 8, 8, x.shape[1]), axis=0)
 
 
-def attention_kernel(
-    x_ref, p_ref, qk_ref, v_out_ref, kq_ref, kt_ref, pc_ref, acc_ref, dq_ref, s_ref, d_ref
-):
-    length = x_ref.shape[0]
-    scale = HEAD_DIM**-0.5
-    blocks = [(b, min(TILE, length - b)) for b in range(0, length, TILE)]
-    for base, rows in blocks:
+def blocks_of(length):
+    return [(base, min(TILE, length - base)) for base in range(0, length, TILE)]
+
+
+def spread(x_ref, p_ref, kq_ref, pc_ref, acc_ref, kt_ref=None):
+    for base, rows in blocks_of(x_ref.shape[0]):
         here = slice(base, base + rows)
-        wide = x_ref[here, :LANES].astype(jnp.float32)
-        swapped = rolled(wide)
+        swapped = rolled(x_ref[here, :LANES].astype(jnp.float32))
         kq_ref[here] = swapped.astype(jnp.bfloat16)
-        kt_ref[:, here] = swapped.T[:HEAD_DIM].astype(jnp.bfloat16)
+        if kt_ref is not None:
+            kt_ref[:, here] = swapped.T[:HEAD_DIM].astype(jnp.bfloat16)
         pc_ref[here] = jnp.broadcast_to(p_ref[:, here], (LANES, rows)).T
         acc_ref[here] = jnp.zeros((rows, LANES), jnp.float32)
+
+
+def query_block(x_ref, here, low):
+    wide = x_ref[here, :LANES].astype(jnp.float32)
+    scaled = jnp.where(low, wide * HEAD_DIM**-0.5, 0.0).astype(jnp.bfloat16)
+    return scaled, jnp.where(low, 0.0, rolled(wide)).astype(jnp.bfloat16)
+
+
+def grad_block(x_ref, here, low):
+    wide = rolled(x_ref[here, LANES:].astype(jnp.float32))
+    return jnp.where(low, wide, 0.0).astype(jnp.bfloat16)
+
+
+def score_tile(kq_ref, pc_ref, query_low, q_base, u_base, u_rows):
+    q_rows = query_low.shape[0]
+    shift = pc_ref[q_base : q_base + 1, :] - pc_ref[u_base : u_base + u_rows]
+    shift = jnp.concatenate([shift] * (q_rows // LANES), axis=1)
+    scores = dot_nt(kq_ref[u_base : u_base + u_rows], query_low) + shift
+    if u_base != q_base:
+        return scores
+    place = lax.broadcasted_iota(jnp.int32, scores.shape, 0)
+    seen = place <= lax.broadcasted_iota(jnp.int32, scores.shape, 1)
+    return jnp.where(seen, scores, FLOOR)
+
+
+def value_kernel(x_ref, p_ref, v_out_ref, peak_ref, share_ref, kq_ref, pc_ref, acc_ref, s_ref):
+    length = x_ref.shape[0]
+    blocks = blocks_of(length)
+    spread(x_ref, p_ref, kq_ref, pc_ref, acc_ref)
     for index, (q_base, q_rows) in enumerate(blocks):
         q_here = slice(q_base, q_base + q_rows)
         low = low_lanes((q_rows, LANES))
-        query_wide = x_ref[q_here, :LANES].astype(jnp.float32)
-        grad_wide = rolled(x_ref[q_here, LANES:].astype(jnp.float32))
-        query_low = jnp.where(low, query_wide * scale, 0.0).astype(jnp.bfloat16)
-        query_high = jnp.where(low, 0.0, rolled(query_wide)).astype(jnp.bfloat16)
-        grad_low = jnp.where(low, grad_wide, 0.0).astype(jnp.bfloat16)
-        pivot = pc_ref[q_base : q_base + 1, :]
+        query_low, _ = query_block(x_ref, q_here, low)
+        grad_low = grad_block(x_ref, q_here, low)
         peak = jnp.full((8, q_rows), FLOOR, jnp.float32)
         for u_base, u_rows in blocks[: index + 1]:
-            u_here = slice(u_base, u_base + u_rows)
-            shift = pivot - pc_ref[u_here]
-            shift = jnp.concatenate([shift] * (q_rows // LANES), axis=1)
-            scores = dot_nt(kq_ref[u_here], query_low) + shift
-            if u_base == q_base:
-                seen = lax.broadcasted_iota(jnp.int32, scores.shape, 0) <= lax.broadcasted_iota(
-                    jnp.int32, scores.shape, 1
-                )
-                scores = jnp.where(seen, scores, FLOOR)
-            s_ref[u_here, :q_rows] = scores
+            scores = score_tile(kq_ref, pc_ref, query_low, q_base, u_base, u_rows)
+            s_ref[u_base : u_base + u_rows, :q_rows] = scores
             peak = jnp.maximum(peak, folded(scores, jnp.max))
         peak = jnp.max(peak, axis=0, keepdims=True)
         total = jnp.zeros((8, q_rows), jnp.float32)
@@ -91,31 +107,12 @@
             s_ref[u_here, :q_rows] = raised
             total = total + folded(raised, jnp.sum)
         share = 1.0 / jnp.sum(total, axis=0, keepdims=True)
-        term = jnp.zeros((8, q_rows), jnp.float32)
+        peak_ref[:, q_here] = peak
+        share_ref[:, q_here] = share
         for u_base, u_rows in blocks[: index + 1]:
             u_here = slice(u_base, u_base + u_rows)
             soft = s_ref[u_here, :q_rows] * share
-            s_ref[u_here, :q_rows] = soft
             acc_ref[u_here] += dot_nn(soft.astype(jnp.bfloat16), grad_low)
-            soft_grad = dot_nt(x_ref[u_here, LANES:], grad_low)
-            d_ref[u_here, :q_rows] = soft_grad
-            term = term + folded(soft * soft_grad, jnp.sum)
-        term = jnp.sum(term, axis=0, keepdims=True)
-        query_grad = jnp.zeros((HEAD_DIM, q_rows), jnp.float32)
-        for u_base, u_rows in blocks[: index + 1]:
-            u_here = slice(u_base, u_base + u_rows)
-            score_low = (s_ref[u_here, :q_rows] * (d_ref[u_here, :q_rows] - term)).astype(
-                jnp.bfloat16
-            )
-            acc_ref[u_here] += dot_nn(score_low, query_high)
-            query_grad = query_grad + dot_nn(kt_ref[:, u_here], score_low)
-        query_grad = jnp.concatenate([query_grad, jnp.zeros_like(query_grad)], axis=0)
-        dq_ref[q_here] = query_grad.T
-    for base, rows in blocks:
-        here = slice(base, base + rows)
-        qk_ref[here] = (
-            jnp.where(low_lanes((rows, LANES)), dq_ref[here], acc_ref[here]) * scale
-        ).astype(jnp.bfloat16)
     planes, kept, _ = v_out_ref.shape
     tokens = length // planes
     for plane in range(planes):
@@ -128,13 +125,54 @@
         )
 
 
-def unpack_value_kernel(x_ref, rows_ref, parts_ref):
+def pair_kernel(
+    x_ref, p_ref, peak_ref, share_ref, qk_ref, kq_ref, kt_ref, pc_ref, acc_ref, s_ref, d_ref
+):
+    blocks = blocks_of(x_ref.shape[0])
+    scale = HEAD_DIM**-0.5
+    spread(x_ref, p_ref, kq_ref, pc_ref, acc_ref, kt_ref)
+    for index, (q_base, q_rows) in enumerate(blocks):
+        q_here = slice(q_base, q_base + q_rows)
+        low = low_lanes((q_rows, LANES))
+        query_low, query_high = query_block(x_ref, q_here, low)
+        grad_low = grad_block(x_ref, q_here, low)
+        peak = peak_ref[:, q_here]
+        share = share_ref[:, q_here]
+        term = jnp.zeros((8, q_rows), jnp.float32)
+        for u_base, u_rows in blocks[: index + 1]:
+            u_here = slice(u_base, u_base + u_rows)
+            scores = score_tile(kq_ref, pc_ref, query_low, q_base, u_base, u_rows)
+            soft = jnp.exp(scores - peak) * share
+            s_ref[u_here, :q_rows] = soft
+            soft_grad = dot_nt(x_ref[u_here, LANES:], grad_low)
+            d_ref[u_here, :q_rows] = soft_grad
+            term = term + folded(soft * soft_grad, jnp.sum)
+        term = jnp.sum(term, axis=0, keepdims=True)
+        query_grad = jnp.zeros((HEAD_DIM, q_rows), jnp.float32)
+        for u_base, u_rows in blocks[: index + 1]:
+            u_here = slice(u_base, u_base + u_rows)
+            score_low = (s_ref[u_here, :q_rows] * (d_ref[u_here, :q_rows] - term)).astype(
+                jnp.bfloat16
+            )
+            acc_ref[u_here] += dot_nn(score_low, query_high)
+            query_grad = query_grad + dot_nn(kt_ref[:, u_here], score_low)
+        query_grad = jnp.concatenate([query_grad, jnp.zeros_like(query_grad)], axis=0)
+        acc_ref[q_here] += query_grad.T
+    for base, rows in blocks:
+        here = slice(base, base + rows)
+        qk_ref[here] = (acc_ref[here] * scale).astype(jnp.bfloat16)
+
+
+def unpack_value_kernel(place_ref, x_ref, rows_ref, mine_ref, away_ref):
     heads, kept, _ = x_ref.shape
-    cores, columns, tokens, _ = parts_ref.shape
+    cores = rows_ref.shape[0]
+    columns, tokens, _ = mine_ref.shape
     rest = tokens - kept
     quarter = LANES // heads * columns
     lane = lax.broadcasted_iota(jnp.int32, (tokens, LANES), 1)
+    first_core = place_ref[0] == 0
     for column in range(columns):
+        step = (column + columns - place_ref[1]) % columns
         parts = [jnp.zeros((tokens, LANES), jnp.float32)] * cores
         for group in range(heads // columns):
             block = x_ref[group * columns + column].astype(jnp.float32)
@@ -145,10 +183,12 @@
                 moved = jnp.concatenate([top, bottom], axis=0)
                 inside = (lane >= home) & (lane < home + quarter)
                 parts[core] = jnp.where(inside, moved, parts[core])
-        for core in range(cores):
-            part = parts[core].astype(jnp.bfloat16)
-            parts_ref[core, column] = part
-            rows_ref[core, :, column * LANES : (column + 1) * LANES] = part
+        mine = jnp.where(first_core, parts[0], parts[1]).astype(jnp.bfloat16)
+        away = jnp.where(first_core, parts[1], parts[0]).astype(jnp.bfloat16)
+        mine_ref[step] = mine
+        away_ref[step] = away
+        rows_ref[0, :, column * LANES : (column + 1) * LANES] = mine
+        rows_ref[1, :, column * LANES : (column + 1) * LANES] = away
 
 
 def unpack_pair_kernel(x_ref, q_ref, k_ref):
@@ -217,37 +257,47 @@
         query_vectors[0], key_vectors[0], value_vectors[0], cotangent[0]
     )
     arrived = exchanged(packed, "sp")
-    input_rows = jnp.concatenate(from_all(inputs[0], "x"), axis=0)
-    input_rows = jnp.concatenate(from_all(input_rows, "core"), axis=0)
+    own_rows = jnp.stack(from_all(inputs[0], "x"))
+    input_rows = jnp.stack([own_rows, shifted(own_rows, "core", 1)], axis=1)
+    input_rows = input_rows.reshape(cores * columns * tokens, model)
     weight_line = placed(from_all(weight_block, "y"), "y")
     weight_half = placed(from_all(weight_line, "x"), "x")
     weight_halves = from_all(weight_half, "core")
     kept = (tokens // 2 + 7) // 8 * 8
-    pair_grad, value_grad = pl.pallas_call(
-        attention_kernel,
-        out_shape=(shaped(length, LANES), shaped(planes, kept, LANES)),
+    arrived, input_rows = lax.optimization_barrier((arrived, input_rows))
+    sequence = arrived.reshape(length, 2 * LANES)
+    wide, tile = pltpu.VMEM((length, LANES), jnp.float32), pltpu.VMEM((length, TILE), jnp.float32)
+    row = shaped(1, length, dtype=jnp.float32)
+    value_grad, peak, share = pl.pallas_call(
+        value_kernel,
+        out_shape=(shaped(planes, kept, LANES), row, row),
+        scratch_shapes=[pltpu.VMEM((length, LANES), jnp.bfloat16), wide, wide, tile],
+    )(sequence, gate_prefix[0])
+    value_back = exchanged(value_grad, "sp")
+    pair_grad = pl.pallas_call(
+        pair_kernel,
+        out_shape=shaped(length, LANES),
         scratch_shapes=[
             pltpu.VMEM((length, LANES), jnp.bfloat16),
             pltpu.VMEM((HEAD_DIM, length), jnp.bfloat16),
-            pltpu.VMEM((length, LANES), jnp.float32),
-            pltpu.VMEM((length, LANES), jnp.float32),
-            pltpu.VMEM((length, LANES), jnp.float32),
-            pltpu.VMEM((length, TILE), jnp.float32),
-            pltpu.VMEM((length, TILE), jnp.float32),
+            wide,
+            wide,
+            tile,
+            tile,
         ],
-    )(arrived.reshape(length, 2 * LANES), gate_prefix[0])
-    value_back = exchanged(value_grad, "sp")
+    )(sequence, gate_prefix[0], peak, share)
     pair_back = exchanged(pair_grad.reshape(planes, tokens, LANES), "sp")
-    value_rows, value_parts = pl.pallas_call(
+    place = jnp.stack([core, lax.axis_index("x")]).astype(jnp.int32)
+    block = shaped(columns, tokens, LANES)
+    whole = pl.BlockSpec(memory_space=pltpu.VMEM)
+    value_rows, mine, away = pl.pallas_call(
         unpack_value_kernel,
-        out_shape=(shaped(cores, tokens, width // cores), shaped(cores, columns, tokens, LANES)),
-    )(value_back)
-    away = shifted(block_of(value_parts, 1 - core), "core", 1)
-    both = jnp.concatenate([block_of(value_parts, core), away], axis=1)
-    pieces = sent_blocks(both, "x")
-    value_cols = jnp.concatenate(
-        [piece[:tokens] for piece in pieces] + [piece[tokens:] for piece in pieces], axis=0
-    )
+        out_shape=(shaped(cores, tokens, width // cores), block, block),
+        in_specs=[pl.BlockSpec(memory_space=pltpu.SMEM), whole],
+    )(place, value_back)
+    both = jnp.stack([mine, shifted(away, "core", 1)], axis=1)
+    pieces = [both[0]] + [shifted(both[step], "x", step) for step in range(1, columns)]
+    value_cols = jnp.stack(pieces).reshape(columns * cores * tokens, LANES)
     partial = lax.dot_general(
         value_cols, input_rows, (((0,), (0,)), ((), ())), preferred_element_type=jnp.float32
     ).astype(jnp.bfloat16)
@@ -261,12 +311,12 @@
     )(pair_back)
     input_grad = sum(
         lax.dot_general(
-            block_of(value_rows, place),
+            value_rows[place],
             half,
             (((1,), (0,)), ((), ())),
             preferred_element_type=jnp.float32,
         )
-        for place, half in zip((core, 1 - core), weight_halves)
+        for place, half in enumerate(weight_halves)
     ).astype(jnp.bfloat16)
     return (query_grad[None], key_grad[None], input_grad[None], weight_grad)
 

time: 230 us -> 237 us (1.030)
  the two profiles are of different devices: /device:TPU:38 before, /device:TPU:58 now
where the time goes in v1:
time: 237 us; the launch traced here: 235 us
  starting transfers between devices  106 us (45%)
  waiting for transfers between devices  72.1 us (30%)
  Pallas kernels  24.9 us (11%)
  local copies, waits for them, and re-layouts  15.7 us (7%)
  other arithmetic  9.13 us (4%)
  matrix products  6.45 us (3%)
    ppermute x18, starting transfers between devices, shifted(): lax.ppermute(x, axis, [(place, (place + step) % count) for place in range...  54 us
    all_to_all x5, starting transfers between devices, exchanged(): return lax.all_to_all(x, axis, split_axis=0, concat_axis=0, tiled=True)  51.6 us
    all_to_all x5, waiting for transfers between devices, exchanged(): return lax.all_to_all(x, axis, split_axis=0, concat_axis=0, tiled=True)  45.3 us
    ppermute x18, waiting for transfers between devices, shifted(): lax.ppermute(x, axis, [(place, (place + step) % count) for place in range...  26.9 us
    pallas_call x1, Pallas kernels, shards(): pl.pallas_call(pair_kernel, out_shape=shaped(length, LANES), scratch_shap...  9.66 us
    pallas_call x1, Pallas kernels, shards(): pl.pallas_call(value_kernel, out_shape=(shaped(planes, kept, LANES), row,...  8.28 us
    dynamic_update_slice x8, local copies, waits for them, and re-layouts, placed(): lax.dynamic_update_index_in_dim(whole, part, (here - step) % count, 0)  7.64 us
    another operation x2, other arithmetic, shards(): input_rows = jnp.stack([own_rows, shifted(own_rows, 'core', 1)], axis=1)  6.88 us
  transfers between devices with their start and end apart: 23, of which 11 were waited for; matrix products, arithmetic and copies ran while one was open for 12% of the time, Pallas kernels for 10%

profile of v1, /device:TPU:58, one launch (start us, length us, event | category | flops | bytes accessed | tf_op | source)
XLA Modules:
  0.0 235.1 jit_solution(9514359978538869797)
XLA Ops:
  2.0 15.2 %all-to-all-start.3 = ((bf16[16,32,128]{2,1,0:T(8,128)(2,1)}), bf16[16,32,128]{2,1,0:T(8,128)(2,1)S(1)}, u32[]{:S(2)}, u32[]{:S(2)}) async-start(bf16[16,32,128]{2,1,0:T(8,128)(2,1)} %broadcast_in_dim.48), calls=%async_computation.3 | async-start | bytes 262144 | tf_op jit(solution)/shard_map/all_to_all | solution.py:206
  20.0 11.5 %all-to-all-done.3 = bf16[16,32,128]{2,1,0:T(8,128)(2,1)S(1)} async-done(((bf16[16,32,128]{2,1,0:T(8,128)(2,1)}), bf16[16,32,128]{2,1,0:T(8,128)(2,1)S(1)}, u32[]{:S(2)}, u32[]{:S(2)}) %all-to-all-start.3) | async-done | bytes 131104 | tf_op jit(solution)/shard_map/all_to_all | solution.py:206
  31.4 4.3 %all-to-all-start = ((bf16[16,136,256]{2,1,0:T(8,128)(2,1)}), bf16[16,136,256]{2,1,0:T(8,128)(2,1)S(1)}, u32[]{:S(2)}, u32[]{:S(2)}) async-start(bf16[16,136,256]{2,1,0:T(8,128)(2,1)} %shard_map.102), calls=%async_computation | async-start | bytes 2228224 | tf_op jit(solution)/shard_map/all_to_all | solution.py:206
  35.8 3.4 %collective-permute-start = (bf16[136,2048]{1,0:T(8,128)(2,1)S(1)}, bf16[136,2048]{1,0:T(8,128)(2,1)S(1)}, u32[]{:S(2)}, u32[]{:S(2)}) collective-permute-start(bf16[136,2048]{1,0:T(8,128)(2,1)S(1)} %bitcast.101), channel_id=1, source_target_pairs={{0,2},{2,4},{4,6},{6,0},{1,3},{3,5},{5,7},{7,1},{8,10},{10,12},{12... | collective-permute-start | bytes 1671176 | tf_op jit(solution)/shard_map/ppermute | solution.py:211
  42.2 4.1 %collective-permute-start.2 = (bf16[136,2048]{1,0:T(8,128)(2,1)S(1)}, bf16[136,2048]{1,0:T(8,128)(2,1)S(1)}, u32[]{:S(2)}, u32[]{:S(2)}) collective-permute-start(bf16[136,2048]{1,0:T(8,128)(2,1)S(1)} %bitcast.103), channel_id=1, source_target_pairs={{0,6},{2,0},{4,2},{6,4},{1,7},{3,1},{5,3},{7,5},{8,14},{10,8},{12,... | collective-permute-start | bytes 1671176 | tf_op jit(solution)/shard_map/ppermute | solution.py:211
  46.3 6.9 %collective-permute-done = bf16[136,2048]{1,0:T(8,128)(2,1)S(1)} collective-permute-done((bf16[136,2048]{1,0:T(8,128)(2,1)S(1)}, bf16[136,2048]{1,0:T(8,128)(2,1)S(1)}, u32[]{:S(2)}, u32[]{:S(2)}) %collective-permute-start) | collective-permute-done | bytes 557088 | tf_op jit(solution)/shard_map/ppermute | solution.py:211
  53.1 5.0 %collective-permute-done.1 = bf16[136,2048]{1,0:T(8,128)(2,1)S(1)} collective-permute-done((bf16[136,2048]{1,0:T(8,128)(2,1)S(1)}, bf16[136,2048]{1,0:T(8,128)(2,1)S(1)}, u32[]{:S(2)}, u32[]{:S(2)}) %collective-permute-start.1) | collective-permute-done | bytes 557088 | tf_op jit(solution)/shard_map/ppermute | solution.py:211
  58.1 9.4 %collective-permute-done.2 = bf16[136,2048]{1,0:T(8,128)(2,1)S(1)} collective-permute-done((bf16[136,2048]{1,0:T(8,128)(2,1)S(1)}, bf16[136,2048]{1,0:T(8,128)(2,1)S(1)}, u32[]{:S(2)}, u32[]{:S(2)}) %collective-permute-start.2) | collective-permute-done | bytes 557088 | tf_op jit(solution)/shard_map/ppermute | solution.py:211
  75.1 4.5 %collective-permute-start.5 = (bf16[32,2048]{1,0:T(8,128)(2,1)}, bf16[32,2048]{1,0:T(8,128)(2,1)}, u32[]{:S(2)}, u32[]{:S(2)}) collective-permute-start(bf16[32,2048]{1,0:T(8,128)(2,1)} %copy_bitcast_fusion), channel_id=1, source_target_pairs={{0,16},{8,24},{16,0},{24,8},{1,17},{9,25},{17,1},{25,9},{2,18},{10... | collective-permute-start | bytes 393224 | tf_op jit(solution)/shard_map/ppermute | solution.py:211
  86.3 4.1 %pad_maximum_fusion = bf16[4,2,136,2048]{3,2,1,0:T(8,128)(2,1)} fusion(bf16[4,1,136,2048]{3,2,1,0:T(8,128)(2,1)} %bitcast.10, bf16[4,1,136,2048]{3,2,1,0:T(8,128)(2,1)S(1)} %get-tuple-element.24), kind=kLoop, calls=%fused_computation | loop fusion | flops 2228224 | bytes 8912896 | tf_op jit(solution)/shard_map/stack | solution.py:261
  91.4 8.3 %shard_map.103 = (bf16[16,72,128]{2,1,0:T(8,128)(2,1)}, f32[1,2176]{1,0:T(1,128)}, f32[1,2176]{1,0:T(1,128)}) custom-call(bf16[2176,256]{1,0:T(8,128)(2,1)} %bitcast.92, f32[1,2176]{1,0:T(1,128)} %bitcast.117), custom_call_target="tpu_custom_call" | custom-call | tf_op jit(solution)/shard_map/pallas_call | solution.py:271
  99.7 12.0 %all-to-all-start.2 = ((bf16[16,72,128]{2,1,0:T(8,128)(2,1)}), bf16[16,72,128]{2,1,0:T(8,128)(2,1)S(1)}, u32[]{:S(2)}, u32[]{:S(2)}) async-start(bf16[16,72,128]{2,1,0:T(8,128)(2,1)} %get-tuple-element.19), calls=%async_computation.2 | async-start | bytes 589824 | tf_op jit(solution)/shard_map/all_to_all | solution.py:206
  121.2 3.9 %collective-permute-start.9 = (bf16[128,2048]{1,0:T(8,128)(2,1)}, bf16[128,2048]{1,0:T(8,128)(2,1)S(1)}, u32[]{:S(2)}, u32[]{:S(2)}) collective-permute-start(bf16[128,2048]{1,0:T(8,128)(2,1)} %bitcast.26), channel_id=1, source_target_pairs={{0,6},{2,0},{4,2},{6,4},{1,7},{3,1},{5,3},{7,5},{8,14},{10,8},{12,... | collective-permute-start | bytes 1572872 | tf_op jit(solution)/shard_map/ppermute | solution.py:211
  126.4 4.2 %all-to-all-done.2.x_ref = bf16[16,72,128]{2,1,0:T(8,128)(2,1)S(1)} async-done(((bf16[16,72,128]{2,1,0:T(8,128)(2,1)}), bf16[16,72,128]{2,1,0:T(8,128)(2,1)S(1)}, u32[]{:S(2)}, u32[]{:S(2)}) %all-to-all-start.2) | async-done | bytes 294944 | tf_op jit(solution)/shard_map/all_to_all | solution.py:206
  140.3 3.0 %collective-permute-start.13 = (bf16[2,136,128]{2,1,0:T(8,128)(2,1)S(1)}, bf16[2,136,128]{2,1,0:T(8,128)(2,1)S(1)}, u32[]{:S(2)}, u32[]{:S(2)}) collective-permute-start(bf16[2,136,128]{2,1,0:T(8,128)(2,1)S(1)} %get-tuple-element.32), channel_id=1, source_target_pairs={{0,4},{2,6},{4,0},{6,2},{1,5},{3,7},{5,1},{7,3},{8,12},{10,14},{12... | collective-permute-start | bytes 208904 | tf_op jit(solution)/shard_map/ppermute | solution.py:211
  143.3 3.9 %collective-permute-start.14 = (bf16[2,136,128]{2,1,0:T(8,128)(2,1)S(1)}, bf16[2,136,128]{2,1,0:T(8,128)(2,1)S(1)}, u32[]{:S(2)}, u32[]{:S(2)}) collective-permute-start(bf16[2,136,128]{2,1,0:T(8,128)(2,1)S(1)} %get-tuple-element.31), channel_id=1, source_target_pairs={{0,6},{2,0},{4,2},{6,4},{1,7},{3,1},{5,3},{7,5},{8,14},{10,8},{12,... | collective-permute-start | bytes 208904 | tf_op jit(solution)/shard_map/ppermute | solution.py:211
  149.5 3.1 %convolution_convert_fusion = bf16[128,2048]{1,0:T(8,128)(2,1)S(1)} fusion(bf16[1088,128]{1,0:T(8,128)(2,1)S(1)} %bitcast.100, bf16[1088,2048]{1,0:T(8,128)(2,1)} %bitcast.91), kind=kOutput, calls=%fused_computation.3 | convolution fusion | flops 570687488 | bytes 5259264 | tf_op jit(solution)/shard_map/dot_general | solution.py:301
  152.7 4.7 %collective-permute-start.15 = (bf16[32,2048]{1,0:T(8,128)(2,1)S(1)}, bf16[32,2048]{1,0:T(8,128)(2,1)S(1)}, u32[]{:S(2)}, u32[]{:S(2)}) collective-permute-start(bf16[32,2048]{1,0:T(8,128)(2,1)S(1)} %get-tuple-element.26), channel_id=1, source_target_pairs={{0,8},{8,16},{16,24},{24,0},{1,9},{9,17},{17,25},{25,1},{2,10},{10... | collective-permute-start | bytes 393224 | tf_op jit(solution)/shard_map/ppermute | solution.py:211
  159.5 3.3 %collective-permute-start.17 = (bf16[32,2048]{1,0:T(8,128)(2,1)S(1)}, bf16[32,2048]{1,0:T(8,128)(2,1)S(1)}, u32[]{:S(2)}, u32[]{:S(2)}) collective-permute-start(bf16[32,2048]{1,0:T(8,128)(2,1)S(1)} %get-tuple-element.27), channel_id=1, source_target_pairs={{0,24},{8,0},{16,8},{24,16},{1,25},{9,1},{17,9},{25,17},{2,26},{10... | collective-permute-start | bytes 393224 | tf_op jit(solution)/shard_map/ppermute | solution.py:211
  168.9 12.2 %all-to-all-start.4 = ((bf16[16,32,128]{2,1,0:T(8,128)(2,1)}), bf16[16,32,128]{2,1,0:T(8,128)(2,1)S(1)}, u32[]{:S(2)}, u32[]{:S(2)}) async-start(bf16[16,32,128]{2,1,0:T(8,128)(2,1)} %copy.28), calls=%async_computation.4 | async-start | bytes 262144 | tf_op jit(solution)/shard_map/all_to_all | solution.py:206
  181.1 9.7 %shard_map.104 = bf16[2176,128]{1,0:T(8,128)(2,1)} custom-call(bf16[2176,256]{1,0:T(8,128)(2,1)} %bitcast.93, f32[1,2176]{1,0:T(1,128)} %bitcast.118, f32[1,2176]{1,0:T(1,128)} %get-tuple-element.15.peak_ref, f32[1,2176]{1,0:T(1,128)} %get-tuple-element.16.share_ref), custom_call_target="tpu_custom_call" | custom-call | tf_op jit(solution)/shard_map/pallas_call | solution.py:277
  190.8 4.2 %all-to-all-done.4 = bf16[16,32,128]{2,1,0:T(8,128)(2,1)S(1)} async-done(((bf16[16,32,128]{2,1,0:T(8,128)(2,1)}), bf16[16,32,128]{2,1,0:T(8,128)(2,1)S(1)}, u32[]{:S(2)}, u32[]{:S(2)}) %all-to-all-start.4) | async-done | bytes 131104 | tf_op jit(solution)/shard_map/all_to_all | solution.py:206
  195.0 7.8 %all-to-all-start.1 = ((bf16[16,136,128]{2,1,0:T(8,128)(2,1)}), bf16[16,136,128]{2,1,0:T(8,128)(2,1)S(1)}, u32[]{:S(2)}, u32[]{:S(2)}) async-start(bf16[16,136,128]{2,1,0:T(8,128)(2,1)} %bitcast.96), calls=%async_computation.1 | async-start | bytes 1114112 | tf_op jit(solution)/shard_map/all_to_all | solution.py:206
  206.8 25.4 %all-to-all-done.1.x_ref = bf16[16,136,128]{2,1,0:T(8,128)(2,1)S(1)} async-done(((bf16[16,136,128]{2,1,0:T(8,128)(2,1)}), bf16[16,136,128]{2,1,0:T(8,128)(2,1)S(1)}, u32[]{:S(2)}, u32[]{:S(2)}) %all-to-all-start.1) | async-done | bytes 557088 | tf_op jit(solution)/shard_map/all_to_all | solution.py:206
  (64 shorter events, 59.9 us)
Async XLA Ops:
  2.0 29.4 %all-to-all-start.3 = ((bf16[16,32,128]{2,1,0:T(8,128)(2,1)}), bf16[16,32,128]{2,1,0:T(8,128)(2,1)S(1)}, u32[]{:S(2)}, u32[]{:S(2)}) async-start(bf16[16,32,128]{2,1,0:T(8,128)(2,1)} %broadcast_in_dim.48), calls=%async_computation.3 | async-start | bytes 262144 | tf_op jit(solution)/shard_map/all_to_all | solution.py:206
  31.4 58.9 %all-to-all-start = ((bf16[16,136,256]{2,1,0:T(8,128)(2,1)}), bf16[16,136,256]{2,1,0:T(8,128)(2,1)S(1)}, u32[]{:S(2)}, u32[]{:S(2)}) async-start(bf16[16,136,256]{2,1,0:T(8,128)(2,1)} %shard_map.102), calls=%async_computation | async-start | bytes 2228224 | tf_op jit(solution)/shard_map/all_to_all | solution.py:206
  35.8 17.4 %collective-permute-start = (bf16[136,2048]{1,0:T(8,128)(2,1)S(1)}, bf16[136,2048]{1,0:T(8,128)(2,1)S(1)}, u32[]{:S(2)}, u32[]{:S(2)}) collective-permute-start(bf16[136,2048]{1,0:T(8,128)(2,1)S(1)} %bitcast.101), channel_id=1, source_target_pairs={{0,2},{2,4},{4,6},{6,0},{1,3},{3,5},{5,7},{7,1},{8,10},{10,12},{12... | collective-permute-start | bytes 1671176 | tf_op jit(solution)/shard_map/ppermute | solution.py:211
  39.2 18.9 %collective-permute-start.1 = (bf16[136,2048]{1,0:T(8,128)(2,1)S(1)}, bf16[136,2048]{1,0:T(8,128)(2,1)S(1)}, u32[]{:S(2)}, u32[]{:S(2)}) collective-permute-start(bf16[136,2048]{1,0:T(8,128)(2,1)S(1)} %bitcast.102), channel_id=1, source_target_pairs={{0,4},{2,6},{4,0},{6,2},{1,5},{3,7},{5,1},{7,3},{8,12},{10,14},{12... | collective-permute-start | bytes 1671176 | tf_op jit(solution)/shard_map/ppermute | solution.py:211
  42.2 25.3 %collective-permute-start.2 = (bf16[136,2048]{1,0:T(8,128)(2,1)S(1)}, bf16[136,2048]{1,0:T(8,128)(2,1)S(1)}, u32[]{:S(2)}, u32[]{:S(2)}) collective-permute-start(bf16[136,2048]{1,0:T(8,128)(2,1)S(1)} %bitcast.103), channel_id=1, source_target_pairs={{0,6},{2,0},{4,2},{6,4},{1,7},{3,1},{5,3},{7,5},{8,14},{10,8},{12,... | collective-permute-start | bytes 1671176 | tf_op jit(solution)/shard_map/ppermute | solution.py:211
  70.3 16.0 %collective-permute-start.3 = (bf16[4,136,2048]{2,1,0:T(8,128)(2,1)}, bf16[4,136,2048]{2,1,0:T(8,128)(2,1)}, u32[]{:S(2)}, u32[]{:S(2)}) collective-permute-start(bf16[4,136,2048]{2,1,0:T(8,128)(2,1)} %get-tuple-element.25), channel_id=1, source_target_pairs={{0,1},{1,0},{2,3},{3,2},{4,5},{5,4},{6,7},{7,6},{8,9},{9,8},{10,11... | collective-permute-start | bytes 6684680 | tf_op jit(solution)/shard_map/ppermute | solution.py:211
  73.0 11.8 %collective-permute-start.4 = (bf16[32,2048]{1,0:T(8,128)(2,1)}, bf16[32,2048]{1,0:T(8,128)(2,1)}, u32[]{:S(2)}, u32[]{:S(2)}) collective-permute-start(bf16[32,2048]{1,0:T(8,128)(2,1)} %copy_bitcast_fusion), channel_id=1, source_target_pairs={{0,8},{8,16},{16,24},{24,0},{1,9},{9,17},{17,25},{25,1},{2,10},{10... | collective-permute-start | bytes 393224 | tf_op jit(solution)/shard_map/ppermute | solution.py:211
  75.1 36.6 %collective-permute-start.5 = (bf16[32,2048]{1,0:T(8,128)(2,1)}, bf16[32,2048]{1,0:T(8,128)(2,1)}, u32[]{:S(2)}, u32[]{:S(2)}) collective-permute-start(bf16[32,2048]{1,0:T(8,128)(2,1)} %copy_bitcast_fusion), channel_id=1, source_target_pairs={{0,16},{8,24},{16,0},{24,8},{1,17},{9,25},{17,1},{25,9},{2,18},{10... | collective-permute-start | bytes 393224 | tf_op jit(solution)/shard_map/ppermute | solution.py:211
  79.6 33.7 %collective-permute-start.6 = (bf16[32,2048]{1,0:T(8,128)(2,1)}, bf16[32,2048]{1,0:T(8,128)(2,1)}, u32[]{:S(2)}, u32[]{:S(2)}) collective-permute-start(bf16[32,2048]{1,0:T(8,128)(2,1)} %copy_bitcast_fusion), channel_id=1, source_target_pairs={{0,24},{8,0},{16,8},{24,16},{1,25},{9,1},{17,9},{25,17},{2,26},{10... | collective-permute-start | bytes 393224 | tf_op jit(solution)/shard_map/ppermute | solution.py:211
  99.7 31.0 %all-to-all-start.2 = ((bf16[16,72,128]{2,1,0:T(8,128)(2,1)}), bf16[16,72,128]{2,1,0:T(8,128)(2,1)S(1)}, u32[]{:S(2)}, u32[]{:S(2)}) async-start(bf16[16,72,128]{2,1,0:T(8,128)(2,1)} %get-tuple-element.19), calls=%async_computation.2 | async-start | bytes 589824 | tf_op jit(solution)/shard_map/all_to_all | solution.py:206
  114.8 20.5 %collective-permute-start.7 = (bf16[128,2048]{1,0:T(8,128)(2,1)}, bf16[128,2048]{1,0:T(8,128)(2,1)S(1)}, u32[]{:S(2)}, u32[]{:S(2)}) collective-permute-start(bf16[128,2048]{1,0:T(8,128)(2,1)} %bitcast.26), channel_id=1, source_target_pairs={{0,2},{2,4},{4,6},{6,0},{1,3},{3,5},{5,7},{7,1},{8,10},{10,12},{12... | collective-permute-start | bytes 1572872 | tf_op jit(solution)/shard_map/ppermute | solution.py:211
  118.1 29.1 %collective-permute-start.8 = (bf16[128,2048]{1,0:T(8,128)(2,1)}, bf16[128,2048]{1,0:T(8,128)(2,1)}, u32[]{:S(2)}, u32[]{:S(2)}) collective-permute-start(bf16[128,2048]{1,0:T(8,128)(2,1)} %bitcast.26), channel_id=1, source_target_pairs={{0,4},{2,6},{4,0},{6,2},{1,5},{3,7},{5,1},{7,3},{8,12},{10,14},{12... | collective-permute-start | bytes 1572872 | tf_op jit(solution)/shard_map/ppermute | solution.py:211
  121.2 41.6 %collective-permute-start.9 = (bf16[128,2048]{1,0:T(8,128)(2,1)}, bf16[128,2048]{1,0:T(8,128)(2,1)S(1)}, u32[]{:S(2)}, u32[]{:S(2)}) collective-permute-start(bf16[128,2048]{1,0:T(8,128)(2,1)} %bitcast.26), channel_id=1, source_target_pairs={{0,6},{2,0},{4,2},{6,4},{1,7},{3,1},{5,3},{7,5},{8,14},{10,8},{12,... | collective-permute-start | bytes 1572872 | tf_op jit(solution)/shard_map/ppermute | solution.py:211
  133.4 3.5 %collective-permute-start.11 = (bf16[4,136,128]{2,1,0:T(8,128)(2,1)}, bf16[4,136,128]{2,1,0:T(8,128)(2,1)S(1)}, u32[]{:S(2)}, u32[]{:S(2)}) collective-permute-start(bf16[4,136,128]{2,1,0:T(8,128)(2,1)} %get-tuple-element.22), channel_id=1, source_target_pairs={{0,1},{1,0},{2,3},{3,2},{4,5},{5,4},{6,7},{7,6},{8,9},{9,8},{10,11... | collective-permute-start | bytes 417800 | tf_op jit(solution)/shard_map/ppermute | solution.py:211
  137.7 10.6 %collective-permute-start.12 = (bf16[2,136,128]{2,1,0:T(8,128)(2,1)S(1)}, bf16[2,136,128]{2,1,0:T(8,128)(2,1)S(1)}, u32[]{:S(2)}, u32[]{:S(2)}) collective-permute-start(bf16[2,136,128]{2,1,0:T(8,128)(2,1)S(1)} %get-tuple-element.30), channel_id=1, source_target_pairs={{0,2},{2,4},{4,6},{6,0},{1,3},{3,5},{5,7},{7,1},{8,10},{10,12},{12... | collective-permute-start | bytes 208904 | tf_op jit(solution)/shard_map/ppermute | solution.py:211
  140.3 8.1 %collective-permute-start.13 = (bf16[2,136,128]{2,1,0:T(8,128)(2,1)S(1)}, bf16[2,136,128]{2,1,0:T(8,128)(2,1)S(1)}, u32[]{:S(2)}, u32[]{:S(2)}) collective-permute-start(bf16[2,136,128]{2,1,0:T(8,128)(2,1)S(1)} %get-tuple-element.32), channel_id=1, source_target_pairs={{0,4},{2,6},{4,0},{6,2},{1,5},{3,7},{5,1},{7,3},{8,12},{10,14},{12... | collective-permute-start | bytes 208904 | tf_op jit(solution)/shard_map/ppermute | solution.py:211
  143.3 6.2 %collective-permute-start.14 = (bf16[2,136,128]{2,1,0:T(8,128)(2,1)S(1)}, bf16[2,136,128]{2,1,0:T(8,128)(2,1)S(1)}, u32[]{:S(2)}, u32[]{:S(2)}) collective-permute-start(bf16[2,136,128]{2,1,0:T(8,128)(2,1)S(1)} %get-tuple-element.31), channel_id=1, source_target_pairs={{0,6},{2,0},{4,2},{6,4},{1,7},{3,1},{5,3},{7,5},{8,14},{10,8},{12,... | collective-permute-start | bytes 208904 | tf_op jit(solution)/shard_map/ppermute | solution.py:211
  152.7 12.4 %collective-permute-start.15 = (bf16[32,2048]{1,0:T(8,128)(2,1)S(1)}, bf16[32,2048]{1,0:T(8,128)(2,1)S(1)}, u32[]{:S(2)}, u32[]{:S(2)}) collective-permute-start(bf16[32,2048]{1,0:T(8,128)(2,1)S(1)} %get-tuple-element.26), channel_id=1, source_target_pairs={{0,8},{8,16},{16,24},{24,0},{1,9},{9,17},{17,25},{25,1},{2,10},{10... | collective-permute-start | bytes 393224 | tf_op jit(solution)/shard_map/ppermute | solution.py:211
  157.4 9.6 %collective-permute-start.16 = (bf16[32,2048]{1,0:T(8,128)(2,1)S(1)}, bf16[32,2048]{1,0:T(8,128)(2,1)S(1)}, u32[]{:S(2)}, u32[]{:S(2)}) collective-permute-start(bf16[32,2048]{1,0:T(8,128)(2,1)S(1)} %get-tuple-element.28), channel_id=1, source_target_pairs={{0,16},{8,24},{16,0},{24,8},{1,17},{9,25},{17,1},{25,9},{2,18},{10... | collective-permute-start | bytes 393224 | tf_op jit(solution)/shard_map/ppermute | solution.py:211
  159.5 8.7 %collective-permute-start.17 = (bf16[32,2048]{1,0:T(8,128)(2,1)S(1)}, bf16[32,2048]{1,0:T(8,128)(2,1)S(1)}, u32[]{:S(2)}, u32[]{:S(2)}) collective-permute-start(bf16[32,2048]{1,0:T(8,128)(2,1)S(1)} %get-tuple-element.27), channel_id=1, source_target_pairs={{0,24},{8,0},{16,8},{24,16},{1,25},{9,1},{17,9},{25,17},{2,26},{10... | collective-permute-start | bytes 393224 | tf_op jit(solution)/shard_map/ppermute | solution.py:211
  162.8 40.0 %copy-start.4 = (bf16[2,136,512]{2,1,0:T(8,128)(2,1)S(1)}, bf16[2,136,512]{2,1,0:T(8,128)(2,1)}, u32[]{:S(2)}) copy-start(bf16[2,136,512]{2,1,0:T(8,128)(2,1)} %get-tuple-element.20) | copy-start | bytes 835588
  162.9 40.0 %collective-permute-start.10 = (bf16[512,2048]{1,0:T(8,128)(2,1)S(1)}, bf16[512,2048]{1,0:T(8,128)(2,1)}, u32[]{:S(2)}, u32[]{:S(2)}) collective-permute-start(bf16[512,2048]{1,0:T(8,128)(2,1)S(1)} %bitcast.94), channel_id=1, source_target_pairs={{0,1},{1,0},{2,3},{3,2},{4,5},{5,4},{6,7},{7,6},{8,9},{9,8},{10,11... | collective-permute-start | bytes 6291464 | tf_op jit(solution)/shard_map/ppermute | solution.py:211
  168.9 26.1 %all-to-all-start.4 = ((bf16[16,32,128]{2,1,0:T(8,128)(2,1)}), bf16[16,32,128]{2,1,0:T(8,128)(2,1)S(1)}, u32[]{:S(2)}, u32[]{:S(2)}) async-start(bf16[16,32,128]{2,1,0:T(8,128)(2,1)} %copy.28), calls=%async_computation.4 | async-start | bytes 262144 | tf_op jit(solution)/shard_map/all_to_all | solution.py:206
  195.0 37.2 %all-to-all-start.1 = ((bf16[16,136,128]{2,1,0:T(8,128)(2,1)}), bf16[16,136,128]{2,1,0:T(8,128)(2,1)S(1)}, u32[]{:S(2)}, u32[]{:S(2)}) async-start(bf16[16,136,128]{2,1,0:T(8,128)(2,1)} %bitcast.96), calls=%async_computation.1 | async-start | bytes 1114112 | tf_op jit(solution)/shard_map/all_to_all | solution.py:206
  (4 other events, 21.1 us)

commit v2 on v1

--- a/solution.py
+++ b/solution.py
@@ -163,12 +163,12 @@
         qk_ref[here] = (acc_ref[here] * scale).astype(jnp.bfloat16)
 
 
-def unpack_value_kernel(place_ref, x_ref, rows_ref, mine_ref, away_ref):
+def unpack_value_kernel(place_ref, x_ref, mine_ref, away_ref):
     heads, kept, _ = x_ref.shape
-    cores = rows_ref.shape[0]
     columns, tokens, _ = mine_ref.shape
     rest = tokens - kept
-    quarter = LANES // heads * columns
+    cores = HEAD_DIM * columns // LANES
+    quarter = HEAD_DIM // cores
     lane = lax.broadcasted_iota(jnp.int32, (tokens, LANES), 1)
     first_core = place_ref[0] == 0
     for column in range(columns):
@@ -183,12 +183,63 @@
                 moved = jnp.concatenate([top, bottom], axis=0)
                 inside = (lane >= home) & (lane < home + quarter)
                 parts[core] = jnp.where(inside, moved, parts[core])
-        mine = jnp.where(first_core, parts[0], parts[1]).astype(jnp.bfloat16)
-        away = jnp.where(first_core, parts[1], parts[0]).astype(jnp.bfloat16)
-        mine_ref[step] = mine
-        away_ref[step] = away
-        rows_ref[0, :, column * LANES : (column + 1) * LANES] = mine
-        rows_ref[1, :, column * LANES : (column + 1) * LANES] = away
+        mine_ref[step] = jnp.where(first_core, parts[0], parts[1]).astype(jnp.bfloat16)
+        away_ref[step] = jnp.where(first_core, parts[1], parts[0]).astype(jnp.bfloat16)
+
+
+def weight_open_kernel(x_ref, out_ref):
+    for plane in range(x_ref.shape[0]):
+        out_ref[:, plane * LANES : (plane + 1) * LANES] = x_ref[plane]
+
+
+def weight_line_kernel(place_ref, *refs):
+    pieces, out_ref = refs[:-1], refs[-1]
+    lines = out_ref.shape[0]
+    for step, piece_ref in enumerate(pieces):
+        out_ref[(place_ref[2] + lines - step) % lines] = piece_ref[...]
+
+
+def stack_kernel(*refs):
+    for step, piece_ref in enumerate(refs[:-1]):
+        refs[-1][step] = piece_ref[...]
+
+
+def dot_tn(a, b):
+    return lax.dot_general(a, b, (((0,), (0,)), ((), ())), preferred_element_type=jnp.float32)
+
+
+def product_kernel(place_ref, own_ref, other_ref, *refs):
+    columns = own_ref.shape[0]
+    pieces, (block_ref,) = refs[:columns], refs[-1:]
+    outs = refs[columns:-1]
+    lines, w_cols, model = block_ref.shape
+    width = 4 * LANES
+    own = jnp.concatenate([piece[0] for piece in pieces], axis=0)
+    other = jnp.concatenate([piece[1] for piece in pieces], axis=0)
+    rows = own.shape[0]
+    for base in range(0, model, width):
+        cols = slice(base, base + width)
+        total = dot_tn(own, own_ref[:, :, cols].reshape(rows, width))
+        total = total + dot_tn(other, other_ref[:, :, cols].reshape(rows, width))
+        block_ref[:, :, cols] = total.astype(jnp.bfloat16).reshape(lines, w_cols, width)
+    for step, out_ref in enumerate(outs):
+        out_ref[...] = block_ref[(place_ref[2] + step) % lines]
+
+
+def input_grad_kernel(both_ref, *refs):
+    columns, cores, tokens, _ = both_ref.shape
+    weights, (mine_ref, away_ref) = refs[:columns], refs[columns:]
+    width = 4 * LANES
+    for base in range(0, mine_ref.shape[1], width):
+        cols = slice(base, base + width)
+        total = jnp.zeros((cores * tokens, width), jnp.float32)
+        for step in range(columns):
+            total = total + dot_nn(
+                both_ref[step].reshape(cores * tokens, LANES),
+                weights[(columns - step) % columns][:, cols],
+            )
+        mine_ref[:, cols] = total[:tokens]
+        away_ref[:, cols] = total[tokens:].astype(jnp.bfloat16)
 
 
 def unpack_pair_kernel(x_ref, q_ref, k_ref):
@@ -211,30 +262,12 @@
     return lax.ppermute(x, axis, [(place, (place + step) % count) for place in range(count)])
 
 
-def block_of(x, index):
-    return lax.dynamic_index_in_dim(x, index, 0, keepdims=False)
-
-
 def from_all(x, axis):
     return [x] + [shifted(x, axis, step) for step in range(1, lax.axis_size(axis))]
 
 
-def sent_blocks(blocks, axis):
-    count = lax.axis_size(axis)
-    here = lax.axis_index(axis)
-    own = block_of(blocks, here)
-    return [own] + [
-        shifted(block_of(blocks, (here + step) % count), axis, step) for step in range(1, count)
-    ]
-
-
-def placed(parts, axis):
-    count = lax.axis_size(axis)
-    here = lax.axis_index(axis)
-    whole = jnp.zeros((count, *parts[0].shape), parts[0].dtype)
-    for step, part in enumerate(parts):
-        whole = lax.dynamic_update_index_in_dim(whole, part, (here - step) % count, 0)
-    return whole.reshape(count * parts[0].shape[0], *parts[0].shape[1:])
+def near(x):
+    return pltpu.with_memory_space_constraint(x, pltpu.VMEM)
 
 
 def shaped(*shape, dtype=jnp.bfloat16):
@@ -243,7 +276,7 @@
 
 def shards(inputs, query_vectors, key_vectors, value_vectors, cotangent, gate_prefix, value_weight):
     planes = lax.axis_size("sp")
-    cores, columns, lines = lax.axis_size("core"), lax.axis_size("x"), lax.axis_size("y")
+    columns, lines = lax.axis_size("x"), lax.axis_size("y")
     core = lax.axis_index("core")
     tokens, model = inputs.shape[1:]
     width = query_vectors.shape[2]
@@ -252,20 +285,27 @@
     w_cols = value_weight.shape[1]
     weight_block = jnp.broadcast_to(value_weight.T, (planes, w_cols, model // planes))
     weight_block = exchanged(weight_block, "sp")
-    weight_block = jnp.moveaxis(weight_block, 0, 1).reshape(w_cols, model)
+    place = jnp.stack([core, lax.axis_index("x"), lax.axis_index("y")]).astype(jnp.int32)
+    small, whole = pl.BlockSpec(memory_space=pltpu.SMEM), pl.BlockSpec(memory_space=pltpu.VMEM)
+    weight_block = pl.pallas_call(weight_open_kernel, out_shape=shaped(w_cols, model))(
+        near(weight_block)
+    )
     packed = pl.pallas_call(pack_kernel, out_shape=shaped(heads, tokens, 2 * LANES))(
         query_vectors[0], key_vectors[0], value_vectors[0], cotangent[0]
     )
     arrived = exchanged(packed, "sp")
-    own_rows = jnp.stack(from_all(inputs[0], "x"))
-    input_rows = jnp.stack([own_rows, shifted(own_rows, "core", 1)], axis=1)
-    input_rows = input_rows.reshape(cores * columns * tokens, model)
-    weight_line = placed(from_all(weight_block, "y"), "y")
-    weight_half = placed(from_all(weight_line, "x"), "x")
-    weight_halves = from_all(weight_half, "core")
+    own_rows = pl.pallas_call(stack_kernel, out_shape=shaped(columns, tokens, model))(
+        inputs[0], *map(near, from_all(inputs[0], "x")[1:])
+    )
+    other_rows = shifted(own_rows, "core", 1)
+    weight_line = pl.pallas_call(
+        weight_line_kernel,
+        out_shape=shaped(lines, w_cols, model),
+        in_specs=[small] + [whole] * lines,
+    )(place, weight_block, *map(near, from_all(weight_block, "y")[1:])).reshape(lines * w_cols, model)
+    weight_pieces = from_all(weight_line, "x")
     kept = (tokens // 2 + 7) // 8 * 8
-    arrived, input_rows = lax.optimization_barrier((arrived, input_rows))
-    sequence = arrived.reshape(length, 2 * LANES)
+    sequence = near(arrived.reshape(length, 2 * LANES))
     wide, tile = pltpu.VMEM((length, LANES), jnp.float32), pltpu.VMEM((length, TILE), jnp.float32)
     row = shaped(1, length, dtype=jnp.float32)
     value_grad, peak, share = pl.pallas_call(
@@ -287,37 +327,31 @@
         ],
     )(sequence, gate_prefix[0], peak, share)
     pair_back = exchanged(pair_grad.reshape(planes, tokens, LANES), "sp")
-    place = jnp.stack([core, lax.axis_index("x")]).astype(jnp.int32)
     block = shaped(columns, tokens, LANES)
-    whole = pl.BlockSpec(memory_space=pltpu.VMEM)
-    value_rows, mine, away = pl.pallas_call(
-        unpack_value_kernel,
-        out_shape=(shaped(cores, tokens, width // cores), block, block),
-        in_specs=[pl.BlockSpec(memory_space=pltpu.SMEM), whole],
-    )(place, value_back)
+    mine, away = pl.pallas_call(
+        unpack_value_kernel, out_shape=(block, block), in_specs=[small, whole]
+    )(place, near(value_back))
     both = jnp.stack([mine, shifted(away, "core", 1)], axis=1)
     pieces = [both[0]] + [shifted(both[step], "x", step) for step in range(1, columns)]
-    value_cols = jnp.stack(pieces).reshape(columns * cores * tokens, LANES)
-    partial = lax.dot_general(
-        value_cols, input_rows, (((0,), (0,)), ((), ())), preferred_element_type=jnp.float32
-    ).astype(jnp.bfloat16)
-    partial = sent_blocks(partial.reshape(lines, w_cols, model), "y")
+    partial = pl.pallas_call(
+        product_kernel,
+        out_shape=(shaped(w_cols, model),) * lines,
+        in_specs=[small] + [whole] * (2 + columns),
+        scratch_shapes=[pltpu.VMEM((lines, w_cols, model), jnp.bfloat16)],
+    )(place, own_rows, near(other_rows), *map(near, pieces))
+    partial = [partial[0]] + [shifted(partial[step], "y", step) for step in range(1, lines)]
     partial = sum(part.astype(jnp.float32) for part in partial).astype(jnp.bfloat16)
     partial = jnp.moveaxis(partial.reshape(w_cols, planes, model // planes), 1, 0)
     partial = exchanged(partial, "sp")
     weight_grad = partial.astype(jnp.float32).sum(axis=0).T
     query_grad, key_grad = pl.pallas_call(
         unpack_pair_kernel, out_shape=(shaped(tokens, width), shaped(tokens, width))
-    )(pair_back)
-    input_grad = sum(
-        lax.dot_general(
-            value_rows[place],
-            half,
-            (((1,), (0,)), ((), ())),
-            preferred_element_type=jnp.float32,
-        )
-        for place, half in enumerate(weight_halves)
-    ).astype(jnp.bfloat16)
+    )(near(pair_back))
+    kept_part, sent_part = pl.pallas_call(
+        input_grad_kernel,
+        out_shape=(shaped(tokens, model, dtype=jnp.float32), shaped(tokens, model)),
+    )(both, *weight_pieces)
+    input_grad = (kept_part + shifted(sent_part, "core", 1)).astype(jnp.bfloat16)
     return (query_grad[None], key_grad[None], input_grad[None], weight_grad)
 
 

time: 237 us -> 246 us (1.038)
  the two profiles are of different devices: /device:TPU:58 before, /device:TPU:11 now
where the time goes in v2:
time: 246 us; the launch traced here: 244 us
  starting transfers between devices  116 us (47%)
  waiting for transfers between devices  82.5 us (34%)
  Pallas kernels  35.4 us (14%)
  other arithmetic  6.6 us (3%)
  local copies, waits for them, and re-layouts  2.72 us (1%)
    ppermute x18, starting transfers between devices, shifted(): lax.ppermute(x, axis, [(place, (place + step) % count) for place in range...  60.1 us
    ppermute x18, waiting for transfers between devices, shifted(): lax.ppermute(x, axis, [(place, (place + step) % count) for place in range...  58 us
    all_to_all x5, starting transfers between devices, exchanged(): return lax.all_to_all(x, axis, split_axis=0, concat_axis=0, tiled=True)  55.9 us
    all_to_all x5, waiting for transfers between devices, exchanged(): return lax.all_to_all(x, axis, split_axis=0, concat_axis=0, tiled=True)  24.5 us
    pallas_call x1, Pallas kernels, shards(): pl.pallas_call(pair_kernel, out_shape=shaped(length, LANES), scratch_shap...  9.14 us
    pallas_call x1, Pallas kernels, shards(): pl.pallas_call(value_kernel, out_shape=(shaped(planes, kept, LANES), row,...  7.74 us
  transfers between devices with their start and end apart: 23, of which 16 were waited for; matrix products, arithmetic and copies ran while one was open for 3% of the time, Pallas kernels for 13%

profile of v2, /device:TPU:11, one launch (start us, length us, event | category | flops | bytes accessed | tf_op | source)
XLA Modules:
  0.0 244.2 jit_solution(14379620807510116890)
XLA Ops:
  3.3 15.0 %all-to-all-start = ((bf16[16,136,256]{2,1,0:T(8,128)(2,1)}), bf16[16,136,256]{2,1,0:T(8,128)(2,1)S(1)}, u32[]{:S(2)}, u32[]{:S(2)}) async-start(bf16[16,136,256]{2,1,0:T(8,128)(2,1)} %shard_map.102), calls=%async_computation | async-start | bytes 2228224 | tf_op jit(solution)/shard_map/all_to_all | solution.py:257
  24.3 3.8 %collective-permute-start.10 = (bf16[136,2048]{1,0:T(8,128)(2,1)S(1)}, bf16[136,2048]{1,0:T(8,128)(2,1)S(1)}, u32[]{:S(2)}, u32[]{:S(2)}) collective-permute-start(bf16[136,2048]{1,0:T(8,128)(2,1)S(1)} %bitcast.45), channel_id=1, source_target_pairs={{0,6},{2,0},{4,2},{6,4},{1,7},{3,1},{5,3},{7,5},{8,14},{10,8},{12,... | collective-permute-start | bytes 1671176 | tf_op jit(solution)/shard_map/ppermute | solution.py:262
  28.1 5.5 %collective-permute-done.8.refs_1_ = bf16[136,2048]{1,0:T(8,128)(2,1)S(1)} collective-permute-done((bf16[136,2048]{1,0:T(8,128)(2,1)S(1)}, bf16[136,2048]{1,0:T(8,128)(2,1)S(1)}, u32[]{:S(2)}, u32[]{:S(2)}) %collective-permute-start.8) | collective-permute-done | bytes 557088 | tf_op jit(solution)/shard_map/ppermute | solution.py:262
  33.5 4.4 %collective-permute-done.9.refs_2_ = bf16[136,2048]{1,0:T(8,128)(2,1)S(1)} collective-permute-done((bf16[136,2048]{1,0:T(8,128)(2,1)S(1)}, bf16[136,2048]{1,0:T(8,128)(2,1)S(1)}, u32[]{:S(2)}, u32[]{:S(2)}) %collective-permute-start.9) | collective-permute-done | bytes 557088 | tf_op jit(solution)/shard_map/ppermute | solution.py:262
  37.9 13.5 %collective-permute-done.10.refs_3_ = bf16[136,2048]{1,0:T(8,128)(2,1)S(1)} collective-permute-done((bf16[136,2048]{1,0:T(8,128)(2,1)S(1)}, bf16[136,2048]{1,0:T(8,128)(2,1)S(1)}, u32[]{:S(2)}, u32[]{:S(2)}) %collective-permute-start.10) | collective-permute-done | bytes 557088 | tf_op jit(solution)/shard_map/ppermute | solution.py:262
  56.5 9.2 %all-to-all-done = bf16[16,136,256]{2,1,0:T(8,128)(2,1)S(1)} async-done(((bf16[16,136,256]{2,1,0:T(8,128)(2,1)}), bf16[16,136,256]{2,1,0:T(8,128)(2,1)S(1)}, u32[]{:S(2)}, u32[]{:S(2)}) %all-to-all-start) | async-done | bytes 1114144 | tf_op jit(solution)/shard_map/all_to_all | solution.py:257
  65.8 7.7 %shard_map.103 = (bf16[16,72,128]{2,1,0:T(8,128)(2,1)}, f32[1,2176]{1,0:T(1,128)}, f32[1,2176]{1,0:T(1,128)}) custom-call(bf16[2176,256]{1,0:T(8,128)(2,1)S(1)} %bitcast.35, f32[1,2176]{1,0:T(1,128)} %bitcast.54), custom_call_target="tpu_custom_call" | custom-call | tf_op jit(solution)/shard_map/pallas_call | solution.py:311
  73.5 13.5 %all-to-all-start.2 = ((bf16[16,72,128]{2,1,0:T(8,128)(2,1)}), bf16[16,72,128]{2,1,0:T(8,128)(2,1)S(1)}, u32[]{:S(2)}, u32[]{:S(2)}) async-start(bf16[16,72,128]{2,1,0:T(8,128)(2,1)} %get-tuple-element.21), calls=%async_computation.2 | async-start | bytes 589824 | tf_op jit(solution)/shard_map/all_to_all | solution.py:257
  87.6 13.7 %all-to-all-done.2.x_ref = bf16[16,72,128]{2,1,0:T(8,128)(2,1)S(1)} async-done(((bf16[16,72,128]{2,1,0:T(8,128)(2,1)}), bf16[16,72,128]{2,1,0:T(8,128)(2,1)S(1)}, u32[]{:S(2)}, u32[]{:S(2)}) %all-to-all-start.2) | async-done | bytes 294944 | tf_op jit(solution)/shard_map/all_to_all | solution.py:257
  103.0 8.1 %collective-permute-start = (bf16[4,136,128]{2,1,0:T(8,128)(2,1)}, bf16[4,136,128]{2,1,0:T(8,128)(2,1)S(1)}, u32[]{:S(2)}, u32[]{:S(2)}) collective-permute-start(bf16[4,136,128]{2,1,0:T(8,128)(2,1)} %get-tuple-element.23), channel_id=1, source_target_pairs={{0,1},{1,0},{2,3},{3,2},{4,5},{5,4},{6,7},{7,6},{8,9},{9,8},{10,11... | collective-permute-start | bytes 417800 | tf_op jit(solution)/shard_map/ppermute | solution.py:262
  111.8 5.7 %all-to-all-start.3 = ((bf16[16,32,128]{2,1,0:T(8,128)(2,1)}), bf16[16,32,128]{2,1,0:T(8,128)(2,1)S(1)}, u32[]{:S(2)}, u32[]{:S(2)}) async-start(bf16[16,32,128]{2,1,0:T(8,128)(2,1)} %broadcast_in_dim.14), calls=%async_computation.3 | async-start | bytes 262144 | tf_op jit(solution)/shard_map/all_to_all | solution.py:257
  124.2 3.8 %collective-permute-start.14 = (bf16[2,136,128]{2,1,0:T(8,128)(2,1)S(1)}, bf16[2,136,128]{2,1,0:T(8,128)(2,1)S(1)}, u32[]{:S(2)}, u32[]{:S(2)}) collective-permute-start(bf16[2,136,128]{2,1,0:T(8,128)(2,1)S(1)} %get-tuple-element.30), channel_id=1, source_target_pairs={{0,6},{2,0},{4,2},{6,4},{1,7},{3,1},{5,3},{7,5},{8,14},{10,8},{12,... | collective-permute-start | bytes 208904 | tf_op jit(solution)/shard_map/ppermute | solution.py:262
  130.1 4.1 %shard_map.111 = (bf16[32,2048]{1,0:T(8,128)(2,1)}, bf16[32,2048]{1,0:T(8,128)(2,1)}, bf16[32,2048]{1,0:T(8,128)(2,1)}, bf16[32,2048]{1,0:T(8,128)(2,1)}) custom-call(s32[3]{0:T(128)} %pad_add_fusion.place_ref, bf16[4,136,2048]{2,1,0:T(8,128)(2,1)} %shard_map.110.own_ref, bf16[4,136,2048]{2,1,0:T(8,128)(2,1)} %collective-permute-done.11.other_ref, ...), custom_call_target="tpu_custom_call" | custom-call | tf_op jit(solution)/shard_map/pallas_call | solution.py:336
  136.3 4.2 %collective-permute-start.16 = (bf16[32,2048]{1,0:T(8,128)(2,1)}, bf16[32,2048]{1,0:T(8,128)(2,1)S(1)}, u32[]{:S(2)}, u32[]{:S(2)}) collective-permute-start(bf16[32,2048]{1,0:T(8,128)(2,1)} %get-tuple-element.28), channel_id=1, source_target_pairs={{0,16},{8,24},{16,0},{24,8},{1,17},{9,25},{17,1},{25,9},{2,18},{10... | collective-permute-start | bytes 393224 | tf_op jit(solution)/shard_map/ppermute | solution.py:262
  140.5 3.5 %collective-permute-start.15 = (bf16[32,2048]{1,0:T(8,128)(2,1)}, bf16[32,2048]{1,0:T(8,128)(2,1)S(1)}, u32[]{:S(2)}, u32[]{:S(2)}) collective-permute-start(bf16[32,2048]{1,0:T(8,128)(2,1)} %get-tuple-element.27), channel_id=1, source_target_pairs={{0,8},{8,16},{16,24},{24,0},{1,9},{9,17},{17,25},{25,1},{2,10},{10... | collective-permute-start | bytes 393224 | tf_op jit(solution)/shard_map/ppermute | solution.py:262
  148.8 11.7 %all-to-all-start.4 = ((bf16[16,32,128]{2,1,0:T(8,128)(2,1)}), bf16[16,32,128]{2,1,0:T(8,128)(2,1)S(1)}, u32[]{:S(2)}, u32[]{:S(2)}) async-start(bf16[16,32,128]{2,1,0:T(8,128)(2,1)} %bitcast_bitcast_fusion), calls=%async_computation.4 | async-start | bytes 262144 | tf_op jit(solution)/shard_map/all_to_all | solution.py:257
  161.8 9.1 %shard_map.104 = bf16[2176,128]{1,0:T(8,128)(2,1)} custom-call(bf16[2176,256]{1,0:T(8,128)(2,1)S(1)} %bitcast.36, f32[1,2176]{1,0:T(1,128)} %bitcast.55, f32[1,2176]{1,0:T(1,128)} %get-tuple-element.17.peak_ref, f32[1,2176]{1,0:T(1,128)} %get-tuple-element.18.share_ref), custom_call_target="tpu_custom_call" | custom-call | tf_op jit(solution)/shard_map/pallas_call | solution.py:317
  172.5 10.0 %all-to-all-start.1 = ((bf16[16,136,128]{2,1,0:T(8,128)(2,1)}), bf16[16,136,128]{2,1,0:T(8,128)(2,1)S(1)}, u32[]{:S(2)}, u32[]{:S(2)}) async-start(bf16[16,136,128]{2,1,0:T(8,128)(2,1)} %bitcast.37), calls=%async_computation.1 | async-start | bytes 1114112 | tf_op jit(solution)/shard_map/all_to_all | solution.py:257
  186.4 4.6 %collective-permute-start.2 = (bf16[32,2048]{1,0:T(8,128)(2,1)}, bf16[32,2048]{1,0:T(8,128)(2,1)S(1)}, u32[]{:S(2)}, u32[]{:S(2)}) collective-permute-start(bf16[32,2048]{1,0:T(8,128)(2,1)} %shard_map.107.refs_0_), channel_id=1, source_target_pairs={{0,16},{8,24},{16,0},{24,8},{1,17},{9,25},{17,1},{25,9},{2,18},{10... | collective-permute-start | bytes 393224 | tf_op jit(solution)/shard_map/ppermute | solution.py:262
  194.2 4.5 %collective-permute-done.3.refs_3_ = bf16[32,2048]{1,0:T(8,128)(2,1)S(1)} collective-permute-done((bf16[32,2048]{1,0:T(8,128)(2,1)}, bf16[32,2048]{1,0:T(8,128)(2,1)S(1)}, u32[]{:S(2)}, u32[]{:S(2)}) %collective-permute-start.3) | collective-permute-done | bytes 131104 | tf_op jit(solution)/shard_map/ppermute | solution.py:262
  205.0 3.6 %collective-permute-start.6 = (bf16[128,2048]{1,0:T(8,128)(2,1)}, bf16[128,2048]{1,0:T(8,128)(2,1)S(1)}, u32[]{:S(2)}, u32[]{:S(2)}) collective-permute-start(bf16[128,2048]{1,0:T(8,128)(2,1)} %bitcast.40), channel_id=1, source_target_pairs={{0,6},{2,0},{4,2},{6,4},{1,7},{3,1},{5,3},{7,5},{8,14},{10,8},{12,... | collective-permute-start | bytes 1572872 | tf_op jit(solution)/shard_map/ppermute | solution.py:262
  209.4 3.6 %collective-permute-done.4.refs_1_ = bf16[128,2048]{1,0:T(8,128)(2,1)S(1)} collective-permute-done((bf16[128,2048]{1,0:T(8,128)(2,1)}, bf16[128,2048]{1,0:T(8,128)(2,1)S(1)}, u32[]{:S(2)}, u32[]{:S(2)}) %collective-permute-start.4) | collective-permute-done | bytes 524320 | tf_op jit(solution)/shard_map/ppermute | solution.py:262
  216.4 14.9 %collective-permute-done.6.refs_3_ = bf16[128,2048]{1,0:T(8,128)(2,1)S(1)} collective-permute-done((bf16[128,2048]{1,0:T(8,128)(2,1)}, bf16[128,2048]{1,0:T(8,128)(2,1)S(1)}, u32[]{:S(2)}, u32[]{:S(2)}) %collective-permute-start.6) | collective-permute-done | bytes 524320 | tf_op jit(solution)/shard_map/ppermute | solution.py:262
  232.2 4.0 %shard_map.109 = (f32[136,2048]{1,0:T(8,128)}, bf16[136,2048]{1,0:T(8,128)(2,1)}) custom-call(bf16[4,2,136,128]{3,2,1,0:T(8,128)(2,1)} %pad_maximum_fusion.both_ref, bf16[128,2048]{1,0:T(8,128)(2,1)} %bitcast.41, bf16[128,2048]{1,0:T(8,128)(2,1)} %copy-done.4, bf16[128,2048]{1,0:T(8,128)(2,1)} %copy-done.5, bf16[128,2048]{1,0:T(8,128)(2,1)} %copy-done.6), custom_call_target="tpu_custom_call" | custom-call | tf_op jit(solution)/shard_map/pallas_call | solution.py:350
  (55 shorter events, 61.4 us)
Async XLA Ops:
  3.3 62.4 %all-to-all-start = ((bf16[16,136,256]{2,1,0:T(8,128)(2,1)}), bf16[16,136,256]{2,1,0:T(8,128)(2,1)S(1)}, u32[]{:S(2)}, u32[]{:S(2)}) async-start(bf16[16,136,256]{2,1,0:T(8,128)(2,1)} %shard_map.102), calls=%async_computation | async-start | bytes 2228224 | tf_op jit(solution)/shard_map/all_to_all | solution.py:257
  18.4 15.1 %collective-permute-start.8 = (bf16[136,2048]{1,0:T(8,128)(2,1)S(1)}, bf16[136,2048]{1,0:T(8,128)(2,1)S(1)}, u32[]{:S(2)}, u32[]{:S(2)}) collective-permute-start(bf16[136,2048]{1,0:T(8,128)(2,1)S(1)} %bitcast.43), channel_id=1, source_target_pairs={{0,2},{2,4},{4,6},{6,0},{1,3},{3,5},{5,7},{7,1},{8,10},{10,12},{12... | collective-permute-start | bytes 1671176 | tf_op jit(solution)/shard_map/ppermute | solution.py:262
  21.5 16.4 %collective-permute-start.9 = (bf16[136,2048]{1,0:T(8,128)(2,1)S(1)}, bf16[136,2048]{1,0:T(8,128)(2,1)S(1)}, u32[]{:S(2)}, u32[]{:S(2)}) collective-permute-start(bf16[136,2048]{1,0:T(8,128)(2,1)S(1)} %bitcast.44), channel_id=1, source_target_pairs={{0,4},{2,6},{4,0},{6,2},{1,5},{3,7},{5,1},{7,3},{8,12},{10,14},{12... | collective-permute-start | bytes 1671176 | tf_op jit(solution)/shard_map/ppermute | solution.py:262
  24.3 27.1 %collective-permute-start.10 = (bf16[136,2048]{1,0:T(8,128)(2,1)S(1)}, bf16[136,2048]{1,0:T(8,128)(2,1)S(1)}, u32[]{:S(2)}, u32[]{:S(2)}) collective-permute-start(bf16[136,2048]{1,0:T(8,128)(2,1)S(1)} %bitcast.45), channel_id=1, source_target_pairs={{0,6},{2,0},{4,2},{6,4},{1,7},{3,1},{5,3},{7,5},{8,14},{10,8},{12,... | collective-permute-start | bytes 1671176 | tf_op jit(solution)/shard_map/ppermute | solution.py:262
  54.0 57.1 %copy-start.7 = (bf16[128,32]{0,1:T(8,128)(2,1)S(1)}, bf16[128,32]{0,1:T(8,128)(2,1)}, u32[]{:S(2)}) copy-start(bf16[128,32]{0,1:T(8,128)(2,1)} %param.13) | copy-start | bytes 24580
  54.0 74.0 %collective-permute-start.11 = (bf16[4,136,2048]{2,1,0:T(8,128)(2,1)}, bf16[4,136,2048]{2,1,0:T(8,128)(2,1)}, u32[]{:S(2)}, u32[]{:S(2)}) collective-permute-start(bf16[4,136,2048]{2,1,0:T(8,128)(2,1)} %shard_map.110.own_ref), channel_id=1, source_target_pairs={{0,1},{1,0},{2,3},{3,2},{4,5},{5,4},{6,7},{7,6},{8,9},{9,8},{10,11... | collective-permute-start | bytes 6684680 | tf_op jit(solution)/shard_map/ppermute | solution.py:262
  73.5 27.8 %all-to-all-start.2 = ((bf16[16,72,128]{2,1,0:T(8,128)(2,1)}), bf16[16,72,128]{2,1,0:T(8,128)(2,1)S(1)}, u32[]{:S(2)}, u32[]{:S(2)}) async-start(bf16[16,72,128]{2,1,0:T(8,128)(2,1)} %get-tuple-element.21), calls=%async_computation.2 | async-start | bytes 589824 | tf_op jit(solution)/shard_map/all_to_all | solution.py:257
  103.0 14.5 %collective-permute-start = (bf16[4,136,128]{2,1,0:T(8,128)(2,1)}, bf16[4,136,128]{2,1,0:T(8,128)(2,1)S(1)}, u32[]{:S(2)}, u32[]{:S(2)}) collective-permute-start(bf16[4,136,128]{2,1,0:T(8,128)(2,1)} %get-tuple-element.23), channel_id=1, source_target_pairs={{0,1},{1,0},{2,3},{3,2},{4,5},{5,4},{6,7},{7,6},{8,9},{9,8},{10,11... | collective-permute-start | bytes 417800 | tf_op jit(solution)/shard_map/ppermute | solution.py:262
  111.8 37.0 %all-to-all-start.3 = ((bf16[16,32,128]{2,1,0:T(8,128)(2,1)}), bf16[16,32,128]{2,1,0:T(8,128)(2,1)S(1)}, u32[]{:S(2)}, u32[]{:S(2)}) async-start(bf16[16,32,128]{2,1,0:T(8,128)(2,1)} %broadcast_in_dim.14), calls=%async_computation.3 | async-start | bytes 262144 | tf_op jit(solution)/shard_map/all_to_all | solution.py:257
  118.3 9.7 %collective-permute-start.12 = (bf16[2,136,128]{2,1,0:T(8,128)(2,1)S(1)}, bf16[2,136,128]{2,1,0:T(8,128)(2,1)S(1)}, u32[]{:S(2)}, u32[]{:S(2)}) collective-permute-start(bf16[2,136,128]{2,1,0:T(8,128)(2,1)S(1)} %get-tuple-element.32), channel_id=1, source_target_pairs={{0,2},{2,4},{4,6},{6,0},{1,3},{3,5},{5,7},{7,1},{8,10},{10,12},{12... | collective-permute-start | bytes 208904 | tf_op jit(solution)/shard_map/ppermute | solution.py:262
  121.5 6.9 %collective-permute-start.13 = (bf16[2,136,128]{2,1,0:T(8,128)(2,1)S(1)}, bf16[2,136,128]{2,1,0:T(8,128)(2,1)S(1)}, u32[]{:S(2)}, u32[]{:S(2)}) collective-permute-start(bf16[2,136,128]{2,1,0:T(8,128)(2,1)S(1)} %get-tuple-element.33), channel_id=1, source_target_pairs={{0,4},{2,6},{4,0},{6,2},{1,5},{3,7},{5,1},{7,3},{8,12},{10,14},{12... | collective-permute-start | bytes 208904 | tf_op jit(solution)/shard_map/ppermute | solution.py:262
  124.2 5.9 %collective-permute-start.14 = (bf16[2,136,128]{2,1,0:T(8,128)(2,1)S(1)}, bf16[2,136,128]{2,1,0:T(8,128)(2,1)S(1)}, u32[]{:S(2)}, u32[]{:S(2)}) collective-permute-start(bf16[2,136,128]{2,1,0:T(8,128)(2,1)S(1)} %get-tuple-element.30), channel_id=1, source_target_pairs={{0,6},{2,0},{4,2},{6,4},{1,7},{3,1},{5,3},{7,5},{8,14},{10,8},{12,... | collective-permute-start | bytes 208904 | tf_op jit(solution)/shard_map/ppermute | solution.py:262
  134.2 9.8 %collective-permute-start.17 = (bf16[32,2048]{1,0:T(8,128)(2,1)}, bf16[32,2048]{1,0:T(8,128)(2,1)S(1)}, u32[]{:S(2)}, u32[]{:S(2)}) collective-permute-start(bf16[32,2048]{1,0:T(8,128)(2,1)} %get-tuple-element.29), channel_id=1, source_target_pairs={{0,24},{8,0},{16,8},{24,16},{1,25},{9,1},{17,9},{25,17},{2,26},{10... | collective-permute-start | bytes 393224 | tf_op jit(solution)/shard_map/ppermute | solution.py:262
  136.3 7.9 %collective-permute-start.16 = (bf16[32,2048]{1,0:T(8,128)(2,1)}, bf16[32,2048]{1,0:T(8,128)(2,1)S(1)}, u32[]{:S(2)}, u32[]{:S(2)}) collective-permute-start(bf16[32,2048]{1,0:T(8,128)(2,1)} %get-tuple-element.28), channel_id=1, source_target_pairs={{0,16},{8,24},{16,0},{24,8},{1,17},{9,25},{17,1},{25,9},{2,18},{10... | collective-permute-start | bytes 393224 | tf_op jit(solution)/shard_map/ppermute | solution.py:262
  140.5 6.6 %collective-permute-start.15 = (bf16[32,2048]{1,0:T(8,128)(2,1)}, bf16[32,2048]{1,0:T(8,128)(2,1)S(1)}, u32[]{:S(2)}, u32[]{:S(2)}) collective-permute-start(bf16[32,2048]{1,0:T(8,128)(2,1)} %get-tuple-element.27), channel_id=1, source_target_pairs={{0,8},{8,16},{16,24},{24,0},{1,9},{9,17},{17,25},{25,1},{2,10},{10... | collective-permute-start | bytes 393224 | tf_op jit(solution)/shard_map/ppermute | solution.py:262
  148.8 23.7 %all-to-all-start.4 = ((bf16[16,32,128]{2,1,0:T(8,128)(2,1)}), bf16[16,32,128]{2,1,0:T(8,128)(2,1)S(1)}, u32[]{:S(2)}, u32[]{:S(2)}) async-start(bf16[16,32,128]{2,1,0:T(8,128)(2,1)} %bitcast_bitcast_fusion), calls=%async_computation.4 | async-start | bytes 262144 | tf_op jit(solution)/shard_map/all_to_all | solution.py:257
  172.5 70.7 %all-to-all-start.1 = ((bf16[16,136,128]{2,1,0:T(8,128)(2,1)}), bf16[16,136,128]{2,1,0:T(8,128)(2,1)S(1)}, u32[]{:S(2)}, u32[]{:S(2)}) async-start(bf16[16,136,128]{2,1,0:T(8,128)(2,1)} %bitcast.37), calls=%async_computation.1 | async-start | bytes 1114112 | tf_op jit(solution)/shard_map/all_to_all | solution.py:257
  183.2 9.8 %collective-permute-start.1 = (bf16[32,2048]{1,0:T(8,128)(2,1)}, bf16[32,2048]{1,0:T(8,128)(2,1)S(1)}, u32[]{:S(2)}, u32[]{:S(2)}) collective-permute-start(bf16[32,2048]{1,0:T(8,128)(2,1)} %shard_map.107.refs_0_), channel_id=1, source_target_pairs={{0,8},{8,16},{16,24},{24,0},{1,9},{9,17},{17,25},{25,1},{2,10},{10... | collective-permute-start | bytes 393224 | tf_op jit(solution)/shard_map/ppermute | solution.py:262
  186.4 7.7 %collective-permute-start.2 = (bf16[32,2048]{1,0:T(8,128)(2,1)}, bf16[32,2048]{1,0:T(8,128)(2,1)S(1)}, u32[]{:S(2)}, u32[]{:S(2)}) collective-permute-start(bf16[32,2048]{1,0:T(8,128)(2,1)} %shard_map.107.refs_0_), channel_id=1, source_target_pairs={{0,16},{8,24},{16,0},{24,8},{1,17},{9,25},{17,1},{25,9},{2,18},{10... | collective-permute-start | bytes 393224 | tf_op jit(solution)/shard_map/ppermute | solution.py:262
  191.0 7.6 %collective-permute-start.3 = (bf16[32,2048]{1,0:T(8,128)(2,1)}, bf16[32,2048]{1,0:T(8,128)(2,1)S(1)}, u32[]{:S(2)}, u32[]{:S(2)}) collective-permute-start(bf16[32,2048]{1,0:T(8,128)(2,1)} %shard_map.107.refs_0_), channel_id=1, source_target_pairs={{0,24},{8,0},{16,8},{24,16},{1,25},{9,1},{17,9},{25,17},{2,26},{10... | collective-permute-start | bytes 393224 | tf_op jit(solution)/shard_map/ppermute | solution.py:262
  200.4 12.6 %collective-permute-start.4 = (bf16[128,2048]{1,0:T(8,128)(2,1)}, bf16[128,2048]{1,0:T(8,128)(2,1)S(1)}, u32[]{:S(2)}, u32[]{:S(2)}) collective-permute-start(bf16[128,2048]{1,0:T(8,128)(2,1)} %bitcast.38), channel_id=1, source_target_pairs={{0,2},{2,4},{4,6},{6,0},{1,3},{3,5},{5,7},{7,1},{8,10},{10,12},{12... | collective-permute-start | bytes 1572872 | tf_op jit(solution)/shard_map/ppermute | solution.py:262
  202.7 13.7 %collective-permute-start.5 = (bf16[128,2048]{1,0:T(8,128)(2,1)}, bf16[128,2048]{1,0:T(8,128)(2,1)S(1)}, u32[]{:S(2)}, u32[]{:S(2)}) collective-permute-start(bf16[128,2048]{1,0:T(8,128)(2,1)} %bitcast.39), channel_id=1, source_target_pairs={{0,4},{2,6},{4,0},{6,2},{1,5},{3,7},{5,1},{7,3},{8,12},{10,14},{12... | collective-permute-start | bytes 1572872 | tf_op jit(solution)/shard_map/ppermute | solution.py:262
  205.0 26.4 %collective-permute-start.6 = (bf16[128,2048]{1,0:T(8,128)(2,1)}, bf16[128,2048]{1,0:T(8,128)(2,1)S(1)}, u32[]{:S(2)}, u32[]{:S(2)}) collective-permute-start(bf16[128,2048]{1,0:T(8,128)(2,1)} %bitcast.40), channel_id=1, source_target_pairs={{0,6},{2,0},{4,2},{6,4},{1,7},{3,1},{5,3},{7,5},{8,14},{10,8},{12,... | collective-permute-start | bytes 1572872 | tf_op jit(solution)/shard_map/ppermute | solution.py:262
  236.2 4.2 %collective-permute-start.7 = (bf16[136,2048]{1,0:T(8,128)(2,1)}, bf16[136,2048]{1,0:T(8,128)(2,1)S(1)}, u32[]{:S(2)}, u32[]{:S(2)}) collective-permute-start(bf16[136,2048]{1,0:T(8,128)(2,1)} %get-tuple-element.25), channel_id=1, source_target_pairs={{0,1},{1,0},{2,3},{3,2},{4,5},{5,4},{6,7},{7,6},{8,9},{9,8},{10,11... | collective-permute-start | bytes 1671176 | tf_op jit(solution)/shard_map/ppermute | solution.py:262
  (7 other events, 132.6 us)

commit v3 on v2

--- a/solution.py
+++ b/solution.py
@@ -196,7 +196,7 @@
     pieces, out_ref = refs[:-1], refs[-1]
     lines = out_ref.shape[0]
     for step, piece_ref in enumerate(pieces):
-        out_ref[(place_ref[2] + lines - step) % lines] = piece_ref[...]
+        out_ref[(place_ref[1] + lines - step) % lines] = piece_ref[...]
 
 
 def stack_kernel(*refs):
@@ -226,17 +226,24 @@
         out_ref[...] = block_ref[(place_ref[2] + step) % lines]
 
 
-def input_grad_kernel(both_ref, *refs):
+def input_grad_kernel(place_ref, both_ref, *refs):
     columns, cores, tokens, _ = both_ref.shape
-    weights, (mine_ref, away_ref) = refs[:columns], refs[columns:]
+    weight_ref = refs[-1]
+    mine_ref, away_ref = refs[-3:-1]
+    lines, w_cols = weight_ref.shape[1:3]
+    for step, piece_ref in enumerate(refs[:-3]):
+        for column in range(columns):
+            weight_ref[column, (place_ref[2] + lines - step) % lines] = piece_ref[
+                column * w_cols : (column + 1) * w_cols
+            ]
     width = 4 * LANES
     for base in range(0, mine_ref.shape[1], width):
         cols = slice(base, base + width)
         total = jnp.zeros((cores * tokens, width), jnp.float32)
         for step in range(columns):
+            weight = weight_ref[(place_ref[1] + step) % columns, :, :, cols]
             total = total + dot_nn(
-                both_ref[step].reshape(cores * tokens, LANES),
-                weights[(columns - step) % columns][:, cols],
+                both_ref[step].reshape(cores * tokens, LANES), weight.reshape(LANES, width)
             )
         mine_ref[:, cols] = total[:tokens]
         away_ref[:, cols] = total[tokens:].astype(jnp.bfloat16)
@@ -300,10 +307,11 @@
     other_rows = shifted(own_rows, "core", 1)
     weight_line = pl.pallas_call(
         weight_line_kernel,
-        out_shape=shaped(lines, w_cols, model),
-        in_specs=[small] + [whole] * lines,
-    )(place, weight_block, *map(near, from_all(weight_block, "y")[1:])).reshape(lines * w_cols, model)
-    weight_pieces = from_all(weight_line, "x")
+        out_shape=shaped(columns, w_cols, model),
+        in_specs=[small] + [whole] * columns,
+    )(place, weight_block, *map(near, from_all(weight_block, "x")[1:]))
+    weight_line = weight_line.reshape(columns * w_cols, model)
+    weight_pieces = from_all(weight_line, "y")
     kept = (tokens // 2 + 7) // 8 * 8
     sequence = near(arrived.reshape(length, 2 * LANES))
     wide, tile = pltpu.VMEM((length, LANES), jnp.float32), pltpu.VMEM((length, TILE), jnp.float32)
@@ -350,7 +358,9 @@
     kept_part, sent_part = pl.pallas_call(
         input_grad_kernel,
         out_shape=(shaped(tokens, model, dtype=jnp.float32), shaped(tokens, model)),
-    )(both, *weight_pieces)
+        in_specs=[small] + [whole] * (1 + lines),
+        scratch_shapes=[pltpu.VMEM((columns, lines, w_cols, model), jnp.bfloat16)],
+    )(place, both, *weight_pieces)
     input_grad = (kept_part + shifted(sent_part, "core", 1)).astype(jnp.bfloat16)
     return (query_grad[None], key_grad[None], input_grad[None], weight_grad)
 

time: 246 us -> 247 us (level)
  the two profiles are of different devices: /device:TPU:11 before, /device:TPU:9 now
where the time goes in v3:
time: 247 us; the launch traced here: 246 us
  starting transfers between devices  119 us (48%)
  waiting for transfers between devices  80.5 us (33%)
  Pallas kernels  35.6 us (14%)
  other arithmetic  6.6 us (3%)
  local copies, waits for them, and re-layouts  2.72 us (1%)
    ppermute x18, starting transfers between devices, shifted(): lax.ppermute(x, axis, [(place, (place + step) % count) for place in range...  64 us
    all_to_all x5, starting transfers between devices, exchanged(): return lax.all_to_all(x, axis, split_axis=0, concat_axis=0, tiled=True)  55.4 us
    ppermute x18, waiting for transfers between devices, shifted(): lax.ppermute(x, axis, [(place, (place + step) % count) for place in range...  55.1 us
    all_to_all x5, waiting for transfers between devices, exchanged(): return lax.all_to_all(x, axis, split_axis=0, concat_axis=0, tiled=True)  25.4 us
    pallas_call x1, Pallas kernels, shards(): pl.pallas_call(pair_kernel, out_shape=shaped(length, LANES), scratch_shap...  9.12 us
    pallas_call x1, Pallas kernels, shards(): pl.pallas_call(value_kernel, out_shape=(shaped(planes, kept, LANES), row,...  7.74 us
  transfers between devices with their start and end apart: 23, of which 15 were waited for; matrix products, arithmetic and copies ran while one was open for 3% of the time, Pallas kernels for 13%

profile of v3, /device:TPU:9, one launch (start us, length us, event | category | flops | bytes accessed | tf_op | source)
XLA Modules:
  0.0 245.7 jit_solution(5661578179940077790)
XLA Ops:
  3.3 15.0 %all-to-all-start = ((bf16[16,136,256]{2,1,0:T(8,128)(2,1)}), bf16[16,136,256]{2,1,0:T(8,128)(2,1)S(1)}, u32[]{:S(2)}, u32[]{:S(2)}) async-start(bf16[16,136,256]{2,1,0:T(8,128)(2,1)} %shard_map.102), calls=%async_computation | async-start | bytes 2228224 | tf_op jit(solution)/shard_map/all_to_all | solution.py:264
  21.5 4.4 %collective-permute-start.9 = (bf16[136,2048]{1,0:T(8,128)(2,1)S(1)}, bf16[136,2048]{1,0:T(8,128)(2,1)S(1)}, u32[]{:S(2)}, u32[]{:S(2)}) collective-permute-start(bf16[136,2048]{1,0:T(8,128)(2,1)S(1)} %bitcast.44), channel_id=1, source_target_pairs={{0,4},{2,6},{4,0},{6,2},{1,5},{3,7},{5,1},{7,3},{8,12},{10,14},{12... | collective-permute-start | bytes 1671176 | tf_op jit(solution)/shard_map/ppermute | solution.py:269
  29.0 5.8 %collective-permute-done.8.refs_1_ = bf16[136,2048]{1,0:T(8,128)(2,1)S(1)} collective-permute-done((bf16[136,2048]{1,0:T(8,128)(2,1)S(1)}, bf16[136,2048]{1,0:T(8,128)(2,1)S(1)}, u32[]{:S(2)}, u32[]{:S(2)}) %collective-permute-start.8) | collective-permute-done | bytes 557088 | tf_op jit(solution)/shard_map/ppermute | solution.py:269
  34.7 12.9 %collective-permute-done.9.refs_2_ = bf16[136,2048]{1,0:T(8,128)(2,1)S(1)} collective-permute-done((bf16[136,2048]{1,0:T(8,128)(2,1)S(1)}, bf16[136,2048]{1,0:T(8,128)(2,1)S(1)}, u32[]{:S(2)}, u32[]{:S(2)}) %collective-permute-start.9) | collective-permute-done | bytes 557088 | tf_op jit(solution)/shard_map/ppermute | solution.py:269
  52.1 3.6 %collective-permute-start.11 = (bf16[4,136,2048]{2,1,0:T(8,128)(2,1)}, bf16[4,136,2048]{2,1,0:T(8,128)(2,1)}, u32[]{:S(2)}, u32[]{:S(2)}) collective-permute-start(bf16[4,136,2048]{2,1,0:T(8,128)(2,1)} %shard_map.110.own_ref), channel_id=1, source_target_pairs={{0,1},{1,0},{2,3},{3,2},{4,5},{5,4},{6,7},{7,6},{8,9},{9,8},{10,11... | collective-permute-start | bytes 6684680 | tf_op jit(solution)/shard_map/ppermute | solution.py:269
  55.6 10.1 %all-to-all-done = bf16[16,136,256]{2,1,0:T(8,128)(2,1)S(1)} async-done(((bf16[16,136,256]{2,1,0:T(8,128)(2,1)}), bf16[16,136,256]{2,1,0:T(8,128)(2,1)S(1)}, u32[]{:S(2)}, u32[]{:S(2)}) %all-to-all-start) | async-done | bytes 1114144 | tf_op jit(solution)/shard_map/all_to_all | solution.py:264
  65.8 7.7 %shard_map.103 = (bf16[16,72,128]{2,1,0:T(8,128)(2,1)}, f32[1,2176]{1,0:T(1,128)}, f32[1,2176]{1,0:T(1,128)}) custom-call(bf16[2176,256]{1,0:T(8,128)(2,1)S(1)} %bitcast.35, f32[1,2176]{1,0:T(1,128)} %bitcast.54), custom_call_target="tpu_custom_call" | custom-call | tf_op jit(solution)/shard_map/pallas_call | solution.py:319
  73.5 13.5 %all-to-all-start.2 = ((bf16[16,72,128]{2,1,0:T(8,128)(2,1)}), bf16[16,72,128]{2,1,0:T(8,128)(2,1)S(1)}, u32[]{:S(2)}, u32[]{:S(2)}) async-start(bf16[16,72,128]{2,1,0:T(8,128)(2,1)} %get-tuple-element.21), calls=%async_computation.2 | async-start | bytes 589824 | tf_op jit(solution)/shard_map/all_to_all | solution.py:264
  87.6 13.7 %all-to-all-done.2.x_ref = bf16[16,72,128]{2,1,0:T(8,128)(2,1)S(1)} async-done(((bf16[16,72,128]{2,1,0:T(8,128)(2,1)}), bf16[16,72,128]{2,1,0:T(8,128)(2,1)S(1)}, u32[]{:S(2)}, u32[]{:S(2)}) %all-to-all-start.2) | async-done | bytes 294944 | tf_op jit(solution)/shard_map/all_to_all | solution.py:264
  103.0 8.1 %collective-permute-start = (bf16[4,136,128]{2,1,0:T(8,128)(2,1)}, bf16[4,136,128]{2,1,0:T(8,128)(2,1)S(1)}, u32[]{:S(2)}, u32[]{:S(2)}) collective-permute-start(bf16[4,136,128]{2,1,0:T(8,128)(2,1)} %get-tuple-element.23), channel_id=1, source_target_pairs={{0,1},{1,0},{2,3},{3,2},{4,5},{5,4},{6,7},{7,6},{8,9},{9,8},{10,11... | collective-permute-start | bytes 417800 | tf_op jit(solution)/shard_map/ppermute | solution.py:269
  111.8 5.7 %all-to-all-start.3 = ((bf16[16,32,128]{2,1,0:T(8,128)(2,1)}), bf16[16,32,128]{2,1,0:T(8,128)(2,1)S(1)}, u32[]{:S(2)}, u32[]{:S(2)}) async-start(bf16[16,32,128]{2,1,0:T(8,128)(2,1)} %broadcast_in_dim.14), calls=%async_computation.3 | async-start | bytes 262144 | tf_op jit(solution)/shard_map/all_to_all | solution.py:264
  121.5 4.4 %collective-permute-start.13 = (bf16[2,136,128]{2,1,0:T(8,128)(2,1)S(1)}, bf16[2,136,128]{2,1,0:T(8,128)(2,1)S(1)}, u32[]{:S(2)}, u32[]{:S(2)}) collective-permute-start(bf16[2,136,128]{2,1,0:T(8,128)(2,1)S(1)} %get-tuple-element.33), channel_id=1, source_target_pairs={{0,4},{2,6},{4,0},{6,2},{1,5},{3,7},{5,1},{7,3},{8,12},{10,14},{12... | collective-permute-start | bytes 208904 | tf_op jit(solution)/shard_map/ppermute | solution.py:269
  131.2 4.1 %shard_map.111 = (bf16[32,2048]{1,0:T(8,128)(2,1)}, bf16[32,2048]{1,0:T(8,128)(2,1)}, bf16[32,2048]{1,0:T(8,128)(2,1)}, bf16[32,2048]{1,0:T(8,128)(2,1)}) custom-call(s32[3]{0:T(128)} %pad_add_fusion.place_ref, bf16[4,136,2048]{2,1,0:T(8,128)(2,1)} %shard_map.110.own_ref, bf16[4,136,2048]{2,1,0:T(8,128)(2,1)} %collective-permute-done.11.other_ref, ...), custom_call_target="tpu_custom_call" | custom-call | tf_op jit(solution)/shard_map/pallas_call | solution.py:344
  137.4 4.2 %collective-permute-start.16 = (bf16[32,2048]{1,0:T(8,128)(2,1)}, bf16[32,2048]{1,0:T(8,128)(2,1)S(1)}, u32[]{:S(2)}, u32[]{:S(2)}) collective-permute-start(bf16[32,2048]{1,0:T(8,128)(2,1)} %get-tuple-element.28), channel_id=1, source_target_pairs={{0,16},{8,24},{16,0},{24,8},{1,17},{9,25},{17,1},{25,9},{2,18},{10... | collective-permute-start | bytes 393224 | tf_op jit(solution)/shard_map/ppermute | solution.py:269
  141.6 3.5 %collective-permute-start.15 = (bf16[32,2048]{1,0:T(8,128)(2,1)}, bf16[32,2048]{1,0:T(8,128)(2,1)S(1)}, u32[]{:S(2)}, u32[]{:S(2)}) collective-permute-start(bf16[32,2048]{1,0:T(8,128)(2,1)} %get-tuple-element.27), channel_id=1, source_target_pairs={{0,8},{8,16},{16,24},{24,0},{1,9},{9,17},{17,25},{25,1},{2,10},{10... | collective-permute-start | bytes 393224 | tf_op jit(solution)/shard_map/ppermute | solution.py:269
  150.4 11.2 %all-to-all-start.4 = ((bf16[16,32,128]{2,1,0:T(8,128)(2,1)}), bf16[16,32,128]{2,1,0:T(8,128)(2,1)S(1)}, u32[]{:S(2)}, u32[]{:S(2)}) async-start(bf16[16,32,128]{2,1,0:T(8,128)(2,1)} %bitcast_bitcast_fusion), calls=%async_computation.4 | async-start | bytes 262144 | tf_op jit(solution)/shard_map/all_to_all | solution.py:264
  162.8 9.1 %shard_map.104 = bf16[2176,128]{1,0:T(8,128)(2,1)} custom-call(bf16[2176,256]{1,0:T(8,128)(2,1)S(1)} %bitcast.36, f32[1,2176]{1,0:T(1,128)} %bitcast.55, f32[1,2176]{1,0:T(1,128)} %get-tuple-element.17.peak_ref, f32[1,2176]{1,0:T(1,128)} %get-tuple-element.18.share_ref), custom_call_target="tpu_custom_call" | custom-call | tf_op jit(solution)/shard_map/pallas_call | solution.py:325
  173.5 10.0 %all-to-all-start.1 = ((bf16[16,136,128]{2,1,0:T(8,128)(2,1)}), bf16[16,136,128]{2,1,0:T(8,128)(2,1)S(1)}, u32[]{:S(2)}, u32[]{:S(2)}) async-start(bf16[16,136,128]{2,1,0:T(8,128)(2,1)} %bitcast.37), calls=%async_computation.1 | async-start | bytes 1114112 | tf_op jit(solution)/shard_map/all_to_all | solution.py:264
  186.3 5.3 %collective-permute-start.2 = (bf16[32,2048]{1,0:T(8,128)(2,1)}, bf16[32,2048]{1,0:T(8,128)(2,1)S(1)}, u32[]{:S(2)}, u32[]{:S(2)}) collective-permute-start(bf16[32,2048]{1,0:T(8,128)(2,1)} %shard_map.107.refs_0_), channel_id=1, source_target_pairs={{0,4},{2,6},{4,0},{6,2},{1,5},{3,7},{5,1},{7,3},{8,12},{10,14},{12... | collective-permute-start | bytes 393224 | tf_op jit(solution)/shard_map/ppermute | solution.py:269
  194.2 4.4 %collective-permute-done.3.refs_3_ = bf16[32,2048]{1,0:T(8,128)(2,1)S(1)} collective-permute-done((bf16[32,2048]{1,0:T(8,128)(2,1)}, bf16[32,2048]{1,0:T(8,128)(2,1)S(1)}, u32[]{:S(2)}, u32[]{:S(2)}) %collective-permute-start.3) | collective-permute-done | bytes 131104 | tf_op jit(solution)/shard_map/ppermute | solution.py:269
  200.3 3.7 %collective-permute-start.4 = (bf16[128,2048]{1,0:T(8,128)(2,1)}, bf16[128,2048]{1,0:T(8,128)(2,1)S(1)}, u32[]{:S(2)}, u32[]{:S(2)}) collective-permute-start(bf16[128,2048]{1,0:T(8,128)(2,1)} %bitcast.38), channel_id=1, source_target_pairs={{0,8},{8,16},{16,24},{24,0},{1,9},{9,17},{17,25},{25,1},{2,10},{10... | collective-permute-start | bytes 1572872 | tf_op jit(solution)/shard_map/ppermute | solution.py:269
  212.4 4.6 %collective-permute-done.5.refs_2_ = bf16[128,2048]{1,0:T(8,128)(2,1)S(1)} collective-permute-done((bf16[128,2048]{1,0:T(8,128)(2,1)}, bf16[128,2048]{1,0:T(8,128)(2,1)S(1)}, u32[]{:S(2)}, u32[]{:S(2)}) %collective-permute-start.5) | collective-permute-done | bytes 524320 | tf_op jit(solution)/shard_map/ppermute | solution.py:269
  217.0 15.3 %collective-permute-done.6.refs_3_ = bf16[128,2048]{1,0:T(8,128)(2,1)S(1)} collective-permute-done((bf16[128,2048]{1,0:T(8,128)(2,1)}, bf16[128,2048]{1,0:T(8,128)(2,1)S(1)}, u32[]{:S(2)}, u32[]{:S(2)}) %collective-permute-start.6) | collective-permute-done | bytes 524320 | tf_op jit(solution)/shard_map/ppermute | solution.py:269
  233.1 4.2 %shard_map.109 = (f32[136,2048]{1,0:T(8,128)}, bf16[136,2048]{1,0:T(8,128)(2,1)}) custom-call(s32[3]{0:T(128)} %pad_add_fusion.place_ref, bf16[4,2,136,128]{3,2,1,0:T(8,128)(2,1)} %pad_maximum_fusion.both_ref, bf16[128,2048]{1,0:T(8,128)(2,1)} %bitcast.41, bf16[128,2048]{1,0:T(8,128)(2,1)} %copy-done.4, bf16[128,2048]{1,0:T(8,128)(2,1)} %copy-done.5, ...), custom_call_target="tpu_custom_call" | custom-call | tf_op jit(solution)/shard_map/pallas_call | solution.py:358
  (55 shorter events, 60.2 us)
Async XLA Ops:
  3.3 62.4 %all-to-all-start = ((bf16[16,136,256]{2,1,0:T(8,128)(2,1)}), bf16[16,136,256]{2,1,0:T(8,128)(2,1)S(1)}, u32[]{:S(2)}, u32[]{:S(2)}) async-start(bf16[16,136,256]{2,1,0:T(8,128)(2,1)} %shard_map.102), calls=%async_computation | async-start | bytes 2228224 | tf_op jit(solution)/shard_map/all_to_all | solution.py:264
  18.4 16.3 %collective-permute-start.8 = (bf16[136,2048]{1,0:T(8,128)(2,1)S(1)}, bf16[136,2048]{1,0:T(8,128)(2,1)S(1)}, u32[]{:S(2)}, u32[]{:S(2)}) collective-permute-start(bf16[136,2048]{1,0:T(8,128)(2,1)S(1)} %bitcast.43), channel_id=1, source_target_pairs={{0,2},{2,4},{4,6},{6,0},{1,3},{3,5},{5,7},{7,1},{8,10},{10,12},{12... | collective-permute-start | bytes 1671176 | tf_op jit(solution)/shard_map/ppermute | solution.py:269
  21.5 26.1 %collective-permute-start.9 = (bf16[136,2048]{1,0:T(8,128)(2,1)S(1)}, bf16[136,2048]{1,0:T(8,128)(2,1)S(1)}, u32[]{:S(2)}, u32[]{:S(2)}) collective-permute-start(bf16[136,2048]{1,0:T(8,128)(2,1)S(1)} %bitcast.44), channel_id=1, source_target_pairs={{0,4},{2,6},{4,0},{6,2},{1,5},{3,7},{5,1},{7,3},{8,12},{10,14},{12... | collective-permute-start | bytes 1671176 | tf_op jit(solution)/shard_map/ppermute | solution.py:269
  25.9 23.6 %collective-permute-start.10 = (bf16[136,2048]{1,0:T(8,128)(2,1)S(1)}, bf16[136,2048]{1,0:T(8,128)(2,1)S(1)}, u32[]{:S(2)}, u32[]{:S(2)}) collective-permute-start(bf16[136,2048]{1,0:T(8,128)(2,1)S(1)} %bitcast.45), channel_id=1, source_target_pairs={{0,6},{2,0},{4,2},{6,4},{1,7},{3,1},{5,3},{7,5},{8,14},{10,8},{12,... | collective-permute-start | bytes 1671176 | tf_op jit(solution)/shard_map/ppermute | solution.py:269
  52.1 59.1 %copy-start.7 = (bf16[128,32]{0,1:T(8,128)(2,1)S(1)}, bf16[128,32]{0,1:T(8,128)(2,1)}, u32[]{:S(2)}) copy-start(bf16[128,32]{0,1:T(8,128)(2,1)} %param.13) | copy-start | bytes 24580
  52.1 76.9 %collective-permute-start.11 = (bf16[4,136,2048]{2,1,0:T(8,128)(2,1)}, bf16[4,136,2048]{2,1,0:T(8,128)(2,1)}, u32[]{:S(2)}, u32[]{:S(2)}) collective-permute-start(bf16[4,136,2048]{2,1,0:T(8,128)(2,1)} %shard_map.110.own_ref), channel_id=1, source_target_pairs={{0,1},{1,0},{2,3},{3,2},{4,5},{5,4},{6,7},{7,6},{8,9},{9,8},{10,11... | collective-permute-start | bytes 6684680 | tf_op jit(solution)/shard_map/ppermute | solution.py:269
  73.5 27.8 %all-to-all-start.2 = ((bf16[16,72,128]{2,1,0:T(8,128)(2,1)}), bf16[16,72,128]{2,1,0:T(8,128)(2,1)S(1)}, u32[]{:S(2)}, u32[]{:S(2)}) async-start(bf16[16,72,128]{2,1,0:T(8,128)(2,1)} %get-tuple-element.21), calls=%async_computation.2 | async-start | bytes 589824 | tf_op jit(solution)/shard_map/all_to_all | solution.py:264
  103.0 14.5 %collective-permute-start = (bf16[4,136,128]{2,1,0:T(8,128)(2,1)}, bf16[4,136,128]{2,1,0:T(8,128)(2,1)S(1)}, u32[]{:S(2)}, u32[]{:S(2)}) collective-permute-start(bf16[4,136,128]{2,1,0:T(8,128)(2,1)} %get-tuple-element.23), channel_id=1, source_target_pairs={{0,1},{1,0},{2,3},{3,2},{4,5},{5,4},{6,7},{7,6},{8,9},{9,8},{10,11... | collective-permute-start | bytes 417800 | tf_op jit(solution)/shard_map/ppermute | solution.py:269
  111.8 38.6 %all-to-all-start.3 = ((bf16[16,32,128]{2,1,0:T(8,128)(2,1)}), bf16[16,32,128]{2,1,0:T(8,128)(2,1)S(1)}, u32[]{:S(2)}, u32[]{:S(2)}) async-start(bf16[16,32,128]{2,1,0:T(8,128)(2,1)} %broadcast_in_dim.14), calls=%async_computation.3 | async-start | bytes 262144 | tf_op jit(solution)/shard_map/all_to_all | solution.py:264
  118.3 10.6 %collective-permute-start.12 = (bf16[2,136,128]{2,1,0:T(8,128)(2,1)S(1)}, bf16[2,136,128]{2,1,0:T(8,128)(2,1)S(1)}, u32[]{:S(2)}, u32[]{:S(2)}) collective-permute-start(bf16[2,136,128]{2,1,0:T(8,128)(2,1)S(1)} %get-tuple-element.32), channel_id=1, source_target_pairs={{0,2},{2,4},{4,6},{6,0},{1,3},{3,5},{5,7},{7,1},{8,10},{10,12},{12... | collective-permute-start | bytes 208904 | tf_op jit(solution)/shard_map/ppermute | solution.py:269
  121.5 7.5 %collective-permute-start.13 = (bf16[2,136,128]{2,1,0:T(8,128)(2,1)S(1)}, bf16[2,136,128]{2,1,0:T(8,128)(2,1)S(1)}, u32[]{:S(2)}, u32[]{:S(2)}) collective-permute-start(bf16[2,136,128]{2,1,0:T(8,128)(2,1)S(1)} %get-tuple-element.33), channel_id=1, source_target_pairs={{0,4},{2,6},{4,0},{6,2},{1,5},{3,7},{5,1},{7,3},{8,12},{10,14},{12... | collective-permute-start | bytes 208904 | tf_op jit(solution)/shard_map/ppermute | solution.py:269
  125.8 5.3 %collective-permute-start.14 = (bf16[2,136,128]{2,1,0:T(8,128)(2,1)S(1)}, bf16[2,136,128]{2,1,0:T(8,128)(2,1)S(1)}, u32[]{:S(2)}, u32[]{:S(2)}) collective-permute-start(bf16[2,136,128]{2,1,0:T(8,128)(2,1)S(1)} %get-tuple-element.30), channel_id=1, source_target_pairs={{0,6},{2,0},{4,2},{6,4},{1,7},{3,1},{5,3},{7,5},{8,14},{10,8},{12,... | collective-permute-start | bytes 208904 | tf_op jit(solution)/shard_map/ppermute | solution.py:269
  135.3 9.8 %collective-permute-start.17 = (bf16[32,2048]{1,0:T(8,128)(2,1)}, bf16[32,2048]{1,0:T(8,128)(2,1)S(1)}, u32[]{:S(2)}, u32[]{:S(2)}) collective-permute-start(bf16[32,2048]{1,0:T(8,128)(2,1)} %get-tuple-element.29), channel_id=1, source_target_pairs={{0,24},{8,0},{16,8},{24,16},{1,25},{9,1},{17,9},{25,17},{2,26},{10... | collective-permute-start | bytes 393224 | tf_op jit(solution)/shard_map/ppermute | solution.py:269
  137.4 8.4 %collective-permute-start.16 = (bf16[32,2048]{1,0:T(8,128)(2,1)}, bf16[32,2048]{1,0:T(8,128)(2,1)S(1)}, u32[]{:S(2)}, u32[]{:S(2)}) collective-permute-start(bf16[32,2048]{1,0:T(8,128)(2,1)} %get-tuple-element.28), channel_id=1, source_target_pairs={{0,16},{8,24},{16,0},{24,8},{1,17},{9,25},{17,1},{25,9},{2,18},{10... | collective-permute-start | bytes 393224 | tf_op jit(solution)/shard_map/ppermute | solution.py:269
  141.6 7.2 %collective-permute-start.15 = (bf16[32,2048]{1,0:T(8,128)(2,1)}, bf16[32,2048]{1,0:T(8,128)(2,1)S(1)}, u32[]{:S(2)}, u32[]{:S(2)}) collective-permute-start(bf16[32,2048]{1,0:T(8,128)(2,1)} %get-tuple-element.27), channel_id=1, source_target_pairs={{0,8},{8,16},{16,24},{24,0},{1,9},{9,17},{17,25},{25,1},{2,10},{10... | collective-permute-start | bytes 393224 | tf_op jit(solution)/shard_map/ppermute | solution.py:269
  150.4 23.1 %all-to-all-start.4 = ((bf16[16,32,128]{2,1,0:T(8,128)(2,1)}), bf16[16,32,128]{2,1,0:T(8,128)(2,1)S(1)}, u32[]{:S(2)}, u32[]{:S(2)}) async-start(bf16[16,32,128]{2,1,0:T(8,128)(2,1)} %bitcast_bitcast_fusion), calls=%async_computation.4 | async-start | bytes 262144 | tf_op jit(solution)/shard_map/all_to_all | solution.py:264
  173.5 71.2 %all-to-all-start.1 = ((bf16[16,136,128]{2,1,0:T(8,128)(2,1)}), bf16[16,136,128]{2,1,0:T(8,128)(2,1)S(1)}, u32[]{:S(2)}, u32[]{:S(2)}) async-start(bf16[16,136,128]{2,1,0:T(8,128)(2,1)} %bitcast.37), calls=%async_computation.1 | async-start | bytes 1114112 | tf_op jit(solution)/shard_map/all_to_all | solution.py:264
  184.2 9.3 %collective-permute-start.1 = (bf16[32,2048]{1,0:T(8,128)(2,1)}, bf16[32,2048]{1,0:T(8,128)(2,1)S(1)}, u32[]{:S(2)}, u32[]{:S(2)}) collective-permute-start(bf16[32,2048]{1,0:T(8,128)(2,1)} %shard_map.107.refs_0_), channel_id=1, source_target_pairs={{0,2},{2,4},{4,6},{6,0},{1,3},{3,5},{5,7},{7,1},{8,10},{10,12},{12... | collective-permute-start | bytes 393224 | tf_op jit(solution)/shard_map/ppermute | solution.py:269
  186.3 7.9 %collective-permute-start.2 = (bf16[32,2048]{1,0:T(8,128)(2,1)}, bf16[32,2048]{1,0:T(8,128)(2,1)S(1)}, u32[]{:S(2)}, u32[]{:S(2)}) collective-permute-start(bf16[32,2048]{1,0:T(8,128)(2,1)} %shard_map.107.refs_0_), channel_id=1, source_target_pairs={{0,4},{2,6},{4,0},{6,2},{1,5},{3,7},{5,1},{7,3},{8,12},{10,14},{12... | collective-permute-start | bytes 393224 | tf_op jit(solution)/shard_map/ppermute | solution.py:269
  191.6 7.0 %collective-permute-start.3 = (bf16[32,2048]{1,0:T(8,128)(2,1)}, bf16[32,2048]{1,0:T(8,128)(2,1)S(1)}, u32[]{:S(2)}, u32[]{:S(2)}) collective-permute-start(bf16[32,2048]{1,0:T(8,128)(2,1)} %shard_map.107.refs_0_), channel_id=1, source_target_pairs={{0,6},{2,0},{4,2},{6,4},{1,7},{3,1},{5,3},{7,5},{8,14},{10,8},{12,... | collective-permute-start | bytes 393224 | tf_op jit(solution)/shard_map/ppermute | solution.py:269
  200.3 12.0 %collective-permute-start.4 = (bf16[128,2048]{1,0:T(8,128)(2,1)}, bf16[128,2048]{1,0:T(8,128)(2,1)S(1)}, u32[]{:S(2)}, u32[]{:S(2)}) collective-permute-start(bf16[128,2048]{1,0:T(8,128)(2,1)} %bitcast.38), channel_id=1, source_target_pairs={{0,8},{8,16},{16,24},{24,0},{1,9},{9,17},{17,25},{25,1},{2,10},{10... | collective-permute-start | bytes 1572872 | tf_op jit(solution)/shard_map/ppermute | solution.py:269
  204.1 12.9 %collective-permute-start.5 = (bf16[128,2048]{1,0:T(8,128)(2,1)}, bf16[128,2048]{1,0:T(8,128)(2,1)S(1)}, u32[]{:S(2)}, u32[]{:S(2)}) collective-permute-start(bf16[128,2048]{1,0:T(8,128)(2,1)} %bitcast.39), channel_id=1, source_target_pairs={{0,16},{8,24},{16,0},{24,8},{1,17},{9,25},{17,1},{25,9},{2,18},{10... | collective-permute-start | bytes 1572872 | tf_op jit(solution)/shard_map/ppermute | solution.py:269
  206.6 25.7 %collective-permute-start.6 = (bf16[128,2048]{1,0:T(8,128)(2,1)}, bf16[128,2048]{1,0:T(8,128)(2,1)S(1)}, u32[]{:S(2)}, u32[]{:S(2)}) collective-permute-start(bf16[128,2048]{1,0:T(8,128)(2,1)} %bitcast.40), channel_id=1, source_target_pairs={{0,24},{8,0},{16,8},{24,16},{1,25},{9,1},{17,9},{25,17},{2,26},{10... | collective-permute-start | bytes 1572872 | tf_op jit(solution)/shard_map/ppermute | solution.py:269
  237.3 4.6 %collective-permute-start.7 = (bf16[136,2048]{1,0:T(8,128)(2,1)}, bf16[136,2048]{1,0:T(8,128)(2,1)S(1)}, u32[]{:S(2)}, u32[]{:S(2)}) collective-permute-start(bf16[136,2048]{1,0:T(8,128)(2,1)} %get-tuple-element.25), channel_id=1, source_target_pairs={{0,1},{1,0},{2,3},{3,2},{4,5},{5,4},{6,7},{7,6},{8,9},{9,8},{10,11... | collective-permute-start | bytes 1671176 | tf_op jit(solution)/shard_map/ppermute | solution.py:269
  (7 other events, 134.6 us)

commit v4 on v3

--- a/solution.py
+++ b/solution.py
@@ -9,6 +9,7 @@
 LANES = 128
 TILE = 256
 FLOOR = -1e30
+VMEM_BYTES = 24 * 1024 * 1024
 
 
 def rolled(x):
@@ -226,8 +227,8 @@
         out_ref[...] = block_ref[(place_ref[2] + step) % lines]
 
 
-def input_grad_kernel(place_ref, both_ref, *refs):
-    columns, cores, tokens, _ = both_ref.shape
+def input_grad_kernel(place_ref, first_ref, second_ref, *refs):
+    columns, tokens, _ = first_ref.shape
     weight_ref = refs[-1]
     mine_ref, away_ref = refs[-3:-1]
     lines, w_cols = weight_ref.shape[1:3]
@@ -239,14 +240,20 @@
     width = 4 * LANES
     for base in range(0, mine_ref.shape[1], width):
         cols = slice(base, base + width)
-        total = jnp.zeros((cores * tokens, width), jnp.float32)
+        first = jnp.zeros((tokens, width), jnp.float32)
+        second = jnp.zeros((tokens, width), jnp.float32)
         for step in range(columns):
             weight = weight_ref[(place_ref[1] + step) % columns, :, :, cols]
-            total = total + dot_nn(
-                both_ref[step].reshape(cores * tokens, LANES), weight.reshape(LANES, width)
-            )
-        mine_ref[:, cols] = total[:tokens]
-        away_ref[:, cols] = total[tokens:].astype(jnp.bfloat16)
+            weight = weight.reshape(LANES, width)
+            first = first + dot_nn(first_ref[step], weight)
+            second = second + dot_nn(second_ref[step], weight)
+        mine_ref[:, cols] = first
+        away_ref[:, cols] = second.astype(jnp.bfloat16)
+
+
+def add_kernel(first_ref, second_ref, out_ref):
+    total = first_ref[...] + second_ref[...].astype(jnp.float32)
+    out_ref[...] = total.astype(jnp.bfloat16)
 
 
 def unpack_pair_kernel(x_ref, q_ref, k_ref):
@@ -339,14 +346,16 @@
     mine, away = pl.pallas_call(
         unpack_value_kernel, out_shape=(block, block), in_specs=[small, whole]
     )(place, near(value_back))
-    both = jnp.stack([mine, shifted(away, "core", 1)], axis=1)
+    brought = shifted(away, "core", 1)
+    both = jnp.stack([mine, brought], axis=1)
     pieces = [both[0]] + [shifted(both[step], "x", step) for step in range(1, columns)]
     partial = pl.pallas_call(
         product_kernel,
+        compiler_params=pltpu.CompilerParams(vmem_limit_bytes=VMEM_BYTES),
         out_shape=(shaped(w_cols, model),) * lines,
         in_specs=[small] + [whole] * (2 + columns),
         scratch_shapes=[pltpu.VMEM((lines, w_cols, model), jnp.bfloat16)],
-    )(place, own_rows, near(other_rows), *map(near, pieces))
+    )(place, near(own_rows), near(other_rows), *map(near, pieces))
     partial = [partial[0]] + [shifted(partial[step], "y", step) for step in range(1, lines)]
     partial = sum(part.astype(jnp.float32) for part in partial).astype(jnp.bfloat16)
     partial = jnp.moveaxis(partial.reshape(w_cols, planes, model // planes), 1, 0)
@@ -358,10 +367,12 @@
     kept_part, sent_part = pl.pallas_call(
         input_grad_kernel,
         out_shape=(shaped(tokens, model, dtype=jnp.float32), shaped(tokens, model)),
-        in_specs=[small] + [whole] * (1 + lines),
+        in_specs=[small] + [whole] * (2 + lines),
         scratch_shapes=[pltpu.VMEM((columns, lines, w_cols, model), jnp.bfloat16)],
-    )(place, both, *weight_pieces)
-    input_grad = (kept_part + shifted(sent_part, "core", 1)).astype(jnp.bfloat16)
+    )(place, mine, near(brought), *weight_pieces)
+    input_grad = pl.pallas_call(add_kernel, out_shape=shaped(tokens, model))(
+        kept_part, near(shifted(sent_part, "core", 1))
+    )
     return (query_grad[None], key_grad[None], input_grad[None], weight_grad)
 
 

time: 247 us -> 245 us (level)
  other arithmetic: 6.6 us -> 2.81 us
  transfers between devices with their start and end apart: 23 -> 23, of which waited for: 15 -> 15; matrix products, arithmetic and copies ran while one was open for 3% -> 1% of each run, Pallas kernels for 13% -> 13%
where the time goes in v4:
time: 245 us; the launch traced here: 244 us
  starting transfers between devices  118 us (48%)
  waiting for transfers between devices  82.2 us (34%)
  Pallas kernels  36.3 us (15%)
  local copies, waits for them, and re-layouts  3.11 us (1%)
  other arithmetic  2.81 us (1%)
    ppermute x18, starting transfers between devices, shifted(): lax.ppermute(x, axis, [(place, (place + step) % count) for place in range...  64.3 us
    ppermute x18, waiting for transfers between devices, shifted(): lax.ppermute(x, axis, [(place, (place + step) % count) for place in range...  55.5 us
    all_to_all x5, starting transfers between devices, exchanged(): return lax.all_to_all(x, axis, split_axis=0, concat_axis=0, tiled=True)  53.9 us
    all_to_all x5, waiting for transfers between devices, exchanged(): return lax.all_to_all(x, axis, split_axis=0, concat_axis=0, tiled=True)  26.7 us
    pallas_call x1, Pallas kernels, shards(): pl.pallas_call(pair_kernel, out_shape=shaped(length, LANES), scratch_shap...  9.13 us
    pallas_call x1, Pallas kernels, shards(): pl.pallas_call(value_kernel, out_shape=(shaped(planes, kept, LANES), row,...  7.74 us
  transfers between devices with their start and end apart: 23, of which 15 were waited for; matrix products, arithmetic and copies ran while one was open for 1% of the time, Pallas kernels for 13%

profile of v4, /device:TPU:9, one launch (start us, length us, event | category | flops | bytes accessed | tf_op | source)
XLA Modules:
  0.0 243.6 jit_solution(14647131847184100833)
XLA Ops:
  3.3 15.0 %all-to-all-start = ((bf16[16,136,256]{2,1,0:T(8,128)(2,1)}), bf16[16,136,256]{2,1,0:T(8,128)(2,1)S(1)}, u32[]{:S(2)}, u32[]{:S(2)}) async-start(bf16[16,136,256]{2,1,0:T(8,128)(2,1)} %shard_map.102), calls=%async_computation | async-start | bytes 2228224 | tf_op jit(solution)/shard_map/all_to_all | solution.py:271
  21.5 4.4 %collective-permute-start.9 = (bf16[136,2048]{1,0:T(8,128)(2,1)S(1)}, bf16[136,2048]{1,0:T(8,128)(2,1)S(1)}, u32[]{:S(2)}, u32[]{:S(2)}) collective-permute-start(bf16[136,2048]{1,0:T(8,128)(2,1)S(1)} %bitcast.44), channel_id=1, source_target_pairs={{0,4},{2,6},{4,0},{6,2},{1,5},{3,7},{5,1},{7,3},{8,12},{10,14},{12... | collective-permute-start | bytes 1671176 | tf_op jit(solution)/shard_map/ppermute | solution.py:276
  29.0 5.8 %collective-permute-done.8.refs_1_ = bf16[136,2048]{1,0:T(8,128)(2,1)S(1)} collective-permute-done((bf16[136,2048]{1,0:T(8,128)(2,1)S(1)}, bf16[136,2048]{1,0:T(8,128)(2,1)S(1)}, u32[]{:S(2)}, u32[]{:S(2)}) %collective-permute-start.8) | collective-permute-done | bytes 557088 | tf_op jit(solution)/shard_map/ppermute | solution.py:276
  34.7 12.9 %collective-permute-done.9.refs_2_ = bf16[136,2048]{1,0:T(8,128)(2,1)S(1)} collective-permute-done((bf16[136,2048]{1,0:T(8,128)(2,1)S(1)}, bf16[136,2048]{1,0:T(8,128)(2,1)S(1)}, u32[]{:S(2)}, u32[]{:S(2)}) %collective-permute-start.9) | collective-permute-done | bytes 557088 | tf_op jit(solution)/shard_map/ppermute | solution.py:276
  52.1 3.6 %collective-permute-start.11 = (bf16[4,136,2048]{2,1,0:T(8,128)(2,1)}, bf16[4,136,2048]{2,1,0:T(8,128)(2,1)}, u32[]{:S(2)}, u32[]{:S(2)}) collective-permute-start(bf16[4,136,2048]{2,1,0:T(8,128)(2,1)} %shard_map.111.own_ref), channel_id=1, source_target_pairs={{0,1},{1,0},{2,3},{3,2},{4,5},{5,4},{6,7},{7,6},{8,9},{9,8},{10,11... | collective-permute-start | bytes 6684680 | tf_op jit(solution)/shard_map/ppermute | solution.py:276
  55.6 10.1 %all-to-all-done = bf16[16,136,256]{2,1,0:T(8,128)(2,1)S(1)} async-done(((bf16[16,136,256]{2,1,0:T(8,128)(2,1)}), bf16[16,136,256]{2,1,0:T(8,128)(2,1)S(1)}, u32[]{:S(2)}, u32[]{:S(2)}) %all-to-all-start) | async-done | bytes 1114144 | tf_op jit(solution)/shard_map/all_to_all | solution.py:271
  65.8 7.7 %shard_map.103 = (bf16[16,72,128]{2,1,0:T(8,128)(2,1)}, f32[1,2176]{1,0:T(1,128)}, f32[1,2176]{1,0:T(1,128)}) custom-call(bf16[2176,256]{1,0:T(8,128)(2,1)S(1)} %bitcast.34, f32[1,2176]{1,0:T(1,128)} %bitcast.52), custom_call_target="tpu_custom_call" | custom-call | tf_op jit(solution)/shard_map/pallas_call | solution.py:326
  73.5 13.5 %all-to-all-start.2 = ((bf16[16,72,128]{2,1,0:T(8,128)(2,1)}), bf16[16,72,128]{2,1,0:T(8,128)(2,1)S(1)}, u32[]{:S(2)}, u32[]{:S(2)}) async-start(bf16[16,72,128]{2,1,0:T(8,128)(2,1)} %get-tuple-element.21), calls=%async_computation.2 | async-start | bytes 589824 | tf_op jit(solution)/shard_map/all_to_all | solution.py:271
  87.6 13.7 %all-to-all-done.2.x_ref = bf16[16,72,128]{2,1,0:T(8,128)(2,1)S(1)} async-done(((bf16[16,72,128]{2,1,0:T(8,128)(2,1)}), bf16[16,72,128]{2,1,0:T(8,128)(2,1)S(1)}, u32[]{:S(2)}, u32[]{:S(2)}) %all-to-all-start.2) | async-done | bytes 294944 | tf_op jit(solution)/shard_map/all_to_all | solution.py:271
  103.0 8.1 %collective-permute-start = (bf16[4,136,128]{2,1,0:T(8,128)(2,1)}, bf16[4,136,128]{2,1,0:T(8,128)(2,1)S(1)}, u32[]{:S(2)}, u32[]{:S(2)}) collective-permute-start(bf16[4,136,128]{2,1,0:T(8,128)(2,1)} %get-tuple-element.23), channel_id=1, source_target_pairs={{0,1},{1,0},{2,3},{3,2},{4,5},{5,4},{6,7},{7,6},{8,9},{9,8},{10,11... | collective-permute-start | bytes 417800 | tf_op jit(solution)/shard_map/ppermute | solution.py:276
  111.8 5.7 %all-to-all-start.3 = ((bf16[16,32,128]{2,1,0:T(8,128)(2,1)}), bf16[16,32,128]{2,1,0:T(8,128)(2,1)S(1)}, u32[]{:S(2)}, u32[]{:S(2)}) async-start(bf16[16,32,128]{2,1,0:T(8,128)(2,1)} %broadcast_in_dim.14), calls=%async_computation.3 | async-start | bytes 262144 | tf_op jit(solution)/shard_map/all_to_all | solution.py:271
  121.5 4.4 %collective-permute-start.13 = (bf16[2,136,128]{2,1,0:T(8,128)(2,1)S(1)}, bf16[2,136,128]{2,1,0:T(8,128)(2,1)S(1)}, u32[]{:S(2)}, u32[]{:S(2)}) collective-permute-start(bf16[2,136,128]{2,1,0:T(8,128)(2,1)S(1)} %get-tuple-element.33), channel_id=1, source_target_pairs={{0,4},{2,6},{4,0},{6,2},{1,5},{3,7},{5,1},{7,3},{8,12},{10,14},{12... | collective-permute-start | bytes 208904 | tf_op jit(solution)/shard_map/ppermute | solution.py:276
  137.6 4.2 %collective-permute-start.16 = (bf16[32,2048]{1,0:T(8,128)(2,1)S(1)}, bf16[32,2048]{1,0:T(8,128)(2,1)S(1)}, u32[]{:S(2)}, u32[]{:S(2)}) collective-permute-start(bf16[32,2048]{1,0:T(8,128)(2,1)S(1)} %get-tuple-element.28), channel_id=1, source_target_pairs={{0,16},{8,24},{16,0},{24,8},{1,17},{9,25},{17,1},{25,9},{2,18},{10... | collective-permute-start | bytes 393224 | tf_op jit(solution)/shard_map/ppermute | solution.py:276
  141.8 3.5 %collective-permute-start.15 = (bf16[32,2048]{1,0:T(8,128)(2,1)S(1)}, bf16[32,2048]{1,0:T(8,128)(2,1)S(1)}, u32[]{:S(2)}, u32[]{:S(2)}) collective-permute-start(bf16[32,2048]{1,0:T(8,128)(2,1)S(1)} %get-tuple-element.27), channel_id=1, source_target_pairs={{0,8},{8,16},{16,24},{24,0},{1,9},{9,17},{17,25},{25,1},{2,10},{10... | collective-permute-start | bytes 393224 | tf_op jit(solution)/shard_map/ppermute | solution.py:276
  149.5 11.0 %all-to-all-start.4 = ((bf16[16,32,128]{2,1,0:T(8,128)(2,1)}), bf16[16,32,128]{2,1,0:T(8,128)(2,1)S(1)}, u32[]{:S(2)}, u32[]{:S(2)}) async-start(bf16[16,32,128]{2,1,0:T(8,128)(2,1)} %bitcast_bitcast_fusion), calls=%async_computation.4 | async-start | bytes 262144 | tf_op jit(solution)/shard_map/all_to_all | solution.py:271
  160.5 9.1 %shard_map.104 = bf16[2176,128]{1,0:T(8,128)(2,1)} custom-call(bf16[2176,256]{1,0:T(8,128)(2,1)S(1)} %bitcast.35, f32[1,2176]{1,0:T(1,128)} %bitcast.53, f32[1,2176]{1,0:T(1,128)} %get-tuple-element.17.peak_ref, f32[1,2176]{1,0:T(1,128)} %get-tuple-element.18.share_ref), custom_call_target="tpu_custom_call" | custom-call | tf_op jit(solution)/shard_map/pallas_call | solution.py:332
  172.5 8.6 %all-to-all-start.1 = ((bf16[16,136,128]{2,1,0:T(8,128)(2,1)}), bf16[16,136,128]{2,1,0:T(8,128)(2,1)S(1)}, u32[]{:S(2)}, u32[]{:S(2)}) async-start(bf16[16,136,128]{2,1,0:T(8,128)(2,1)} %bitcast.37), calls=%async_computation.1 | async-start | bytes 1114112 | tf_op jit(solution)/shard_map/all_to_all | solution.py:271
  184.0 5.2 %collective-permute-start.2 = (bf16[32,2048]{1,0:T(8,128)(2,1)}, bf16[32,2048]{1,0:T(8,128)(2,1)S(1)}, u32[]{:S(2)}, u32[]{:S(2)}) collective-permute-start(bf16[32,2048]{1,0:T(8,128)(2,1)} %shard_map.107.refs_0_), channel_id=1, source_target_pairs={{0,4},{2,6},{4,0},{6,2},{1,5},{3,7},{5,1},{7,3},{8,12},{10,14},{12... | collective-permute-start | bytes 393224 | tf_op jit(solution)/shard_map/ppermute | solution.py:276
  191.7 4.3 %collective-permute-done.3.refs_3_ = bf16[32,2048]{1,0:T(8,128)(2,1)S(1)} collective-permute-done((bf16[32,2048]{1,0:T(8,128)(2,1)}, bf16[32,2048]{1,0:T(8,128)(2,1)S(1)}, u32[]{:S(2)}, u32[]{:S(2)}) %collective-permute-start.3) | collective-permute-done | bytes 131104 | tf_op jit(solution)/shard_map/ppermute | solution.py:276
  197.8 4.1 %collective-permute-start.4 = (bf16[128,2048]{1,0:T(8,128)(2,1)}, bf16[128,2048]{1,0:T(8,128)(2,1)S(1)}, u32[]{:S(2)}, u32[]{:S(2)}) collective-permute-start(bf16[128,2048]{1,0:T(8,128)(2,1)} %bitcast.38), channel_id=1, source_target_pairs={{0,8},{8,16},{16,24},{24,0},{1,9},{9,17},{17,25},{25,1},{2,10},{10... | collective-permute-start | bytes 1572872 | tf_op jit(solution)/shard_map/ppermute | solution.py:276
  207.5 3.4 %collective-permute-done.4.refs_1_ = bf16[128,2048]{1,0:T(8,128)(2,1)S(1)} collective-permute-done((bf16[128,2048]{1,0:T(8,128)(2,1)}, bf16[128,2048]{1,0:T(8,128)(2,1)S(1)}, u32[]{:S(2)}, u32[]{:S(2)}) %collective-permute-start.4) | collective-permute-done | bytes 524320 | tf_op jit(solution)/shard_map/ppermute | solution.py:276
  210.9 4.0 %collective-permute-done.5.refs_2_ = bf16[128,2048]{1,0:T(8,128)(2,1)S(1)} collective-permute-done((bf16[128,2048]{1,0:T(8,128)(2,1)}, bf16[128,2048]{1,0:T(8,128)(2,1)S(1)}, u32[]{:S(2)}, u32[]{:S(2)}) %collective-permute-start.5) | collective-permute-done | bytes 524320 | tf_op jit(solution)/shard_map/ppermute | solution.py:276
  214.8 15.3 %collective-permute-done.6.refs_3_ = bf16[128,2048]{1,0:T(8,128)(2,1)S(1)} collective-permute-done((bf16[128,2048]{1,0:T(8,128)(2,1)}, bf16[128,2048]{1,0:T(8,128)(2,1)S(1)}, u32[]{:S(2)}, u32[]{:S(2)}) %collective-permute-start.6) | collective-permute-done | bytes 524320 | tf_op jit(solution)/shard_map/ppermute | solution.py:276
  231.0 4.2 %shard_map.109 = (f32[136,2048]{1,0:T(8,128)}, bf16[136,2048]{1,0:T(8,128)(2,1)}) custom-call(s32[3]{0:T(128)} %pad_add_fusion.place_ref, bf16[4,136,128]{2,1,0:T(8,128)(2,1)} %get-tuple-element.22.first_ref, bf16[4,136,128]{2,1,0:T(8,128)(2,1)S(1)} %collective-permute-done.second_ref, bf16[128,2048]{1,0:T(8,128)(2,1)} %bitcast.41, ...), custom_call_target="tpu_custom_call" | custom-call | tf_op jit(solution)/shard_map/pallas_call | solution.py:367
  (52 shorter events, 60.9 us)
Async XLA Ops:
  3.3 62.4 %all-to-all-start = ((bf16[16,136,256]{2,1,0:T(8,128)(2,1)}), bf16[16,136,256]{2,1,0:T(8,128)(2,1)S(1)}, u32[]{:S(2)}, u32[]{:S(2)}) async-start(bf16[16,136,256]{2,1,0:T(8,128)(2,1)} %shard_map.102), calls=%async_computation | async-start | bytes 2228224 | tf_op jit(solution)/shard_map/all_to_all | solution.py:271
  18.4 16.3 %collective-permute-start.8 = (bf16[136,2048]{1,0:T(8,128)(2,1)S(1)}, bf16[136,2048]{1,0:T(8,128)(2,1)S(1)}, u32[]{:S(2)}, u32[]{:S(2)}) collective-permute-start(bf16[136,2048]{1,0:T(8,128)(2,1)S(1)} %bitcast.43), channel_id=1, source_target_pairs={{0,2},{2,4},{4,6},{6,0},{1,3},{3,5},{5,7},{7,1},{8,10},{10,12},{12... | collective-permute-start | bytes 1671176 | tf_op jit(solution)/shard_map/ppermute | solution.py:276
  21.5 26.1 %collective-permute-start.9 = (bf16[136,2048]{1,0:T(8,128)(2,1)S(1)}, bf16[136,2048]{1,0:T(8,128)(2,1)S(1)}, u32[]{:S(2)}, u32[]{:S(2)}) collective-permute-start(bf16[136,2048]{1,0:T(8,128)(2,1)S(1)} %bitcast.44), channel_id=1, source_target_pairs={{0,4},{2,6},{4,0},{6,2},{1,5},{3,7},{5,1},{7,3},{8,12},{10,14},{12... | collective-permute-start | bytes 1671176 | tf_op jit(solution)/shard_map/ppermute | solution.py:276
  25.9 23.6 %collective-permute-start.10 = (bf16[136,2048]{1,0:T(8,128)(2,1)S(1)}, bf16[136,2048]{1,0:T(8,128)(2,1)S(1)}, u32[]{:S(2)}, u32[]{:S(2)}) collective-permute-start(bf16[136,2048]{1,0:T(8,128)(2,1)S(1)} %bitcast.45), channel_id=1, source_target_pairs={{0,6},{2,0},{4,2},{6,4},{1,7},{3,1},{5,3},{7,5},{8,14},{10,8},{12,... | collective-permute-start | bytes 1671176 | tf_op jit(solution)/shard_map/ppermute | solution.py:276
  52.1 59.0 %copy-start.6 = (bf16[128,32]{0,1:T(8,128)(2,1)S(1)}, bf16[128,32]{0,1:T(8,128)(2,1)}, u32[]{:S(2)}) copy-start(bf16[128,32]{0,1:T(8,128)(2,1)} %param.13) | copy-start | bytes 24580
  52.1 76.9 %collective-permute-start.11 = (bf16[4,136,2048]{2,1,0:T(8,128)(2,1)}, bf16[4,136,2048]{2,1,0:T(8,128)(2,1)}, u32[]{:S(2)}, u32[]{:S(2)}) collective-permute-start(bf16[4,136,2048]{2,1,0:T(8,128)(2,1)} %shard_map.111.own_ref), channel_id=1, source_target_pairs={{0,1},{1,0},{2,3},{3,2},{4,5},{5,4},{6,7},{7,6},{8,9},{9,8},{10,11... | collective-permute-start | bytes 6684680 | tf_op jit(solution)/shard_map/ppermute | solution.py:276
  73.5 27.8 %all-to-all-start.2 = ((bf16[16,72,128]{2,1,0:T(8,128)(2,1)}), bf16[16,72,128]{2,1,0:T(8,128)(2,1)S(1)}, u32[]{:S(2)}, u32[]{:S(2)}) async-start(bf16[16,72,128]{2,1,0:T(8,128)(2,1)} %get-tuple-element.21), calls=%async_computation.2 | async-start | bytes 589824 | tf_op jit(solution)/shard_map/all_to_all | solution.py:271
  103.0 14.5 %collective-permute-start = (bf16[4,136,128]{2,1,0:T(8,128)(2,1)}, bf16[4,136,128]{2,1,0:T(8,128)(2,1)S(1)}, u32[]{:S(2)}, u32[]{:S(2)}) collective-permute-start(bf16[4,136,128]{2,1,0:T(8,128)(2,1)} %get-tuple-element.23), channel_id=1, source_target_pairs={{0,1},{1,0},{2,3},{3,2},{4,5},{5,4},{6,7},{7,6},{8,9},{9,8},{10,11... | collective-permute-start | bytes 417800 | tf_op jit(solution)/shard_map/ppermute | solution.py:276
  111.8 37.7 %all-to-all-start.3 = ((bf16[16,32,128]{2,1,0:T(8,128)(2,1)}), bf16[16,32,128]{2,1,0:T(8,128)(2,1)S(1)}, u32[]{:S(2)}, u32[]{:S(2)}) async-start(bf16[16,32,128]{2,1,0:T(8,128)(2,1)} %broadcast_in_dim.14), calls=%async_computation.3 | async-start | bytes 262144 | tf_op jit(solution)/shard_map/all_to_all | solution.py:271
  118.3 10.6 %collective-permute-start.12 = (bf16[2,136,128]{2,1,0:T(8,128)(2,1)S(1)}, bf16[2,136,128]{2,1,0:T(8,128)(2,1)S(1)}, u32[]{:S(2)}, u32[]{:S(2)}) collective-permute-start(bf16[2,136,128]{2,1,0:T(8,128)(2,1)S(1)} %get-tuple-element.32), channel_id=1, source_target_pairs={{0,2},{2,4},{4,6},{6,0},{1,3},{3,5},{5,7},{7,1},{8,10},{10,12},{12... | collective-permute-start | bytes 208904 | tf_op jit(solution)/shard_map/ppermute | solution.py:276
  121.5 7.5 %collective-permute-start.13 = (bf16[2,136,128]{2,1,0:T(8,128)(2,1)S(1)}, bf16[2,136,128]{2,1,0:T(8,128)(2,1)S(1)}, u32[]{:S(2)}, u32[]{:S(2)}) collective-permute-start(bf16[2,136,128]{2,1,0:T(8,128)(2,1)S(1)} %get-tuple-element.33), channel_id=1, source_target_pairs={{0,4},{2,6},{4,0},{6,2},{1,5},{3,7},{5,1},{7,3},{8,12},{10,14},{12... | collective-permute-start | bytes 208904 | tf_op jit(solution)/shard_map/ppermute | solution.py:276
  125.8 5.3 %collective-permute-start.14 = (bf16[2,136,128]{2,1,0:T(8,128)(2,1)S(1)}, bf16[2,136,128]{2,1,0:T(8,128)(2,1)S(1)}, u32[]{:S(2)}, u32[]{:S(2)}) collective-permute-start(bf16[2,136,128]{2,1,0:T(8,128)(2,1)S(1)} %get-tuple-element.30), channel_id=1, source_target_pairs={{0,6},{2,0},{4,2},{6,4},{1,7},{3,1},{5,3},{7,5},{8,14},{10,8},{12,... | collective-permute-start | bytes 208904 | tf_op jit(solution)/shard_map/ppermute | solution.py:276
  135.5 9.8 %collective-permute-start.17 = (bf16[32,2048]{1,0:T(8,128)(2,1)S(1)}, bf16[32,2048]{1,0:T(8,128)(2,1)S(1)}, u32[]{:S(2)}, u32[]{:S(2)}) collective-permute-start(bf16[32,2048]{1,0:T(8,128)(2,1)S(1)} %get-tuple-element.29), channel_id=1, source_target_pairs={{0,24},{8,0},{16,8},{24,16},{1,25},{9,1},{17,9},{25,17},{2,26},{10... | collective-permute-start | bytes 393224 | tf_op jit(solution)/shard_map/ppermute | solution.py:276
  137.6 8.2 %collective-permute-start.16 = (bf16[32,2048]{1,0:T(8,128)(2,1)S(1)}, bf16[32,2048]{1,0:T(8,128)(2,1)S(1)}, u32[]{:S(2)}, u32[]{:S(2)}) collective-permute-start(bf16[32,2048]{1,0:T(8,128)(2,1)S(1)} %get-tuple-element.28), channel_id=1, source_target_pairs={{0,16},{8,24},{16,0},{24,8},{1,17},{9,25},{17,1},{25,9},{2,18},{10... | collective-permute-start | bytes 393224 | tf_op jit(solution)/shard_map/ppermute | solution.py:276
  141.8 7.0 %collective-permute-start.15 = (bf16[32,2048]{1,0:T(8,128)(2,1)S(1)}, bf16[32,2048]{1,0:T(8,128)(2,1)S(1)}, u32[]{:S(2)}, u32[]{:S(2)}) collective-permute-start(bf16[32,2048]{1,0:T(8,128)(2,1)S(1)} %get-tuple-element.27), channel_id=1, source_target_pairs={{0,8},{8,16},{16,24},{24,0},{1,9},{9,17},{17,25},{25,1},{2,10},{10... | collective-permute-start | bytes 393224 | tf_op jit(solution)/shard_map/ppermute | solution.py:276
  149.5 23.0 %all-to-all-start.4 = ((bf16[16,32,128]{2,1,0:T(8,128)(2,1)}), bf16[16,32,128]{2,1,0:T(8,128)(2,1)S(1)}, u32[]{:S(2)}, u32[]{:S(2)}) async-start(bf16[16,32,128]{2,1,0:T(8,128)(2,1)} %bitcast_bitcast_fusion), calls=%async_computation.4 | async-start | bytes 262144 | tf_op jit(solution)/shard_map/all_to_all | solution.py:271
  172.5 70.0 %all-to-all-start.1 = ((bf16[16,136,128]{2,1,0:T(8,128)(2,1)}), bf16[16,136,128]{2,1,0:T(8,128)(2,1)S(1)}, u32[]{:S(2)}, u32[]{:S(2)}) async-start(bf16[16,136,128]{2,1,0:T(8,128)(2,1)} %bitcast.37), calls=%async_computation.1 | async-start | bytes 1114112 | tf_op jit(solution)/shard_map/all_to_all | solution.py:271
  181.8 9.3 %collective-permute-start.1 = (bf16[32,2048]{1,0:T(8,128)(2,1)}, bf16[32,2048]{1,0:T(8,128)(2,1)S(1)}, u32[]{:S(2)}, u32[]{:S(2)}) collective-permute-start(bf16[32,2048]{1,0:T(8,128)(2,1)} %shard_map.107.refs_0_), channel_id=1, source_target_pairs={{0,2},{2,4},{4,6},{6,0},{1,3},{3,5},{5,7},{7,1},{8,10},{10,12},{12... | collective-permute-start | bytes 393224 | tf_op jit(solution)/shard_map/ppermute | solution.py:276
  184.0 7.7 %collective-permute-start.2 = (bf16[32,2048]{1,0:T(8,128)(2,1)}, bf16[32,2048]{1,0:T(8,128)(2,1)S(1)}, u32[]{:S(2)}, u32[]{:S(2)}) collective-permute-start(bf16[32,2048]{1,0:T(8,128)(2,1)} %shard_map.107.refs_0_), channel_id=1, source_target_pairs={{0,4},{2,6},{4,0},{6,2},{1,5},{3,7},{5,1},{7,3},{8,12},{10,14},{12... | collective-permute-start | bytes 393224 | tf_op jit(solution)/shard_map/ppermute | solution.py:276
  189.2 6.8 %collective-permute-start.3 = (bf16[32,2048]{1,0:T(8,128)(2,1)}, bf16[32,2048]{1,0:T(8,128)(2,1)S(1)}, u32[]{:S(2)}, u32[]{:S(2)}) collective-permute-start(bf16[32,2048]{1,0:T(8,128)(2,1)} %shard_map.107.refs_0_), channel_id=1, source_target_pairs={{0,6},{2,0},{4,2},{6,4},{1,7},{3,1},{5,3},{7,5},{8,14},{10,8},{12,... | collective-permute-start | bytes 393224 | tf_op jit(solution)/shard_map/ppermute | solution.py:276
  197.8 13.1 %collective-permute-start.4 = (bf16[128,2048]{1,0:T(8,128)(2,1)}, bf16[128,2048]{1,0:T(8,128)(2,1)S(1)}, u32[]{:S(2)}, u32[]{:S(2)}) collective-permute-start(bf16[128,2048]{1,0:T(8,128)(2,1)} %bitcast.38), channel_id=1, source_target_pairs={{0,8},{8,16},{16,24},{24,0},{1,9},{9,17},{17,25},{25,1},{2,10},{10... | collective-permute-start | bytes 1572872 | tf_op jit(solution)/shard_map/ppermute | solution.py:276
  201.9 13.0 %collective-permute-start.5 = (bf16[128,2048]{1,0:T(8,128)(2,1)}, bf16[128,2048]{1,0:T(8,128)(2,1)S(1)}, u32[]{:S(2)}, u32[]{:S(2)}) collective-permute-start(bf16[128,2048]{1,0:T(8,128)(2,1)} %bitcast.39), channel_id=1, source_target_pairs={{0,16},{8,24},{16,0},{24,8},{1,17},{9,25},{17,1},{25,9},{2,18},{10... | collective-permute-start | bytes 1572872 | tf_op jit(solution)/shard_map/ppermute | solution.py:276
  204.4 25.8 %collective-permute-start.6 = (bf16[128,2048]{1,0:T(8,128)(2,1)}, bf16[128,2048]{1,0:T(8,128)(2,1)S(1)}, u32[]{:S(2)}, u32[]{:S(2)}) collective-permute-start(bf16[128,2048]{1,0:T(8,128)(2,1)} %bitcast.40), channel_id=1, source_target_pairs={{0,24},{8,0},{16,8},{24,16},{1,25},{9,1},{17,9},{25,17},{2,26},{10... | collective-permute-start | bytes 1572872 | tf_op jit(solution)/shard_map/ppermute | solution.py:276
  235.2 4.6 %collective-permute-start.7 = (bf16[136,2048]{1,0:T(8,128)(2,1)}, bf16[136,2048]{1,0:T(8,128)(2,1)S(1)}, u32[]{:S(2)}, u32[]{:S(2)}) collective-permute-start(bf16[136,2048]{1,0:T(8,128)(2,1)} %get-tuple-element.25), channel_id=1, source_target_pairs={{0,1},{1,0},{2,3},{3,2},{4,5},{5,4},{6,7},{7,6},{8,9},{9,8},{10,11... | collective-permute-start | bytes 1671176 | tf_op jit(solution)/shard_map/ppermute | solution.py:276
  (6 other events, 95.7 us)

commit v5 on v4

--- a/solution.py
+++ b/solution.py
@@ -114,16 +114,23 @@
             u_here = slice(u_base, u_base + u_rows)
             soft = s_ref[u_here, :q_rows] * share
             acc_ref[u_here] += dot_nn(soft.astype(jnp.bfloat16), grad_low)
-    planes, kept, _ = v_out_ref.shape
+    planes, cores, kept, _ = v_out_ref.shape
     tokens = length // planes
+    quarter = HEAD_DIM // cores
+    lane = lax.broadcasted_iota(jnp.int32, (kept, LANES), 1)
     for plane in range(planes):
-        base = plane * tokens
-        first = acc_ref[base : base + kept]
-        second = acc_ref[base + kept : base + tokens]
-        second = jnp.concatenate([second, first[: 2 * kept - tokens]], axis=0)
-        v_out_ref[plane] = jnp.where(low_lanes(first.shape), first, rolled(second)).astype(
-            jnp.bfloat16
-        )
+        for core in range(cores):
+            packed = jnp.zeros((kept, LANES), jnp.float32)
+            for group in range(LANES // quarter):
+                base = plane * tokens + group * kept
+                rows = min(kept, tokens - group * kept)
+                part = acc_ref[base : base + rows]
+                if rows < kept:
+                    part = jnp.concatenate([part, jnp.zeros((kept - rows, LANES), jnp.float32)])
+                home = group * quarter
+                part = pltpu.roll(part, (home - core * quarter) % LANES, 1)
+                packed = jnp.where((lane >= home) & (lane < home + quarter), part, packed)
+            v_out_ref[plane, core] = packed.astype(jnp.bfloat16)
 
 
 def pair_kernel(
@@ -164,28 +171,33 @@
         qk_ref[here] = (acc_ref[here] * scale).astype(jnp.bfloat16)
 
 
-def unpack_value_kernel(place_ref, x_ref, mine_ref, away_ref):
-    heads, kept, _ = x_ref.shape
-    columns, tokens, _ = mine_ref.shape
-    rest = tokens - kept
-    cores = HEAD_DIM * columns // LANES
+def pair_steps(here):
+    return [here, 3 - here, here + 1 - 2 * (here % 2), (here + 2) % 4]
+
+
+def unpack_value_kernel(place_ref, x_ref, own_ref, flip_ref, far_ref):
+    cores, tokens, _ = own_ref.shape
+    out_refs = [own_ref, flip_ref, far_ref.at[0], far_ref.at[1]]
+    columns = len(out_refs)
+    heads, kept = x_ref.shape[0] // cores, x_ref.shape[1]
     quarter = HEAD_DIM // cores
+    groups = LANES // quarter
     lane = lax.broadcasted_iota(jnp.int32, (tokens, LANES), 1)
-    first_core = place_ref[0] == 0
-    for column in range(columns):
-        step = (column + columns - place_ref[1]) % columns
-        parts = [jnp.zeros((tokens, LANES), jnp.float32)] * cores
-        for group in range(heads // columns):
-            block = x_ref[group * columns + column].astype(jnp.float32)
-            for core in range(cores):
-                home = group * quarter
-                top = pltpu.roll(block, (home - core * quarter) % LANES, 1)
-                bottom = pltpu.roll(block, (home - core * quarter - HEAD_DIM) % LANES, 1)[:rest]
-                moved = jnp.concatenate([top, bottom], axis=0)
-                inside = (lane >= home) & (lane < home + quarter)
-                parts[core] = jnp.where(inside, moved, parts[core])
-        mine_ref[step] = jnp.where(first_core, parts[0], parts[1]).astype(jnp.bfloat16)
-        away_ref[step] = jnp.where(first_core, parts[1], parts[0]).astype(jnp.bfloat16)
+    for out_ref, column in zip(out_refs, pair_steps(place_ref[1])):
+        for source in range(cores):
+            whole = jnp.zeros((tokens, LANES), jnp.float32)
+            for line in range(heads // columns):
+                block = x_ref[(line * columns + column) * cores + source].astype(jnp.float32)
+                home = line * quarter
+                rows = [
+                    pltpu.roll(block, (home - group * quarter) % LANES, 1)[
+                        : min(kept, tokens - group * kept)
+                    ]
+                    for group in range(groups)
+                ]
+                moved = jnp.concatenate(rows, axis=0)
+                whole = jnp.where((lane >= home) & (lane < home + quarter), moved, whole)
+            out_ref[(source + cores - place_ref[0]) % cores] = whole.astype(jnp.bfloat16)
 
 
 def weight_open_kernel(x_ref, out_ref):
@@ -209,14 +221,16 @@
     return lax.dot_general(a, b, (((0,), (0,)), ((), ())), preferred_element_type=jnp.float32)
 
 
-def product_kernel(place_ref, own_ref, other_ref, *refs):
-    columns = own_ref.shape[0]
-    pieces, (block_ref,) = refs[:columns], refs[-1:]
-    outs = refs[columns:-1]
+def product_kernel(place_ref, own_ref, other_ref, here_ref, first_ref, second_ref, *refs):
+    outs, block_ref = refs[:-1], refs[-1]
     lines, w_cols, model = block_ref.shape
     width = 4 * LANES
-    own = jnp.concatenate([piece[0] for piece in pieces], axis=0)
-    other = jnp.concatenate([piece[1] for piece in pieces], axis=0)
+    own, other = (
+        jnp.concatenate(
+            [here_ref[core], second_ref[0, core], first_ref[0, core], second_ref[1, core]], axis=0
+        )
+        for core in range(here_ref.shape[0])
+    )
     rows = own.shape[0]
     for base in range(0, model, width):
         cols = slice(base, base + width)
@@ -227,11 +241,14 @@
         out_ref[...] = block_ref[(place_ref[2] + step) % lines]
 
 
-def input_grad_kernel(place_ref, first_ref, second_ref, *refs):
-    columns, tokens, _ = first_ref.shape
+def input_grad_kernel(place_ref, *refs):
     weight_ref = refs[-1]
+    columns, lines = weight_ref.shape[:2]
+    own_ref, flip_ref, far_ref = refs[:3]
+    blocks, refs = [own_ref, flip_ref, far_ref.at[0], far_ref.at[1]], refs[3:]
+    tokens = own_ref.shape[1]
     mine_ref, away_ref = refs[-3:-1]
-    lines, w_cols = weight_ref.shape[1:3]
+    w_cols = weight_ref.shape[2]
     for step, piece_ref in enumerate(refs[:-3]):
         for column in range(columns):
             weight_ref[column, (place_ref[2] + lines - step) % lines] = piece_ref[
@@ -242,11 +259,10 @@
         cols = slice(base, base + width)
         first = jnp.zeros((tokens, width), jnp.float32)
         second = jnp.zeros((tokens, width), jnp.float32)
-        for step in range(columns):
-            weight = weight_ref[(place_ref[1] + step) % columns, :, :, cols]
-            weight = weight.reshape(LANES, width)
-            first = first + dot_nn(first_ref[step], weight)
-            second = second + dot_nn(second_ref[step], weight)
+        for block, column in zip(blocks, pair_steps(place_ref[1])):
+            weight = weight_ref[column, :, :, cols].reshape(LANES, width)
+            first = first + dot_nn(block[0], weight)
+            second = second + dot_nn(block[1], weight)
         mine_ref[:, cols] = first
         away_ref[:, cols] = second.astype(jnp.bfloat16)
 
@@ -276,6 +292,10 @@
     return lax.ppermute(x, axis, [(place, (place + step) % count) for place in range(count)])
 
 
+def paired(x, step):
+    return lax.ppermute(x, "x", [(place, pair_steps(place)[step]) for place in range(4)])
+
+
 def from_all(x, axis):
     return [x] + [shifted(x, axis, step) for step in range(1, lax.axis_size(axis))]
 
@@ -290,7 +310,7 @@
 
 def shards(inputs, query_vectors, key_vectors, value_vectors, cotangent, gate_prefix, value_weight):
     planes = lax.axis_size("sp")
-    columns, lines = lax.axis_size("x"), lax.axis_size("y")
+    cores, columns, lines = lax.axis_size("core"), lax.axis_size("x"), lax.axis_size("y")
     core = lax.axis_index("core")
     tokens, model = inputs.shape[1:]
     width = query_vectors.shape[2]
@@ -309,7 +329,7 @@
     )
     arrived = exchanged(packed, "sp")
     own_rows = pl.pallas_call(stack_kernel, out_shape=shaped(columns, tokens, model))(
-        inputs[0], *map(near, from_all(inputs[0], "x")[1:])
+        inputs[0], *[near(paired(inputs[0], step)) for step in range(1, columns)]
     )
     other_rows = shifted(own_rows, "core", 1)
     weight_line = pl.pallas_call(
@@ -319,16 +339,16 @@
     )(place, weight_block, *map(near, from_all(weight_block, "x")[1:]))
     weight_line = weight_line.reshape(columns * w_cols, model)
     weight_pieces = from_all(weight_line, "y")
-    kept = (tokens // 2 + 7) // 8 * 8
+    kept = (tokens // (2 * cores) + 7) // 8 * 8
     sequence = near(arrived.reshape(length, 2 * LANES))
     wide, tile = pltpu.VMEM((length, LANES), jnp.float32), pltpu.VMEM((length, TILE), jnp.float32)
     row = shaped(1, length, dtype=jnp.float32)
     value_grad, peak, share = pl.pallas_call(
         value_kernel,
-        out_shape=(shaped(planes, kept, LANES), row, row),
+        out_shape=(shaped(planes, cores, kept, LANES), row, row),
         scratch_shapes=[pltpu.VMEM((length, LANES), jnp.bfloat16), wide, wide, tile],
     )(sequence, gate_prefix[0])
-    value_back = exchanged(value_grad, "sp")
+    value_back = exchanged(value_grad.reshape(planes * cores, kept, LANES), ("sp", "core"))
     pair_grad = pl.pallas_call(
         pair_kernel,
         out_shape=shaped(length, LANES),
@@ -342,20 +362,21 @@
         ],
     )(sequence, gate_prefix[0], peak, share)
     pair_back = exchanged(pair_grad.reshape(planes, tokens, LANES), "sp")
-    block = shaped(columns, tokens, LANES)
-    mine, away = pl.pallas_call(
-        unpack_value_kernel, out_shape=(block, block), in_specs=[small, whole]
+    block = shaped(cores, tokens, LANES)
+    blocks = pl.pallas_call(
+        unpack_value_kernel,
+        out_shape=(block, block, shaped(2, cores, tokens, LANES)),
+        in_specs=[small, whole],
     )(place, near(value_back))
-    brought = shifted(away, "core", 1)
-    both = jnp.stack([mine, brought], axis=1)
-    pieces = [both[0]] + [shifted(both[step], "x", step) for step in range(1, columns)]
+    first = paired(blocks[2], 2)
+    second = paired(jnp.stack([blocks[1], first[1]]), 1)
     partial = pl.pallas_call(
         product_kernel,
         compiler_params=pltpu.CompilerParams(vmem_limit_bytes=VMEM_BYTES),
         out_shape=(shaped(w_cols, model),) * lines,
-        in_specs=[small] + [whole] * (2 + columns),
+        in_specs=[small] + [whole] * 5,
         scratch_shapes=[pltpu.VMEM((lines, w_cols, model), jnp.bfloat16)],
-    )(place, near(own_rows), near(other_rows), *map(near, pieces))
+    )(place, near(own_rows), near(other_rows), blocks[0], near(first), near(second))
     partial = [partial[0]] + [shifted(partial[step], "y", step) for step in range(1, lines)]
     partial = sum(part.astype(jnp.float32) for part in partial).astype(jnp.bfloat16)
     partial = jnp.moveaxis(partial.reshape(w_cols, planes, model // planes), 1, 0)
@@ -367,9 +388,9 @@
     kept_part, sent_part = pl.pallas_call(
         input_grad_kernel,
         out_shape=(shaped(tokens, model, dtype=jnp.float32), shaped(tokens, model)),
-        in_specs=[small] + [whole] * (2 + lines),
+        in_specs=[small] + [whole] * (3 + lines),
         scratch_shapes=[pltpu.VMEM((columns, lines, w_cols, model), jnp.bfloat16)],
-    )(place, mine, near(brought), *weight_pieces)
+    )(place, *blocks, *weight_pieces)
     input_grad = pl.pallas_call(add_kernel, out_shape=shaped(tokens, model))(
         kept_part, near(shifted(sent_part, "core", 1))
     )

time: 245 us -> 249 us (1.016)
  the two profiles are of different devices: /device:TPU:9 before, /device:TPU:56 now
where the time goes in v5:
time: 249 us; the launch traced here: 248 us
  starting transfers between devices  84.6 us (34%)
  blocking collectives  72.2 us (29%)
  waiting for transfers between devices  49 us (20%)
  Pallas kernels  36.6 us (15%)
  other arithmetic  2.87 us (1%)
    all_to_all x1, blocking collectives, exchanged(): return lax.all_to_all(x, axis, split_axis=0, concat_axis=0, tiled=True)  72.2 us
    ppermute x11, starting transfers between devices, shifted(): lax.ppermute(x, axis, [(place, (place + step) % count) for place in range...  34.5 us
    all_to_all x4, starting transfers between devices, exchanged(): return lax.all_to_all(x, axis, split_axis=0, concat_axis=0, tiled=True)  34.4 us
    ppermute x5, waiting for transfers between devices, paired(): lax.ppermute(x, 'x', [(place, pair_steps(place)[step]) for place in range...  27.5 us
    all_to_all x4, waiting for transfers between devices, exchanged(): return lax.all_to_all(x, axis, split_axis=0, concat_axis=0, tiled=True)  17.2 us
    ppermute x5, starting transfers between devices, paired(): lax.ppermute(x, 'x', [(place, pair_steps(place)[step]) for place in range...  15.7 us
    pallas_call x1, Pallas kernels, shards(): pl.pallas_call(pair_kernel, out_shape=shaped(length, LANES), scratch_shap...  9.11 us
    pallas_call x1, Pallas kernels, shards(): pl.pallas_call(value_kernel, out_shape=(shaped(planes, cores, kept, LANES...  7.89 us
  transfers between devices with their start and end apart: 20, of which 8 were waited for; matrix products, arithmetic and copies ran while one was open for 1% of the time, Pallas kernels for 14%

profile of v5, /device:TPU:56, one launch (start us, length us, event | category | flops | bytes accessed | tf_op | source)
XLA Modules:
  0.0 247.7 jit_solution(8836536933960131417)
XLA Ops:
  0.6 2.7 %shard_map.102 = bf16[16,136,256]{2,1,0:T(8,128)(2,1)} custom-call(bf16[136,1024]{1,0:T(8,128)(2,1)} %bitcast.35, bf16[136,1024]{1,0:T(8,128)(2,1)} %bitcast.36, bf16[136,1024]{1,0:T(8,128)(2,1)} %bitcast.37, bf16[136,1024]{1,0:T(8,128)(2,1)} %bitcast.38), custom_call_target="tpu_custom_call" | custom-call | tf_op jit(solution)/shard_map/pallas_call | solution.py:327
  3.3 72.2 %all_to_all.25 = bf16[16,136,256]{2,1,0:T(8,128)(2,1)S(1)} all-to-all(bf16[16,136,256]{2,1,0:T(8,128)(2,1)} %shard_map.102), channel_id=1, replica_groups=mesh['sp'=16,'y'=4,'x'=4,'core'=2] {'sp'}, dimensions={0} | all-to-all | bytes 2228224 | tf_op jit(solution)/shard_map/all_to_all | solution.py:287
  76.2 4.0 %all-to-all-start.3 = ((bf16[16,32,128]{2,1,0:T(8,128)(2,1)}), bf16[16,32,128]{2,1,0:T(8,128)(2,1)S(1)}, u32[]{:S(2)}, u32[]{:S(2)}) async-start(bf16[16,32,128]{2,1,0:T(8,128)(2,1)} %broadcast_in_dim.14), calls=%async_computation.3 | async-start | bytes 262144 | tf_op jit(solution)/shard_map/all_to_all | solution.py:287
  80.1 7.9 %shard_map.103 = (bf16[16,2,40,128]{3,2,1,0:T(8,128)(2,1)}, f32[1,2176]{1,0:T(1,128)}, f32[1,2176]{1,0:T(1,128)}) custom-call(bf16[2176,256]{1,0:T(8,128)(2,1)S(1)} %bitcast.26, f32[1,2176]{1,0:T(1,128)} %bitcast.40), custom_call_target="tpu_custom_call" | custom-call | tf_op jit(solution)/shard_map/pallas_call | solution.py:346
  88.0 5.9 %all-to-all-done.3.x_ref = bf16[16,32,128]{2,1,0:T(8,128)(2,1)S(1)} async-done(((bf16[16,32,128]{2,1,0:T(8,128)(2,1)}), bf16[16,32,128]{2,1,0:T(8,128)(2,1)S(1)}, u32[]{:S(2)}, u32[]{:S(2)}) %all-to-all-start.3) | async-done | bytes 131104 | tf_op jit(solution)/shard_map/all_to_all | solution.py:287
  94.0 6.3 %all-to-all-start.2 = ((bf16[32,40,128]{2,1,0:T(8,128)(2,1)}), bf16[32,40,128]{2,1,0:T(8,128)(2,1)S(1)}, u32[]{:S(2)}, u32[]{:S(2)}) async-start(bf16[32,40,128]{2,1,0:T(8,128)(2,1)} %bitcast.34), calls=%async_computation.2 | async-start | bytes 655360 | tf_op jit(solution)/shard_map/all_to_all | solution.py:287
  100.3 4.7 %collective-permute-start.7 = (bf16[136,2048]{1,0:T(8,128)(2,1)}, bf16[136,2048]{1,0:T(8,128)(2,1)S(1)}, u32[]{:S(2)}, u32[]{:S(2)}) collective-permute-start(bf16[136,2048]{1,0:T(8,128)(2,1)} %bitcast.16.refs_0_), channel_id=1, source_target_pairs={{0,6},{2,4},{4,2},{6,0},{1,7},{3,5},{5,3},{7,1},{8,14},{10,12},{12... | collective-permute-start | bytes 1671176 | tf_op jit(solution)/shard_map/ppermute | solution.py:296
  107.1 3.6 %collective-permute-start.9 = (bf16[136,2048]{1,0:T(8,128)(2,1)}, bf16[136,2048]{1,0:T(8,128)(2,1)S(1)}, u32[]{:S(2)}, u32[]{:S(2)}) collective-permute-start(bf16[136,2048]{1,0:T(8,128)(2,1)} %bitcast.16.refs_0_), channel_id=1, source_target_pairs={{0,4},{2,6},{4,0},{6,2},{1,5},{3,7},{5,1},{7,3},{8,12},{10,14},{12... | collective-permute-start | bytes 1671176 | tf_op jit(solution)/shard_map/ppermute | solution.py:296
  110.7 7.5 %collective-permute-done.7.refs_1_ = bf16[136,2048]{1,0:T(8,128)(2,1)S(1)} collective-permute-done((bf16[136,2048]{1,0:T(8,128)(2,1)}, bf16[136,2048]{1,0:T(8,128)(2,1)S(1)}, u32[]{:S(2)}, u32[]{:S(2)}) %collective-permute-start.7) | collective-permute-done | bytes 557088 | tf_op jit(solution)/shard_map/ppermute | solution.py:296
  118.2 4.3 %collective-permute-done.8.refs_2_ = bf16[136,2048]{1,0:T(8,128)(2,1)S(1)} collective-permute-done((bf16[136,2048]{1,0:T(8,128)(2,1)}, bf16[136,2048]{1,0:T(8,128)(2,1)S(1)}, u32[]{:S(2)}, u32[]{:S(2)}) %collective-permute-start.8) | collective-permute-done | bytes 557088 | tf_op jit(solution)/shard_map/ppermute | solution.py:296
  122.6 10.7 %collective-permute-done.9.refs_3_ = bf16[136,2048]{1,0:T(8,128)(2,1)S(1)} collective-permute-done((bf16[136,2048]{1,0:T(8,128)(2,1)}, bf16[136,2048]{1,0:T(8,128)(2,1)S(1)}, u32[]{:S(2)}, u32[]{:S(2)}) %collective-permute-start.9) | collective-permute-done | bytes 557088 | tf_op jit(solution)/shard_map/ppermute | solution.py:296
  138.0 9.1 %shard_map.104 = bf16[2176,128]{1,0:T(8,128)(2,1)} custom-call(bf16[2176,256]{1,0:T(8,128)(2,1)S(1)} %bitcast.27, f32[1,2176]{1,0:T(1,128)} %bitcast.41, f32[1,2176]{1,0:T(1,128)} %get-tuple-element.18.peak_ref, f32[1,2176]{1,0:T(1,128)} %get-tuple-element.19.share_ref), custom_call_target="tpu_custom_call" | custom-call | tf_op jit(solution)/shard_map/pallas_call | solution.py:352
  147.1 12.2 %all-to-all-start.1 = ((bf16[16,136,128]{2,1,0:T(8,128)(2,1)}), bf16[16,136,128]{2,1,0:T(8,128)(2,1)S(1)}, u32[]{:S(2)}, u32[]{:S(2)}) async-start(bf16[16,136,128]{2,1,0:T(8,128)(2,1)} %bitcast.28), calls=%async_computation.1 | async-start | bytes 1114112 | tf_op jit(solution)/shard_map/all_to_all | solution.py:287
  162.1 5.9 %collective-permute-start.1 = (bf16[32,2048]{1,0:T(8,128)(2,1)}, bf16[32,2048]{1,0:T(8,128)(2,1)S(1)}, u32[]{:S(2)}, u32[]{:S(2)}) collective-permute-start(bf16[32,2048]{1,0:T(8,128)(2,1)} %shard_map.107.refs_0_), channel_id=1, source_target_pairs={{0,4},{2,6},{4,0},{6,2},{1,5},{3,7},{5,1},{7,3},{8,12},{10,14},{12... | collective-permute-start | bytes 393224 | tf_op jit(solution)/shard_map/ppermute | solution.py:292
  182.7 4.5 %collective-permute-start.4 = (bf16[128,2048]{1,0:T(8,128)(2,1)}, bf16[128,2048]{1,0:T(8,128)(2,1)}, u32[]{:S(2)}, u32[]{:S(2)}) collective-permute-start(bf16[128,2048]{1,0:T(8,128)(2,1)} %bitcast.30), channel_id=1, source_target_pairs={{0,16},{8,24},{16,0},{24,8},{1,17},{9,25},{17,1},{25,9},{2,18},{10... | collective-permute-start | bytes 1572872 | tf_op jit(solution)/shard_map/ppermute | solution.py:292
  190.0 3.2 %collective-permute-start.12 = (bf16[2,2,136,128]{3,2,1,0:T(8,128)(2,1)S(1)}, bf16[2,2,136,128]{3,2,1,0:T(8,128)(2,1)S(1)}, u32[]{:S(2)}, u32[]{:S(2)}) collective-permute-start(bf16[2,2,136,128]{3,2,1,0:T(8,128)(2,1)S(1)} %pad_maximum_fusion), channel_id=1, source_target_pairs={{0,6},{2,4},{4,2},{6,0},{1,7},{3,5},{5,3},{7,1},{8,14},{10,12},{12... | collective-permute-start | bytes 417800 | tf_op jit(solution)/shard_map/ppermute | solution.py:296
  193.3 4.9 %collective-permute-done.12.second_ref = bf16[2,2,136,128]{3,2,1,0:T(8,128)(2,1)S(1)} collective-permute-done((bf16[2,2,136,128]{3,2,1,0:T(8,128)(2,1)S(1)}, bf16[2,2,136,128]{3,2,1,0:T(8,128)(2,1)S(1)}, u32[]{:S(2)}, u32[]{:S(2)}) %collective-permute-start.12) | collective-permute-done | bytes 139296 | tf_op jit(solution)/shard_map/ppermute | solution.py:296
  199.1 2.7 %shard_map.112 = (bf16[32,2048]{1,0:T(8,128)(2,1)S(1)}, bf16[32,2048]{1,0:T(8,128)(2,1)S(1)}, bf16[32,2048]{1,0:T(8,128)(2,1)S(1)}, bf16[32,2048]{1,0:T(8,128)(2,1)S(1)}) custom-call(s32[3]{0:T(128)S(1)} %copy-done.4, bf16[4,136,2048]{2,1,0:T(8,128)(2,1)S(1)} %copy-done, bf16[4,136,2048]{2,1,0:T(8,128)(2,1)} %collective-permute-done.10.other_ref, ...), custom_call_target="tpu_custom_call" | custom-call | tf_op jit(solution)/shard_map/pallas_call | solution.py:373
  201.8 2.8 %collective-permute-start.15 = (bf16[32,2048]{1,0:T(8,128)(2,1)S(1)}, bf16[32,2048]{1,0:T(8,128)(2,1)S(1)}, u32[]{:S(2)}, u32[]{:S(2)}) collective-permute-start(bf16[32,2048]{1,0:T(8,128)(2,1)S(1)} %get-tuple-element.31), channel_id=1, source_target_pairs={{0,24},{8,0},{16,8},{24,16},{1,25},{9,1},{17,9},{25,17},{2,26},{10... | collective-permute-start | bytes 393224 | tf_op jit(solution)/shard_map/ppermute | solution.py:292
  204.6 5.7 %collective-permute-start.14 = (bf16[32,2048]{1,0:T(8,128)(2,1)S(1)}, bf16[32,2048]{1,0:T(8,128)(2,1)S(1)}, u32[]{:S(2)}, u32[]{:S(2)}) collective-permute-start(bf16[32,2048]{1,0:T(8,128)(2,1)S(1)} %get-tuple-element.30), channel_id=1, source_target_pairs={{0,16},{8,24},{16,0},{24,8},{1,17},{9,25},{17,1},{25,9},{2,18},{10... | collective-permute-start | bytes 393224 | tf_op jit(solution)/shard_map/ppermute | solution.py:292
  210.3 3.2 %collective-permute-start.13 = (bf16[32,2048]{1,0:T(8,128)(2,1)S(1)}, bf16[32,2048]{1,0:T(8,128)(2,1)S(1)}, u32[]{:S(2)}, u32[]{:S(2)}) collective-permute-start(bf16[32,2048]{1,0:T(8,128)(2,1)S(1)} %get-tuple-element.29), channel_id=1, source_target_pairs={{0,8},{8,16},{16,24},{24,0},{1,9},{9,17},{17,25},{25,1},{2,10},{10... | collective-permute-start | bytes 393224 | tf_op jit(solution)/shard_map/ppermute | solution.py:292
  213.5 4.3 %shard_map.109 = (f32[136,2048]{1,0:T(8,128)}, bf16[136,2048]{1,0:T(8,128)(2,1)}) custom-call(s32[3]{0:T(128)} %pad_add_fusion.place_ref, bf16[2,136,128]{2,1,0:T(8,128)(2,1)} %get-tuple-element.23.refs_0_.here_ref, bf16[2,136,128]{2,1,0:T(8,128)(2,1)} %get-tuple-element.24.refs_1_, bf16[2,2,136,128]{3,2,1,0:T(8,128)(2,1)} %get-tuple-element.25.refs_2_, ...), custom_call_target="tpu_custom_call" | custom-call | tf_op jit(solution)/shard_map/pallas_call | solution.py:388
  220.5 12.0 %all-to-all-start.4 = ((bf16[16,32,128]{2,1,0:T(8,128)(2,1)}), bf16[16,32,128]{2,1,0:T(8,128)(2,1)S(1)}, u32[]{:S(2)}, u32[]{:S(2)}) async-start(bf16[16,32,128]{2,1,0:T(8,128)(2,1)} %bitcast_bitcast_fusion), calls=%async_computation.4 | async-start | bytes 262144 | tf_op jit(solution)/shard_map/all_to_all | solution.py:287
  235.8 11.3 %all-to-all-done.4 = bf16[16,32,128]{2,1,0:T(8,128)(2,1)S(1)} async-done(((bf16[16,32,128]{2,1,0:T(8,128)(2,1)}), bf16[16,32,128]{2,1,0:T(8,128)(2,1)S(1)}, u32[]{:S(2)}, u32[]{:S(2)}) %all-to-all-start.4) | async-done | bytes 131104 | tf_op jit(solution)/shard_map/all_to_all | solution.py:287
  (46 shorter events, 35.1 us)
Async XLA Ops:
  3.3 72.2 %copy-start.5 = (bf16[128,32]{0,1:T(8,128)(2,1)S(1)}, bf16[128,32]{0,1:T(8,128)(2,1)}, u32[]{:S(2)}) copy-start(bf16[128,32]{0,1:T(8,128)(2,1)} %param.13) | copy-start | bytes 24580
  76.2 17.8 %all-to-all-start.3 = ((bf16[16,32,128]{2,1,0:T(8,128)(2,1)}), bf16[16,32,128]{2,1,0:T(8,128)(2,1)S(1)}, u32[]{:S(2)}, u32[]{:S(2)}) async-start(bf16[16,32,128]{2,1,0:T(8,128)(2,1)} %broadcast_in_dim.14), calls=%async_computation.3 | async-start | bytes 262144 | tf_op jit(solution)/shard_map/all_to_all | solution.py:287
  94.0 53.1 %all-to-all-start.2 = ((bf16[32,40,128]{2,1,0:T(8,128)(2,1)}), bf16[32,40,128]{2,1,0:T(8,128)(2,1)S(1)}, u32[]{:S(2)}, u32[]{:S(2)}) async-start(bf16[32,40,128]{2,1,0:T(8,128)(2,1)} %bitcast.34), calls=%async_computation.2 | async-start | bytes 655360 | tf_op jit(solution)/shard_map/all_to_all | solution.py:287
  100.3 18.0 %collective-permute-start.7 = (bf16[136,2048]{1,0:T(8,128)(2,1)}, bf16[136,2048]{1,0:T(8,128)(2,1)S(1)}, u32[]{:S(2)}, u32[]{:S(2)}) collective-permute-start(bf16[136,2048]{1,0:T(8,128)(2,1)} %bitcast.16.refs_0_), channel_id=1, source_target_pairs={{0,6},{2,4},{4,2},{6,0},{1,7},{3,5},{5,3},{7,1},{8,14},{10,12},{12... | collective-permute-start | bytes 1671176 | tf_op jit(solution)/shard_map/ppermute | solution.py:296
  105.0 17.6 %collective-permute-start.8 = (bf16[136,2048]{1,0:T(8,128)(2,1)}, bf16[136,2048]{1,0:T(8,128)(2,1)S(1)}, u32[]{:S(2)}, u32[]{:S(2)}) collective-permute-start(bf16[136,2048]{1,0:T(8,128)(2,1)} %bitcast.16.refs_0_), channel_id=1, source_target_pairs={{0,2},{2,0},{4,6},{6,4},{1,3},{3,1},{5,7},{7,5},{8,10},{10,8},{12,... | collective-permute-start | bytes 1671176 | tf_op jit(solution)/shard_map/ppermute | solution.py:296
  107.1 26.2 %collective-permute-start.9 = (bf16[136,2048]{1,0:T(8,128)(2,1)}, bf16[136,2048]{1,0:T(8,128)(2,1)S(1)}, u32[]{:S(2)}, u32[]{:S(2)}) collective-permute-start(bf16[136,2048]{1,0:T(8,128)(2,1)} %bitcast.16.refs_0_), channel_id=1, source_target_pairs={{0,4},{2,6},{4,0},{6,2},{1,5},{3,7},{5,1},{7,3},{8,12},{10,14},{12... | collective-permute-start | bytes 1671176 | tf_op jit(solution)/shard_map/ppermute | solution.py:296
  135.9 57.4 %collective-permute-start.10 = (bf16[4,136,2048]{2,1,0:T(8,128)(2,1)}, bf16[4,136,2048]{2,1,0:T(8,128)(2,1)}, u32[]{:S(2)}, u32[]{:S(2)}) collective-permute-start(bf16[4,136,2048]{2,1,0:T(8,128)(2,1)} %shard_map.111.own_ref), channel_id=1, source_target_pairs={{0,1},{1,0},{2,3},{3,2},{4,5},{5,4},{6,7},{7,6},{8,9},{9,8},{10,11... | collective-permute-start | bytes 6684680 | tf_op jit(solution)/shard_map/ppermute | solution.py:292
  147.1 12.2 %copy-start.2 = (bf16[16,32,128]{2,1,0:T(8,128)(2,1)S(1)}, bf16[16,32,128]{2,1,0:T(8,128)(2,1)}, u32[]{:S(2)}) copy-start(bf16[16,32,128]{2,1,0:T(8,128)(2,1)} %copy-done.1) | copy-start | bytes 393220
  147.1 51.1 %copy-start = (bf16[4,136,2048]{2,1,0:T(8,128)(2,1)S(1)}, bf16[4,136,2048]{2,1,0:T(8,128)(2,1)}, u32[]{:S(2)}) copy-start(bf16[4,136,2048]{2,1,0:T(8,128)(2,1)} %shard_map.111.own_ref) | copy-start | bytes 6684676
  147.1 73.4 %all-to-all-start.1 = ((bf16[16,136,128]{2,1,0:T(8,128)(2,1)}), bf16[16,136,128]{2,1,0:T(8,128)(2,1)S(1)}, u32[]{:S(2)}, u32[]{:S(2)}) async-start(bf16[16,136,128]{2,1,0:T(8,128)(2,1)} %bitcast.28), calls=%async_computation.1 | async-start | bytes 1114112 | tf_op jit(solution)/shard_map/all_to_all | solution.py:287
  160.0 10.9 %collective-permute-start = (bf16[32,2048]{1,0:T(8,128)(2,1)}, bf16[32,2048]{1,0:T(8,128)(2,1)S(1)}, u32[]{:S(2)}, u32[]{:S(2)}) collective-permute-start(bf16[32,2048]{1,0:T(8,128)(2,1)} %shard_map.107.refs_0_), channel_id=1, source_target_pairs={{0,2},{2,4},{4,6},{6,0},{1,3},{3,5},{5,7},{7,1},{8,10},{10,12},{12... | collective-permute-start | bytes 393224 | tf_op jit(solution)/shard_map/ppermute | solution.py:292
  162.1 10.3 %collective-permute-start.1 = (bf16[32,2048]{1,0:T(8,128)(2,1)}, bf16[32,2048]{1,0:T(8,128)(2,1)S(1)}, u32[]{:S(2)}, u32[]{:S(2)}) collective-permute-start(bf16[32,2048]{1,0:T(8,128)(2,1)} %shard_map.107.refs_0_), channel_id=1, source_target_pairs={{0,4},{2,6},{4,0},{6,2},{1,5},{3,7},{5,1},{7,3},{8,12},{10,14},{12... | collective-permute-start | bytes 393224 | tf_op jit(solution)/shard_map/ppermute | solution.py:292
  168.0 7.1 %collective-permute-start.2 = (bf16[32,2048]{1,0:T(8,128)(2,1)}, bf16[32,2048]{1,0:T(8,128)(2,1)S(1)}, u32[]{:S(2)}, u32[]{:S(2)}) collective-permute-start(bf16[32,2048]{1,0:T(8,128)(2,1)} %shard_map.107.refs_0_), channel_id=1, source_target_pairs={{0,6},{2,0},{4,2},{6,4},{1,7},{3,1},{5,3},{7,5},{8,14},{10,8},{12,... | collective-permute-start | bytes 393224 | tf_op jit(solution)/shard_map/ppermute | solution.py:292
  170.8 27.4 %copy-start.4 = (s32[3]{0:T(128)S(1)}, s32[3]{0:T(128)}, u32[]{:S(2)}) copy-start(s32[3]{0:T(128)} %pad_add_fusion.place_ref) | copy-start | bytes 40
  176.8 33.5 %collective-permute-start.3 = (bf16[128,2048]{1,0:T(8,128)(2,1)}, bf16[128,2048]{1,0:T(8,128)(2,1)}, u32[]{:S(2)}, u32[]{:S(2)}) collective-permute-start(bf16[128,2048]{1,0:T(8,128)(2,1)} %bitcast.29), channel_id=1, source_target_pairs={{0,8},{8,16},{16,24},{24,0},{1,9},{9,17},{17,25},{25,1},{2,10},{10... | collective-permute-start | bytes 1572872 | tf_op jit(solution)/shard_map/ppermute | solution.py:292
  180.6 8.5 %collective-permute-start.11 = (bf16[2,2,136,128]{3,2,1,0:T(8,128)(2,1)}, bf16[2,2,136,128]{3,2,1,0:T(8,128)(2,1)S(1)}, u32[]{:S(2)}, u32[]{:S(2)}) collective-permute-start(bf16[2,2,136,128]{3,2,1,0:T(8,128)(2,1)} %get-tuple-element.25.refs_2_), channel_id=1, source_target_pairs={{0,2},{2,0},{4,6},{6,4},{1,3},{3,1},{5,7},{7,5},{8,10},{10,8},{12,... | collective-permute-start | bytes 417800 | tf_op jit(solution)/shard_map/ppermute | solution.py:296
  182.7 30.8 %collective-permute-start.4 = (bf16[128,2048]{1,0:T(8,128)(2,1)}, bf16[128,2048]{1,0:T(8,128)(2,1)}, u32[]{:S(2)}, u32[]{:S(2)}) collective-permute-start(bf16[128,2048]{1,0:T(8,128)(2,1)} %bitcast.30), channel_id=1, source_target_pairs={{0,16},{8,24},{16,0},{24,8},{1,17},{9,25},{17,1},{25,9},{2,18},{10... | collective-permute-start | bytes 1572872 | tf_op jit(solution)/shard_map/ppermute | solution.py:292
  187.2 26.3 %collective-permute-start.5 = (bf16[128,2048]{1,0:T(8,128)(2,1)}, bf16[128,2048]{1,0:T(8,128)(2,1)}, u32[]{:S(2)}, u32[]{:S(2)}) collective-permute-start(bf16[128,2048]{1,0:T(8,128)(2,1)} %bitcast.31), channel_id=1, source_target_pairs={{0,24},{8,0},{16,8},{24,16},{1,25},{9,1},{17,9},{25,17},{2,26},{10... | collective-permute-start | bytes 1572872 | tf_op jit(solution)/shard_map/ppermute | solution.py:292
  190.0 8.2 %collective-permute-start.12 = (bf16[2,2,136,128]{3,2,1,0:T(8,128)(2,1)S(1)}, bf16[2,2,136,128]{3,2,1,0:T(8,128)(2,1)S(1)}, u32[]{:S(2)}, u32[]{:S(2)}) collective-permute-start(bf16[2,2,136,128]{3,2,1,0:T(8,128)(2,1)S(1)} %pad_maximum_fusion), channel_id=1, source_target_pairs={{0,6},{2,4},{4,2},{6,0},{1,7},{3,5},{5,3},{7,1},{8,14},{10,12},{12... | collective-permute-start | bytes 417800 | tf_op jit(solution)/shard_map/ppermute | solution.py:296
  201.8 18.0 %collective-permute-start.15 = (bf16[32,2048]{1,0:T(8,128)(2,1)S(1)}, bf16[32,2048]{1,0:T(8,128)(2,1)S(1)}, u32[]{:S(2)}, u32[]{:S(2)}) collective-permute-start(bf16[32,2048]{1,0:T(8,128)(2,1)S(1)} %get-tuple-element.31), channel_id=1, source_target_pairs={{0,24},{8,0},{16,8},{24,16},{1,25},{9,1},{17,9},{25,17},{2,26},{10... | collective-permute-start | bytes 393224 | tf_op jit(solution)/shard_map/ppermute | solution.py:292
  204.6 15.2 %collective-permute-start.14 = (bf16[32,2048]{1,0:T(8,128)(2,1)S(1)}, bf16[32,2048]{1,0:T(8,128)(2,1)S(1)}, u32[]{:S(2)}, u32[]{:S(2)}) collective-permute-start(bf16[32,2048]{1,0:T(8,128)(2,1)S(1)} %get-tuple-element.30), channel_id=1, source_target_pairs={{0,16},{8,24},{16,0},{24,8},{1,17},{9,25},{17,1},{25,9},{2,18},{10... | collective-permute-start | bytes 393224 | tf_op jit(solution)/shard_map/ppermute | solution.py:292
  210.3 9.5 %collective-permute-start.13 = (bf16[32,2048]{1,0:T(8,128)(2,1)S(1)}, bf16[32,2048]{1,0:T(8,128)(2,1)S(1)}, u32[]{:S(2)}, u32[]{:S(2)}) collective-permute-start(bf16[32,2048]{1,0:T(8,128)(2,1)S(1)} %get-tuple-element.29), channel_id=1, source_target_pairs={{0,8},{8,16},{16,24},{24,0},{1,9},{9,17},{17,25},{25,1},{2,10},{10... | collective-permute-start | bytes 393224 | tf_op jit(solution)/shard_map/ppermute | solution.py:292
  217.9 14.7 %collective-permute-start.6 = (bf16[136,2048]{1,0:T(8,128)(2,1)}, bf16[136,2048]{1,0:T(8,128)(2,1)S(1)}, u32[]{:S(2)}, u32[]{:S(2)}) collective-permute-start(bf16[136,2048]{1,0:T(8,128)(2,1)} %get-tuple-element.27), channel_id=1, source_target_pairs={{0,1},{1,0},{2,3},{3,2},{4,5},{5,4},{6,7},{7,6},{8,9},{9,8},{10,11... | collective-permute-start | bytes 1671176 | tf_op jit(solution)/shard_map/ppermute | solution.py:292
  220.5 26.5 %all-to-all-start.4 = ((bf16[16,32,128]{2,1,0:T(8,128)(2,1)}), bf16[16,32,128]{2,1,0:T(8,128)(2,1)S(1)}, u32[]{:S(2)}, u32[]{:S(2)}) async-start(bf16[16,32,128]{2,1,0:T(8,128)(2,1)} %bitcast_bitcast_fusion), calls=%async_computation.4 | async-start | bytes 262144 | tf_op jit(solution)/shard_map/all_to_all | solution.py:287
  (2 other events, 7.2 us)

commit v6 on v4

--- a/solution.py
+++ b/solution.py
@@ -20,20 +20,25 @@
     return lax.broadcasted_iota(jnp.int32, shape, 1) < HEAD_DIM
 
 
-def pack_kernel(q_ref, k_ref, v_ref, g_ref, out_ref):
-    heads, tokens, _ = out_ref.shape
+def pack_kernel(q_ref, k_ref, v_ref, g_ref, w_ref, first_ref, second_ref):
+    heads, tokens, _ = second_ref.shape
     low = low_lanes((tokens, LANES))
     for pair in range(heads // 2):
         cols = slice(pair * LANES, (pair + 1) * LANES)
-        for first_ref, second_ref, lane in ((q_ref, k_ref, 0), (v_ref, g_ref, LANES)):
-            first = first_ref[:, cols].astype(jnp.float32)
-            second = second_ref[:, cols].astype(jnp.float32)
-            out_ref[2 * pair, :, lane : lane + LANES] = jnp.where(
-                low, first, rolled(second)
-            ).astype(jnp.bfloat16)
-            out_ref[2 * pair + 1, :, lane : lane + LANES] = jnp.where(
-                low, rolled(first), second
-            ).astype(jnp.bfloat16)
+        for one_ref, two_ref, out_ref in ((q_ref, k_ref, first_ref), (v_ref, g_ref, second_ref)):
+            one = one_ref[:, cols].astype(jnp.float32)
+            two = two_ref[:, cols].astype(jnp.float32)
+            out_ref[2 * pair, :tokens] = jnp.where(low, one, rolled(two)).astype(jnp.bfloat16)
+            out_ref[2 * pair + 1, :tokens] = jnp.where(low, rolled(one), two).astype(jnp.bfloat16)
+    for head in range(heads):
+        first_ref[head, tokens:] = w_ref[...]
+
+
+def open_kernel(x_ref, qk_ref, weight_ref):
+    planes, tokens, _ = qk_ref.shape
+    for plane in range(planes):
+        qk_ref[plane] = x_ref[plane, :tokens]
+        weight_ref[:, plane * LANES : (plane + 1) * LANES] = x_ref[plane, tokens:]
 
 
 def dot_nt(a, b):
@@ -52,25 +57,26 @@
     return [(base, min(TILE, length - base)) for base in range(0, length, TILE)]
 
 
-def spread(x_ref, p_ref, kq_ref, pc_ref, acc_ref, kt_ref=None):
+def spread(x_ref, p_ref, kq_ref, pc_ref, acc_ref=None, kt_ref=None):
     for base, rows in blocks_of(x_ref.shape[0]):
         here = slice(base, base + rows)
-        swapped = rolled(x_ref[here, :LANES].astype(jnp.float32))
+        swapped = rolled(x_ref[here].astype(jnp.float32))
         kq_ref[here] = swapped.astype(jnp.bfloat16)
         if kt_ref is not None:
             kt_ref[:, here] = swapped.T[:HEAD_DIM].astype(jnp.bfloat16)
         pc_ref[here] = jnp.broadcast_to(p_ref[:, here], (LANES, rows)).T
-        acc_ref[here] = jnp.zeros((rows, LANES), jnp.float32)
+        if acc_ref is not None:
+            acc_ref[here] = jnp.zeros((rows, LANES), jnp.float32)
 
 
 def query_block(x_ref, here, low):
-    wide = x_ref[here, :LANES].astype(jnp.float32)
+    wide = x_ref[here].astype(jnp.float32)
     scaled = jnp.where(low, wide * HEAD_DIM**-0.5, 0.0).astype(jnp.bfloat16)
     return scaled, jnp.where(low, 0.0, rolled(wide)).astype(jnp.bfloat16)
 
 
 def grad_block(x_ref, here, low):
-    wide = rolled(x_ref[here, LANES:].astype(jnp.float32))
+    wide = rolled(x_ref[here].astype(jnp.float32))
     return jnp.where(low, wide, 0.0).astype(jnp.bfloat16)
 
 
@@ -86,15 +92,12 @@
     return jnp.where(seen, scores, FLOOR)
 
 
-def value_kernel(x_ref, p_ref, v_out_ref, peak_ref, share_ref, kq_ref, pc_ref, acc_ref, s_ref):
-    length = x_ref.shape[0]
-    blocks = blocks_of(length)
-    spread(x_ref, p_ref, kq_ref, pc_ref, acc_ref)
+def stats_kernel(x_ref, p_ref, peak_ref, share_ref, kq_ref, pc_ref, s_ref):
+    blocks = blocks_of(x_ref.shape[0])
+    spread(x_ref, p_ref, kq_ref, pc_ref)
     for index, (q_base, q_rows) in enumerate(blocks):
         q_here = slice(q_base, q_base + q_rows)
-        low = low_lanes((q_rows, LANES))
-        query_low, _ = query_block(x_ref, q_here, low)
-        grad_low = grad_block(x_ref, q_here, low)
+        query_low, _ = query_block(x_ref, q_here, low_lanes((q_rows, LANES)))
         peak = jnp.full((8, q_rows), FLOOR, jnp.float32)
         for u_base, u_rows in blocks[: index + 1]:
             scores = score_tile(kq_ref, pc_ref, query_low, q_base, u_base, u_rows)
@@ -103,17 +106,27 @@
         peak = jnp.max(peak, axis=0, keepdims=True)
         total = jnp.zeros((8, q_rows), jnp.float32)
         for u_base, u_rows in blocks[: index + 1]:
-            u_here = slice(u_base, u_base + u_rows)
-            raised = jnp.exp(s_ref[u_here, :q_rows] - peak)
-            s_ref[u_here, :q_rows] = raised
+            raised = jnp.exp(s_ref[u_base : u_base + u_rows, :q_rows] - peak)
             total = total + folded(raised, jnp.sum)
-        share = 1.0 / jnp.sum(total, axis=0, keepdims=True)
         peak_ref[:, q_here] = peak
-        share_ref[:, q_here] = share
+        share_ref[:, q_here] = 1.0 / jnp.sum(total, axis=0, keepdims=True)
+
+
+def value_kernel(x_ref, y_ref, p_ref, peak_ref, share_ref, v_out_ref, kq_ref, pc_ref, acc_ref):
+    length = x_ref.shape[0]
+    blocks = blocks_of(length)
+    spread(x_ref, p_ref, kq_ref, pc_ref, acc_ref)
+    for index, (q_base, q_rows) in enumerate(blocks):
+        q_here = slice(q_base, q_base + q_rows)
+        low = low_lanes((q_rows, LANES))
+        query_low, _ = query_block(x_ref, q_here, low)
+        grad_low = grad_block(y_ref, q_here, low)
+        peak = peak_ref[:, q_here]
+        share = share_ref[:, q_here]
         for u_base, u_rows in blocks[: index + 1]:
-            u_here = slice(u_base, u_base + u_rows)
-            soft = s_ref[u_here, :q_rows] * share
-            acc_ref[u_here] += dot_nn(soft.astype(jnp.bfloat16), grad_low)
+            scores = score_tile(kq_ref, pc_ref, query_low, q_base, u_base, u_rows)
+            soft = (jnp.exp(scores - peak) * share).astype(jnp.bfloat16)
+            acc_ref[u_base : u_base + u_rows] += dot_nn(soft, grad_low)
     planes, kept, _ = v_out_ref.shape
     tokens = length // planes
     for plane in range(planes):
@@ -127,7 +140,7 @@
 
 
 def pair_kernel(
-    x_ref, p_ref, peak_ref, share_ref, qk_ref, kq_ref, kt_ref, pc_ref, acc_ref, s_ref, d_ref
+    x_ref, y_ref, p_ref, peak_ref, share_ref, qk_ref, kq_ref, kt_ref, pc_ref, acc_ref, s_ref, d_ref
 ):
     blocks = blocks_of(x_ref.shape[0])
     scale = HEAD_DIM**-0.5
@@ -136,7 +149,7 @@
         q_here = slice(q_base, q_base + q_rows)
         low = low_lanes((q_rows, LANES))
         query_low, query_high = query_block(x_ref, q_here, low)
-        grad_low = grad_block(x_ref, q_here, low)
+        grad_low = grad_block(y_ref, q_here, low)
         peak = peak_ref[:, q_here]
         share = share_ref[:, q_here]
         term = jnp.zeros((8, q_rows), jnp.float32)
@@ -145,7 +158,7 @@
             scores = score_tile(kq_ref, pc_ref, query_low, q_base, u_base, u_rows)
             soft = jnp.exp(scores - peak) * share
             s_ref[u_here, :q_rows] = soft
-            soft_grad = dot_nt(x_ref[u_here, LANES:], grad_low)
+            soft_grad = dot_nt(y_ref[u_here], grad_low)
             d_ref[u_here, :q_rows] = soft_grad
             term = term + folded(soft * soft_grad, jnp.sum)
         term = jnp.sum(term, axis=0, keepdims=True)
@@ -188,11 +201,6 @@
         away_ref[step] = jnp.where(first_core, parts[1], parts[0]).astype(jnp.bfloat16)
 
 
-def weight_open_kernel(x_ref, out_ref):
-    for plane in range(x_ref.shape[0]):
-        out_ref[:, plane * LANES : (plane + 1) * LANES] = x_ref[plane]
-
-
 def weight_line_kernel(place_ref, *refs):
     pieces, out_ref = refs[:-1], refs[-1]
     lines = out_ref.shape[0]
@@ -297,17 +305,18 @@
     heads = width // HEAD_DIM
     length = planes * tokens
     w_cols = value_weight.shape[1]
-    weight_block = jnp.broadcast_to(value_weight.T, (planes, w_cols, model // planes))
-    weight_block = exchanged(weight_block, "sp")
     place = jnp.stack([core, lax.axis_index("x"), lax.axis_index("y")]).astype(jnp.int32)
     small, whole = pl.BlockSpec(memory_space=pltpu.SMEM), pl.BlockSpec(memory_space=pltpu.VMEM)
-    weight_block = pl.pallas_call(weight_open_kernel, out_shape=shaped(w_cols, model))(
-        near(weight_block)
-    )
-    packed = pl.pallas_call(pack_kernel, out_shape=shaped(heads, tokens, 2 * LANES))(
-        query_vectors[0], key_vectors[0], value_vectors[0], cotangent[0]
-    )
-    arrived = exchanged(packed, "sp")
+    first, second = pl.pallas_call(
+        pack_kernel,
+        out_shape=(shaped(heads, tokens + w_cols, LANES), shaped(heads, tokens, LANES)),
+    )(query_vectors[0], key_vectors[0], value_vectors[0], cotangent[0], value_weight.T)
+    first = exchanged(first, "sp")
+    second = near(exchanged(second, "sp").reshape(length, LANES))
+    sequence, weight_block = pl.pallas_call(
+        open_kernel, out_shape=(shaped(planes, tokens, LANES), shaped(w_cols, model))
+    )(near(first))
+    sequence = sequence.reshape(length, LANES)
     own_rows = pl.pallas_call(stack_kernel, out_shape=shaped(columns, tokens, model))(
         inputs[0], *map(near, from_all(inputs[0], "x")[1:])
     )
@@ -320,14 +329,17 @@
     weight_line = weight_line.reshape(columns * w_cols, model)
     weight_pieces = from_all(weight_line, "y")
     kept = (tokens // 2 + 7) // 8 * 8
-    sequence = near(arrived.reshape(length, 2 * LANES))
     wide, tile = pltpu.VMEM((length, LANES), jnp.float32), pltpu.VMEM((length, TILE), jnp.float32)
+    swapped = pltpu.VMEM((length, LANES), jnp.bfloat16)
     row = shaped(1, length, dtype=jnp.float32)
-    value_grad, peak, share = pl.pallas_call(
+    peak, share = pl.pallas_call(
+        stats_kernel, out_shape=(row, row), scratch_shapes=[swapped, wide, tile]
+    )(sequence, gate_prefix[0])
+    value_grad = pl.pallas_call(
         value_kernel,
-        out_shape=(shaped(planes, kept, LANES), row, row),
-        scratch_shapes=[pltpu.VMEM((length, LANES), jnp.bfloat16), wide, wide, tile],
-    )(sequence, gate_prefix[0])
+        out_shape=shaped(planes, kept, LANES),
+        scratch_shapes=[swapped, wide, wide],
+    )(sequence, second, gate_prefix[0], peak, share)
     value_back = exchanged(value_grad, "sp")
     pair_grad = pl.pallas_call(
         pair_kernel,
@@ -340,7 +352,7 @@
             tile,
             tile,
         ],
-    )(sequence, gate_prefix[0], peak, share)
+    )(sequence, second, gate_prefix[0], peak, share)
     pair_back = exchanged(pair_grad.reshape(planes, tokens, LANES), "sp")
     block = shaped(columns, tokens, LANES)
     mine, away = pl.pallas_call(

time: 245 us -> 268 us (1.094)
  the two profiles are of different devices: /device:TPU:9 before, /device:TPU:1 now
where the time goes in v6:
time: 268 us; the launch traced here: 266 us
  starting transfers between devices  100 us (37%)
  waiting for transfers between devices  70.4 us (26%)
  blocking collectives  50.2 us (19%)
  Pallas kernels  39.2 us (15%)
  other arithmetic  2.77 us (1%)
    ppermute x18, starting transfers between devices, shifted(): lax.ppermute(x, axis, [(place, (place + step) % count) for place in range...  66 us
    ppermute x18, waiting for transfers between devices, shifted(): lax.ppermute(x, axis, [(place, (place + step) % count) for place in range...  54 us
    all_to_all x1, blocking collectives, exchanged(): return lax.all_to_all(x, axis, split_axis=0, concat_axis=0, tiled=True)  50.2 us
    all_to_all x4, starting transfers between devices, exchanged(): return lax.all_to_all(x, axis, split_axis=0, concat_axis=0, tiled=True)  34.3 us
    all_to_all x4, waiting for transfers between devices, exchanged(): return lax.all_to_all(x, axis, split_axis=0, concat_axis=0, tiled=True)  16.5 us
    pallas_call x1, Pallas kernels, shards(): pl.pallas_call(pair_kernel, out_shape=shaped(length, LANES), scratch_shap...  9.44 us
  transfers between devices with their start and end apart: 22, of which 15 were waited for; matrix products, arithmetic and copies ran while one was open for 1% of the time, Pallas kernels for 12%

profile of v6, /device:TPU:1, one launch (start us, length us, event | category | flops | bytes accessed | tf_op | source)
XLA Modules:
  0.0 266.3 jit_solution(14412770990422646117)
XLA Ops:
  3.4 50.2 %all_to_all.25.x_ref = bf16[16,168,128]{2,1,0:T(8,128)(2,1)} all-to-all(bf16[16,168,128]{2,1,0:T(8,128)(2,1)} %get-tuple-element.20), channel_id=1, replica_groups=mesh['sp'=16,'y'=4,'x'=4,'core'=2] {'sp'}, dimensions={0} | all-to-all | bytes 1376256 | tf_op jit(solution)/shard_map/all_to_all | solution.py:279
  53.6 8.2 %all-to-all-start.1 = ((bf16[16,136,128]{2,1,0:T(8,128)(2,1)}), bf16[16,136,128]{2,1,0:T(8,128)(2,1)S(1)}, u32[]{:S(2)}, u32[]{:S(2)}) async-start(bf16[16,136,128]{2,1,0:T(8,128)(2,1)} %get-tuple-element.22), calls=%async_computation.1 | async-start | bytes 1114112 | tf_op jit(solution)/shard_map/all_to_all | solution.py:279
  64.9 4.4 %collective-permute-start.9 = (bf16[136,2048]{1,0:T(8,128)(2,1)S(1)}, bf16[136,2048]{1,0:T(8,128)(2,1)S(1)}, u32[]{:S(2)}, u32[]{:S(2)}) collective-permute-start(bf16[136,2048]{1,0:T(8,128)(2,1)S(1)} %bitcast.48), channel_id=1, source_target_pairs={{0,4},{2,6},{4,0},{6,2},{1,5},{3,7},{5,1},{7,3},{8,12},{10,14},{12... | collective-permute-start | bytes 1671176 | tf_op jit(solution)/shard_map/ppermute | solution.py:284
  72.3 5.8 %collective-permute-done.8.refs_1_ = bf16[136,2048]{1,0:T(8,128)(2,1)S(1)} collective-permute-done((bf16[136,2048]{1,0:T(8,128)(2,1)S(1)}, bf16[136,2048]{1,0:T(8,128)(2,1)S(1)}, u32[]{:S(2)}, u32[]{:S(2)}) %collective-permute-start.8) | collective-permute-done | bytes 557088 | tf_op jit(solution)/shard_map/ppermute | solution.py:284
  78.2 12.9 %collective-permute-done.9.refs_2_ = bf16[136,2048]{1,0:T(8,128)(2,1)S(1)} collective-permute-done((bf16[136,2048]{1,0:T(8,128)(2,1)S(1)}, bf16[136,2048]{1,0:T(8,128)(2,1)S(1)}, u32[]{:S(2)}, u32[]{:S(2)}) %collective-permute-start.9) | collective-permute-done | bytes 557088 | tf_op jit(solution)/shard_map/ppermute | solution.py:284
  95.4 3.6 %collective-permute-start.11 = (bf16[4,136,2048]{2,1,0:T(8,128)(2,1)}, bf16[4,136,2048]{2,1,0:T(8,128)(2,1)}, u32[]{:S(2)}, u32[]{:S(2)}) collective-permute-start(bf16[4,136,2048]{2,1,0:T(8,128)(2,1)} %shard_map.112.own_ref), channel_id=1, source_target_pairs={{0,1},{1,0},{2,3},{3,2},{4,5},{5,4},{6,7},{7,6},{8,9},{9,8},{10,11... | collective-permute-start | bytes 6684680 | tf_op jit(solution)/shard_map/ppermute | solution.py:284
  101.0 4.8 %shard_map.104 = (f32[1,2176]{1,0:T(1,128)}, f32[1,2176]{1,0:T(1,128)}) custom-call(bf16[2176,128]{1,0:T(8,128)(2,1)} %bitcast.38, f32[1,2176]{1,0:T(1,128)} %bitcast.56), custom_call_target="tpu_custom_call" | custom-call | tf_op jit(solution)/shard_map/pallas_call | solution.py:335
  105.8 5.2 %shard_map.107 = bf16[16,72,128]{2,1,0:T(8,128)(2,1)} custom-call(bf16[2176,128]{1,0:T(8,128)(2,1)} %bitcast.39, bf16[2176,128]{1,0:T(8,128)(2,1)S(1)} %bitcast.35, f32[1,2176]{1,0:T(1,128)} %bitcast.57, f32[1,2176]{1,0:T(1,128)} %get-tuple-element.23.peak_ref, f32[1,2176]{1,0:T(1,128)} %get-tuple-element.24.share_ref), custom_call_target="tpu_custom_call" | custom-call | tf_op jit(solution)/shard_map/pallas_call | solution.py:338
  111.0 11.5 %all-to-all-start.3 = ((bf16[16,72,128]{2,1,0:T(8,128)(2,1)}), bf16[16,72,128]{2,1,0:T(8,128)(2,1)S(1)}, u32[]{:S(2)}, u32[]{:S(2)}) async-start(bf16[16,72,128]{2,1,0:T(8,128)(2,1)} %shard_map.107), calls=%async_computation.3 | async-start | bytes 589824 | tf_op jit(solution)/shard_map/all_to_all | solution.py:279
  123.0 14.0 %all-to-all-done.3.x_ref = bf16[16,72,128]{2,1,0:T(8,128)(2,1)S(1)} async-done(((bf16[16,72,128]{2,1,0:T(8,128)(2,1)}), bf16[16,72,128]{2,1,0:T(8,128)(2,1)S(1)}, u32[]{:S(2)}, u32[]{:S(2)}) %all-to-all-start.3) | async-done | bytes 294944 | tf_op jit(solution)/shard_map/all_to_all | solution.py:279
  138.7 7.9 %collective-permute-start = (bf16[4,136,128]{2,1,0:T(8,128)(2,1)}, bf16[4,136,128]{2,1,0:T(8,128)(2,1)S(1)}, u32[]{:S(2)}, u32[]{:S(2)}) collective-permute-start(bf16[4,136,128]{2,1,0:T(8,128)(2,1)} %get-tuple-element.28), channel_id=1, source_target_pairs={{0,1},{1,0},{2,3},{3,2},{4,5},{5,4},{6,7},{7,6},{8,9},{9,8},{10,11... | collective-permute-start | bytes 417800 | tf_op jit(solution)/shard_map/ppermute | solution.py:284
  148.6 4.0 %collective-permute-start.12 = (bf16[2,136,128]{2,1,0:T(8,128)(2,1)S(1)}, bf16[2,136,128]{2,1,0:T(8,128)(2,1)S(1)}, u32[]{:S(2)}, u32[]{:S(2)}) collective-permute-start(bf16[2,136,128]{2,1,0:T(8,128)(2,1)S(1)} %get-tuple-element.38), channel_id=1, source_target_pairs={{0,2},{2,4},{4,6},{6,0},{1,3},{3,5},{5,7},{7,1},{8,10},{10,12},{12... | collective-permute-start | bytes 208904 | tf_op jit(solution)/shard_map/ppermute | solution.py:284
  164.3 4.8 %collective-permute-start.17 = (bf16[32,2048]{1,0:T(8,128)(2,1)S(1)}, bf16[32,2048]{1,0:T(8,128)(2,1)S(1)}, u32[]{:S(2)}, u32[]{:S(2)}) collective-permute-start(bf16[32,2048]{1,0:T(8,128)(2,1)S(1)} %get-tuple-element.35), channel_id=1, source_target_pairs={{0,24},{8,0},{16,8},{24,16},{1,25},{9,1},{17,9},{25,17},{2,26},{10... | collective-permute-start | bytes 393224 | tf_op jit(solution)/shard_map/ppermute | solution.py:284
  179.8 5.7 %all-to-all-start.4 = ((bf16[16,32,128]{2,1,0:T(8,128)(2,1)}), bf16[16,32,128]{2,1,0:T(8,128)(2,1)S(1)}, u32[]{:S(2)}, u32[]{:S(2)}) async-start(bf16[16,32,128]{2,1,0:T(8,128)(2,1)} %bitcast_bitcast_fusion), calls=%async_computation.4 | async-start | bytes 262144 | tf_op jit(solution)/shard_map/all_to_all | solution.py:279
  185.5 9.4 %shard_map.105 = bf16[2176,128]{1,0:T(8,128)(2,1)} custom-call(bf16[2176,128]{1,0:T(8,128)(2,1)} %bitcast.40, bf16[2176,128]{1,0:T(8,128)(2,1)S(1)} %bitcast.36, f32[1,2176]{1,0:T(1,128)} %bitcast.58, f32[1,2176]{1,0:T(1,128)} %get-tuple-element.23.peak_ref, f32[1,2176]{1,0:T(1,128)} %get-tuple-element.24.share_ref), custom_call_target="tpu_custom_call" | custom-call | tf_op jit(solution)/shard_map/pallas_call | solution.py:344
  197.5 9.0 %all-to-all-start.2 = ((bf16[16,136,128]{2,1,0:T(8,128)(2,1)}), bf16[16,136,128]{2,1,0:T(8,128)(2,1)S(1)}, u32[]{:S(2)}, u32[]{:S(2)}) async-start(bf16[16,136,128]{2,1,0:T(8,128)(2,1)} %bitcast.41), calls=%async_computation.2 | async-start | bytes 1114112 | tf_op jit(solution)/shard_map/all_to_all | solution.py:279
  209.4 4.6 %collective-permute-start.2 = (bf16[32,2048]{1,0:T(8,128)(2,1)S(1)}, bf16[32,2048]{1,0:T(8,128)(2,1)S(1)}, u32[]{:S(2)}, u32[]{:S(2)}) collective-permute-start(bf16[32,2048]{1,0:T(8,128)(2,1)S(1)} %copy-done.7), channel_id=1, source_target_pairs={{0,4},{2,6},{4,0},{6,2},{1,5},{3,7},{5,1},{7,3},{8,12},{10,14},{12... | collective-permute-start | bytes 393224 | tf_op jit(solution)/shard_map/ppermute | solution.py:284
  216.6 4.0 %collective-permute-done.3.refs_3_ = bf16[32,2048]{1,0:T(8,128)(2,1)S(1)} collective-permute-done((bf16[32,2048]{1,0:T(8,128)(2,1)S(1)}, bf16[32,2048]{1,0:T(8,128)(2,1)S(1)}, u32[]{:S(2)}, u32[]{:S(2)}) %collective-permute-start.3) | collective-permute-done | bytes 131104 | tf_op jit(solution)/shard_map/ppermute | solution.py:284
  224.5 4.1 %collective-permute-start.5 = (bf16[128,2048]{1,0:T(8,128)(2,1)}, bf16[128,2048]{1,0:T(8,128)(2,1)S(1)}, u32[]{:S(2)}, u32[]{:S(2)}) collective-permute-start(bf16[128,2048]{1,0:T(8,128)(2,1)} %bitcast.43), channel_id=1, source_target_pairs={{0,16},{8,24},{16,0},{24,8},{1,17},{9,25},{17,1},{25,9},{2,18},{10... | collective-permute-start | bytes 1572872 | tf_op jit(solution)/shard_map/ppermute | solution.py:284
  228.6 4.0 %collective-permute-start.6 = (bf16[128,2048]{1,0:T(8,128)(2,1)}, bf16[128,2048]{1,0:T(8,128)(2,1)S(1)}, u32[]{:S(2)}, u32[]{:S(2)}) collective-permute-start(bf16[128,2048]{1,0:T(8,128)(2,1)} %bitcast.44), channel_id=1, source_target_pairs={{0,24},{8,0},{16,8},{24,16},{1,25},{9,1},{17,9},{25,17},{2,26},{10... | collective-permute-start | bytes 1572872 | tf_op jit(solution)/shard_map/ppermute | solution.py:284
  234.6 12.2 %collective-permute-done.5.refs_2_ = bf16[128,2048]{1,0:T(8,128)(2,1)S(1)} collective-permute-done((bf16[128,2048]{1,0:T(8,128)(2,1)}, bf16[128,2048]{1,0:T(8,128)(2,1)S(1)}, u32[]{:S(2)}, u32[]{:S(2)}) %collective-permute-start.5) | collective-permute-done | bytes 524320 | tf_op jit(solution)/shard_map/ppermute | solution.py:284
  246.8 4.6 %collective-permute-done.6.refs_3_ = bf16[128,2048]{1,0:T(8,128)(2,1)S(1)} collective-permute-done((bf16[128,2048]{1,0:T(8,128)(2,1)}, bf16[128,2048]{1,0:T(8,128)(2,1)S(1)}, u32[]{:S(2)}, u32[]{:S(2)}) %collective-permute-start.6) | collective-permute-done | bytes 524320 | tf_op jit(solution)/shard_map/ppermute | solution.py:284
  252.2 4.2 %shard_map.110 = (f32[136,2048]{1,0:T(8,128)}, bf16[136,2048]{1,0:T(8,128)(2,1)}) custom-call(s32[3]{0:T(128)} %pad_add_fusion.place_ref, bf16[4,136,128]{2,1,0:T(8,128)(2,1)} %get-tuple-element.27.first_ref, bf16[4,136,128]{2,1,0:T(8,128)(2,1)S(1)} %collective-permute-done.second_ref, bf16[128,2048]{1,0:T(8,128)(2,1)} %bitcast.45, ...), custom_call_target="tpu_custom_call" | custom-call | tf_op jit(solution)/shard_map/pallas_call | solution.py:379
  256.4 4.3 %collective-permute-start.7 = (bf16[136,2048]{1,0:T(8,128)(2,1)}, bf16[136,2048]{1,0:T(8,128)(2,1)S(1)}, u32[]{:S(2)}, u32[]{:S(2)}) collective-permute-start(bf16[136,2048]{1,0:T(8,128)(2,1)} %get-tuple-element.31), channel_id=1, source_target_pairs={{0,1},{1,0},{2,3},{3,2},{4,5},{5,4},{6,7},{7,6},{8,9},{9,8},{10,11... | collective-permute-start | bytes 1671176 | tf_op jit(solution)/shard_map/ppermute | solution.py:284
  (53 shorter events, 62.3 us)
Async XLA Ops:
  0.6 61.1 %copy-start.3 = (bf16[1,136,2048]{2,1,0:T(8,128)(2,1)S(1)}, bf16[1,136,2048]{2,1,0:T(8,128)(2,1)}, u32[]{:S(2)}) copy-start(bf16[1,136,2048]{2,1,0:T(8,128)(2,1)} %param.7) | copy-start | bytes 1671172
  53.6 52.2 %all-to-all-start.1 = ((bf16[16,136,128]{2,1,0:T(8,128)(2,1)}), bf16[16,136,128]{2,1,0:T(8,128)(2,1)S(1)}, u32[]{:S(2)}, u32[]{:S(2)}) async-start(bf16[16,136,128]{2,1,0:T(8,128)(2,1)} %get-tuple-element.22), calls=%async_computation.1 | async-start | bytes 1114112 | tf_op jit(solution)/shard_map/all_to_all | solution.py:279
  61.7 16.4 %collective-permute-start.8 = (bf16[136,2048]{1,0:T(8,128)(2,1)S(1)}, bf16[136,2048]{1,0:T(8,128)(2,1)S(1)}, u32[]{:S(2)}, u32[]{:S(2)}) collective-permute-start(bf16[136,2048]{1,0:T(8,128)(2,1)S(1)} %bitcast.47), channel_id=1, source_target_pairs={{0,2},{2,4},{4,6},{6,0},{1,3},{3,5},{5,7},{7,1},{8,10},{10,12},{12... | collective-permute-start | bytes 1671176 | tf_op jit(solution)/shard_map/ppermute | solution.py:284
  64.9 26.2 %collective-permute-start.9 = (bf16[136,2048]{1,0:T(8,128)(2,1)S(1)}, bf16[136,2048]{1,0:T(8,128)(2,1)S(1)}, u32[]{:S(2)}, u32[]{:S(2)}) collective-permute-start(bf16[136,2048]{1,0:T(8,128)(2,1)S(1)} %bitcast.48), channel_id=1, source_target_pairs={{0,4},{2,6},{4,0},{6,2},{1,5},{3,7},{5,1},{7,3},{8,12},{10,14},{12... | collective-permute-start | bytes 1671176 | tf_op jit(solution)/shard_map/ppermute | solution.py:284
  69.2 23.6 %collective-permute-start.10 = (bf16[136,2048]{1,0:T(8,128)(2,1)S(1)}, bf16[136,2048]{1,0:T(8,128)(2,1)S(1)}, u32[]{:S(2)}, u32[]{:S(2)}) collective-permute-start(bf16[136,2048]{1,0:T(8,128)(2,1)S(1)} %bitcast.49), channel_id=1, source_target_pairs={{0,6},{2,0},{4,2},{6,4},{1,7},{3,1},{5,3},{7,5},{8,14},{10,8},{12,... | collective-permute-start | bytes 1671176 | tf_op jit(solution)/shard_map/ppermute | solution.py:284
  95.4 65.6 %copy-start = (bf16[4,136,2048]{2,1,0:T(8,128)(2,1)S(1)}, bf16[4,136,2048]{2,1,0:T(8,128)(2,1)}, u32[]{:S(2)}) copy-start(bf16[4,136,2048]{2,1,0:T(8,128)(2,1)} %shard_map.112.own_ref) | copy-start | bytes 6684676
  95.4 63.8 %collective-permute-start.11 = (bf16[4,136,2048]{2,1,0:T(8,128)(2,1)}, bf16[4,136,2048]{2,1,0:T(8,128)(2,1)}, u32[]{:S(2)}, u32[]{:S(2)}) collective-permute-start(bf16[4,136,2048]{2,1,0:T(8,128)(2,1)} %shard_map.112.own_ref), channel_id=1, source_target_pairs={{0,1},{1,0},{2,3},{3,2},{4,5},{5,4},{6,7},{7,6},{8,9},{9,8},{10,11... | collective-permute-start | bytes 6684680 | tf_op jit(solution)/shard_map/ppermute | solution.py:284
  111.0 26.0 %all-to-all-start.3 = ((bf16[16,72,128]{2,1,0:T(8,128)(2,1)}), bf16[16,72,128]{2,1,0:T(8,128)(2,1)S(1)}, u32[]{:S(2)}, u32[]{:S(2)}) async-start(bf16[16,72,128]{2,1,0:T(8,128)(2,1)} %shard_map.107), calls=%async_computation.3 | async-start | bytes 589824 | tf_op jit(solution)/shard_map/all_to_all | solution.py:279
  138.7 9.1 %collective-permute-start = (bf16[4,136,128]{2,1,0:T(8,128)(2,1)}, bf16[4,136,128]{2,1,0:T(8,128)(2,1)S(1)}, u32[]{:S(2)}, u32[]{:S(2)}) collective-permute-start(bf16[4,136,128]{2,1,0:T(8,128)(2,1)} %get-tuple-element.28), channel_id=1, source_target_pairs={{0,1},{1,0},{2,3},{3,2},{4,5},{5,4},{6,7},{7,6},{8,9},{9,8},{10,11... | collective-permute-start | bytes 417800 | tf_op jit(solution)/shard_map/ppermute | solution.py:284
  148.6 10.6 %collective-permute-start.12 = (bf16[2,136,128]{2,1,0:T(8,128)(2,1)S(1)}, bf16[2,136,128]{2,1,0:T(8,128)(2,1)S(1)}, u32[]{:S(2)}, u32[]{:S(2)}) collective-permute-start(bf16[2,136,128]{2,1,0:T(8,128)(2,1)S(1)} %get-tuple-element.38), channel_id=1, source_target_pairs={{0,2},{2,4},{4,6},{6,0},{1,3},{3,5},{5,7},{7,1},{8,10},{10,12},{12... | collective-permute-start | bytes 208904 | tf_op jit(solution)/shard_map/ppermute | solution.py:284
  152.6 6.6 %collective-permute-start.13 = (bf16[2,136,128]{2,1,0:T(8,128)(2,1)S(1)}, bf16[2,136,128]{2,1,0:T(8,128)(2,1)S(1)}, u32[]{:S(2)}, u32[]{:S(2)}) collective-permute-start(bf16[2,136,128]{2,1,0:T(8,128)(2,1)S(1)} %get-tuple-element.39), channel_id=1, source_target_pairs={{0,4},{2,6},{4,0},{6,2},{1,5},{3,7},{5,1},{7,3},{8,12},{10,14},{12... | collective-permute-start | bytes 208904 | tf_op jit(solution)/shard_map/ppermute | solution.py:284
  155.9 5.1 %collective-permute-start.14 = (bf16[2,136,128]{2,1,0:T(8,128)(2,1)S(1)}, bf16[2,136,128]{2,1,0:T(8,128)(2,1)S(1)}, u32[]{:S(2)}, u32[]{:S(2)}) collective-permute-start(bf16[2,136,128]{2,1,0:T(8,128)(2,1)S(1)} %get-tuple-element.36), channel_id=1, source_target_pairs={{0,6},{2,0},{4,2},{6,4},{1,7},{3,1},{5,3},{7,5},{8,14},{10,8},{12,... | collective-permute-start | bytes 208904 | tf_op jit(solution)/shard_map/ppermute | solution.py:284
  164.3 9.7 %collective-permute-start.17 = (bf16[32,2048]{1,0:T(8,128)(2,1)S(1)}, bf16[32,2048]{1,0:T(8,128)(2,1)S(1)}, u32[]{:S(2)}, u32[]{:S(2)}) collective-permute-start(bf16[32,2048]{1,0:T(8,128)(2,1)S(1)} %get-tuple-element.35), channel_id=1, source_target_pairs={{0,24},{8,0},{16,8},{24,16},{1,25},{9,1},{17,9},{25,17},{2,26},{10... | collective-permute-start | bytes 393224 | tf_op jit(solution)/shard_map/ppermute | solution.py:284
  169.1 7.2 %collective-permute-start.16 = (bf16[32,2048]{1,0:T(8,128)(2,1)S(1)}, bf16[32,2048]{1,0:T(8,128)(2,1)S(1)}, u32[]{:S(2)}, u32[]{:S(2)}) collective-permute-start(bf16[32,2048]{1,0:T(8,128)(2,1)S(1)} %get-tuple-element.34), channel_id=1, source_target_pairs={{0,16},{8,24},{16,0},{24,8},{1,17},{9,25},{17,1},{25,9},{2,18},{10... | collective-permute-start | bytes 393224 | tf_op jit(solution)/shard_map/ppermute | solution.py:284
  171.3 7.7 %collective-permute-start.15 = (bf16[32,2048]{1,0:T(8,128)(2,1)S(1)}, bf16[32,2048]{1,0:T(8,128)(2,1)S(1)}, u32[]{:S(2)}, u32[]{:S(2)}) collective-permute-start(bf16[32,2048]{1,0:T(8,128)(2,1)S(1)} %get-tuple-element.33), channel_id=1, source_target_pairs={{0,8},{8,16},{16,24},{24,0},{1,9},{9,17},{17,25},{25,1},{2,10},{10... | collective-permute-start | bytes 393224 | tf_op jit(solution)/shard_map/ppermute | solution.py:284
  179.8 17.7 %all-to-all-start.4 = ((bf16[16,32,128]{2,1,0:T(8,128)(2,1)}), bf16[16,32,128]{2,1,0:T(8,128)(2,1)S(1)}, u32[]{:S(2)}, u32[]{:S(2)}) async-start(bf16[16,32,128]{2,1,0:T(8,128)(2,1)} %bitcast_bitcast_fusion), calls=%async_computation.4 | async-start | bytes 262144 | tf_op jit(solution)/shard_map/all_to_all | solution.py:279
  197.5 67.8 %all-to-all-start.2 = ((bf16[16,136,128]{2,1,0:T(8,128)(2,1)}), bf16[16,136,128]{2,1,0:T(8,128)(2,1)S(1)}, u32[]{:S(2)}, u32[]{:S(2)}) async-start(bf16[16,136,128]{2,1,0:T(8,128)(2,1)} %bitcast.41), calls=%async_computation.2 | async-start | bytes 1114112 | tf_op jit(solution)/shard_map/all_to_all | solution.py:279
  206.5 9.4 %collective-permute-start.1 = (bf16[32,2048]{1,0:T(8,128)(2,1)S(1)}, bf16[32,2048]{1,0:T(8,128)(2,1)S(1)}, u32[]{:S(2)}, u32[]{:S(2)}) collective-permute-start(bf16[32,2048]{1,0:T(8,128)(2,1)S(1)} %copy-done.7), channel_id=1, source_target_pairs={{0,2},{2,4},{4,6},{6,0},{1,3},{3,5},{5,7},{7,1},{8,10},{10,12},{12... | collective-permute-start | bytes 393224 | tf_op jit(solution)/shard_map/ppermute | solution.py:284
  209.4 7.2 %collective-permute-start.2 = (bf16[32,2048]{1,0:T(8,128)(2,1)S(1)}, bf16[32,2048]{1,0:T(8,128)(2,1)S(1)}, u32[]{:S(2)}, u32[]{:S(2)}) collective-permute-start(bf16[32,2048]{1,0:T(8,128)(2,1)S(1)} %copy-done.7), channel_id=1, source_target_pairs={{0,4},{2,6},{4,0},{6,2},{1,5},{3,7},{5,1},{7,3},{8,12},{10,14},{12... | collective-permute-start | bytes 393224 | tf_op jit(solution)/shard_map/ppermute | solution.py:284
  214.0 6.7 %collective-permute-start.3 = (bf16[32,2048]{1,0:T(8,128)(2,1)S(1)}, bf16[32,2048]{1,0:T(8,128)(2,1)S(1)}, u32[]{:S(2)}, u32[]{:S(2)}) collective-permute-start(bf16[32,2048]{1,0:T(8,128)(2,1)S(1)} %copy-done.7), channel_id=1, source_target_pairs={{0,6},{2,0},{4,2},{6,4},{1,7},{3,1},{5,3},{7,5},{8,14},{10,8},{12,... | collective-permute-start | bytes 393224 | tf_op jit(solution)/shard_map/ppermute | solution.py:284
  222.4 12.2 %collective-permute-start.4 = (bf16[128,2048]{1,0:T(8,128)(2,1)}, bf16[128,2048]{1,0:T(8,128)(2,1)S(1)}, u32[]{:S(2)}, u32[]{:S(2)}) collective-permute-start(bf16[128,2048]{1,0:T(8,128)(2,1)} %bitcast.42), channel_id=1, source_target_pairs={{0,8},{8,16},{16,24},{24,0},{1,9},{9,17},{17,25},{25,1},{2,10},{10... | collective-permute-start | bytes 1572872 | tf_op jit(solution)/shard_map/ppermute | solution.py:284
  224.5 22.3 %collective-permute-start.5 = (bf16[128,2048]{1,0:T(8,128)(2,1)}, bf16[128,2048]{1,0:T(8,128)(2,1)S(1)}, u32[]{:S(2)}, u32[]{:S(2)}) collective-permute-start(bf16[128,2048]{1,0:T(8,128)(2,1)} %bitcast.43), channel_id=1, source_target_pairs={{0,16},{8,24},{16,0},{24,8},{1,17},{9,25},{17,1},{25,9},{2,18},{10... | collective-permute-start | bytes 1572872 | tf_op jit(solution)/shard_map/ppermute | solution.py:284
  228.6 22.8 %collective-permute-start.6 = (bf16[128,2048]{1,0:T(8,128)(2,1)}, bf16[128,2048]{1,0:T(8,128)(2,1)S(1)}, u32[]{:S(2)}, u32[]{:S(2)}) collective-permute-start(bf16[128,2048]{1,0:T(8,128)(2,1)} %bitcast.44), channel_id=1, source_target_pairs={{0,24},{8,0},{16,8},{24,16},{1,25},{9,1},{17,9},{25,17},{2,26},{10... | collective-permute-start | bytes 1572872 | tf_op jit(solution)/shard_map/ppermute | solution.py:284
  256.4 6.1 %collective-permute-start.7 = (bf16[136,2048]{1,0:T(8,128)(2,1)}, bf16[136,2048]{1,0:T(8,128)(2,1)S(1)}, u32[]{:S(2)}, u32[]{:S(2)}) collective-permute-start(bf16[136,2048]{1,0:T(8,128)(2,1)} %get-tuple-element.31), channel_id=1, source_target_pairs={{0,1},{1,0},{2,3},{3,2},{4,5},{5,4},{6,7},{7,6},{8,9},{9,8},{10,11... | collective-permute-start | bytes 1671176 | tf_op jit(solution)/shard_map/ppermute | solution.py:284
  (6 other events, 66.0 us)

commit v7 on v4

--- a/solution.py
+++ b/solution.py
@@ -48,57 +48,41 @@
     return op(x.reshape(x.shape[0] // 8, 8, x.shape[1]), axis=0)
 
 
-def blocks_of(length):
-    return [(base, min(TILE, length - base)) for base in range(0, length, TILE)]
-
-
-def spread(x_ref, p_ref, kq_ref, pc_ref, acc_ref, kt_ref=None):
-    for base, rows in blocks_of(x_ref.shape[0]):
+def attention_kernel(
+    x_ref, p_ref, qk_ref, v_out_ref, kq_ref, kt_ref, pc_ref, acc_ref, dq_ref, s_ref, d_ref
+):
+    length = x_ref.shape[0]
+    scale = HEAD_DIM**-0.5
+    blocks = [(b, min(TILE, length - b)) for b in range(0, length, TILE)]
+    for base, rows in blocks:
         here = slice(base, base + rows)
-        swapped = rolled(x_ref[here, :LANES].astype(jnp.float32))
+        wide = x_ref[here, :LANES].astype(jnp.float32)
+        swapped = rolled(wide)
         kq_ref[here] = swapped.astype(jnp.bfloat16)
-        if kt_ref is not None:
-            kt_ref[:, here] = swapped.T[:HEAD_DIM].astype(jnp.bfloat16)
+        kt_ref[:, here] = swapped.T[:HEAD_DIM].astype(jnp.bfloat16)
         pc_ref[here] = jnp.broadcast_to(p_ref[:, here], (LANES, rows)).T
         acc_ref[here] = jnp.zeros((rows, LANES), jnp.float32)
-
-
-def query_block(x_ref, here, low):
-    wide = x_ref[here, :LANES].astype(jnp.float32)
-    scaled = jnp.where(low, wide * HEAD_DIM**-0.5, 0.0).astype(jnp.bfloat16)
-    return scaled, jnp.where(low, 0.0, rolled(wide)).astype(jnp.bfloat16)
-
-
-def grad_block(x_ref, here, low):
-    wide = rolled(x_ref[here, LANES:].astype(jnp.float32))
-    return jnp.where(low, wide, 0.0).astype(jnp.bfloat16)
-
-
-def score_tile(kq_ref, pc_ref, query_low, q_base, u_base, u_rows):
-    q_rows = query_low.shape[0]
-    shift = pc_ref[q_base : q_base + 1, :] - pc_ref[u_base : u_base + u_rows]
-    shift = jnp.concatenate([shift] * (q_rows // LANES), axis=1)
-    scores = dot_nt(kq_ref[u_base : u_base + u_rows], query_low) + shift
-    if u_base != q_base:
-        return scores
-    place = lax.broadcasted_iota(jnp.int32, scores.shape, 0)
-    seen = place <= lax.broadcasted_iota(jnp.int32, scores.shape, 1)
-    return jnp.where(seen, scores, FLOOR)
-
-
-def value_kernel(x_ref, p_ref, v_out_ref, peak_ref, share_ref, kq_ref, pc_ref, acc_ref, s_ref):
-    length = x_ref.shape[0]
-    blocks = blocks_of(length)
-    spread(x_ref, p_ref, kq_ref, pc_ref, acc_ref)
     for index, (q_base, q_rows) in enumerate(blocks):
         q_here = slice(q_base, q_base + q_rows)
         low = low_lanes((q_rows, LANES))
-        query_low, _ = query_block(x_ref, q_here, low)
-        grad_low = grad_block(x_ref, q_here, low)
+        query_wide = x_ref[q_here, :LANES].astype(jnp.float32)
+        grad_wide = rolled(x_ref[q_here, LANES:].astype(jnp.float32))
+        query_low = jnp.where(low, query_wide * scale, 0.0).astype(jnp.bfloat16)
+        query_high = jnp.where(low, 0.0, rolled(query_wide)).astype(jnp.bfloat16)
+        grad_low = jnp.where(low, grad_wide, 0.0).astype(jnp.bfloat16)
+        pivot = pc_ref[q_base : q_base + 1, :]
         peak = jnp.full((8, q_rows), FLOOR, jnp.float32)
         for u_base, u_rows in blocks[: index + 1]:
-            scores = score_tile(kq_ref, pc_ref, query_low, q_base, u_base, u_rows)
-            s_ref[u_base : u_base + u_rows, :q_rows] = scores
+            u_here = slice(u_base, u_base + u_rows)
+            shift = pivot - pc_ref[u_here]
+            shift = jnp.concatenate([shift] * (q_rows // LANES), axis=1)
+            scores = dot_nt(kq_ref[u_here], query_low) + shift
+            if u_base == q_base:
+                seen = lax.broadcasted_iota(jnp.int32, scores.shape, 0) <= lax.broadcasted_iota(
+                    jnp.int32, scores.shape, 1
+                )
+                scores = jnp.where(seen, scores, FLOOR)
+            s_ref[u_here, :q_rows] = scores
             peak = jnp.maximum(peak, folded(scores, jnp.max))
         peak = jnp.max(peak, axis=0, keepdims=True)
         total = jnp.zeros((8, q_rows), jnp.float32)
@@ -108,43 +92,12 @@
             s_ref[u_here, :q_rows] = raised
             total = total + folded(raised, jnp.sum)
         share = 1.0 / jnp.sum(total, axis=0, keepdims=True)
-        peak_ref[:, q_here] = peak
-        share_ref[:, q_here] = share
+        term = jnp.zeros((8, q_rows), jnp.float32)
         for u_base, u_rows in blocks[: index + 1]:
             u_here = slice(u_base, u_base + u_rows)
             soft = s_ref[u_here, :q_rows] * share
+            s_ref[u_here, :q_rows] = soft
             acc_ref[u_here] += dot_nn(soft.astype(jnp.bfloat16), grad_low)
-    planes, kept, _ = v_out_ref.shape
-    tokens = length // planes
-    for plane in range(planes):
-        base = plane * tokens
-        first = acc_ref[base : base + kept]
-        second = acc_ref[base + kept : base + tokens]
-        second = jnp.concatenate([second, first[: 2 * kept - tokens]], axis=0)
-        v_out_ref[plane] = jnp.where(low_lanes(first.shape), first, rolled(second)).astype(
-            jnp.bfloat16
-        )
-
-
-def pair_kernel(
-    x_ref, p_ref, peak_ref, share_ref, qk_ref, kq_ref, kt_ref, pc_ref, acc_ref, s_ref, d_ref
-):
-    blocks = blocks_of(x_ref.shape[0])
-    scale = HEAD_DIM**-0.5
-    spread(x_ref, p_ref, kq_ref, pc_ref, acc_ref, kt_ref)
-    for index, (q_base, q_rows) in enumerate(blocks):
-        q_here = slice(q_base, q_base + q_rows)
-        low = low_lanes((q_rows, LANES))
-        query_low, query_high = query_block(x_ref, q_here, low)
-        grad_low = grad_block(x_ref, q_here, low)
-        peak = peak_ref[:, q_here]
-        share = share_ref[:, q_here]
-        term = jnp.zeros((8, q_rows), jnp.float32)
-        for u_base, u_rows in blocks[: index + 1]:
-            u_here = slice(u_base, u_base + u_rows)
-            scores = score_tile(kq_ref, pc_ref, query_low, q_base, u_base, u_rows)
-            soft = jnp.exp(scores - peak) * share
-            s_ref[u_here, :q_rows] = soft
             soft_grad = dot_nt(x_ref[u_here, LANES:], grad_low)
             d_ref[u_here, :q_rows] = soft_grad
             term = term + folded(soft * soft_grad, jnp.sum)
@@ -158,10 +111,27 @@
             acc_ref[u_here] += dot_nn(score_low, query_high)
             query_grad = query_grad + dot_nn(kt_ref[:, u_here], score_low)
         query_grad = jnp.concatenate([query_grad, jnp.zeros_like(query_grad)], axis=0)
-        acc_ref[q_here] += query_grad.T
+        dq_ref[q_here] = query_grad.T
     for base, rows in blocks:
         here = slice(base, base + rows)
-        qk_ref[here] = (acc_ref[here] * scale).astype(jnp.bfloat16)
+        qk_ref[here] = (
+            jnp.where(low_lanes((rows, LANES)), dq_ref[here], acc_ref[here]) * scale
+        ).astype(jnp.bfloat16)
+    planes, kept, _ = v_out_ref.shape
+    tokens = length // planes
+    for plane in range(planes):
+        base = plane * tokens
+        first = acc_ref[base : base + kept]
+        second = acc_ref[base + kept : base + tokens]
+        second = jnp.concatenate([second, first[: 2 * kept - tokens]], axis=0)
+        v_out_ref[plane] = jnp.where(low_lanes(first.shape), first, rolled(second)).astype(
+            jnp.bfloat16
+        )
+
+
+def spread_kernel(w_ref, out_ref):
+    for plane in range(out_ref.shape[0]):
+        out_ref[plane] = w_ref[...]
 
 
 def unpack_value_kernel(place_ref, x_ref, mine_ref, away_ref):
@@ -297,17 +267,19 @@
     heads = width // HEAD_DIM
     length = planes * tokens
     w_cols = value_weight.shape[1]
-    weight_block = jnp.broadcast_to(value_weight.T, (planes, w_cols, model // planes))
-    weight_block = exchanged(weight_block, "sp")
     place = jnp.stack([core, lax.axis_index("x"), lax.axis_index("y")]).astype(jnp.int32)
     small, whole = pl.BlockSpec(memory_space=pltpu.SMEM), pl.BlockSpec(memory_space=pltpu.VMEM)
+    packed = pl.pallas_call(pack_kernel, out_shape=shaped(heads, tokens, 2 * LANES))(
+        query_vectors[0], key_vectors[0], value_vectors[0], cotangent[0]
+    )
+    arrived = exchanged(packed, "sp")
+    weight_block = pl.pallas_call(
+        spread_kernel, out_shape=shaped(planes, w_cols, model // planes)
+    )(value_weight.T)
+    weight_block = exchanged(weight_block, "sp")
     weight_block = pl.pallas_call(weight_open_kernel, out_shape=shaped(w_cols, model))(
         near(weight_block)
     )
-    packed = pl.pallas_call(pack_kernel, out_shape=shaped(heads, tokens, 2 * LANES))(
-        query_vectors[0], key_vectors[0], value_vectors[0], cotangent[0]
-    )
-    arrived = exchanged(packed, "sp")
     own_rows = pl.pallas_call(stack_kernel, out_shape=shaped(columns, tokens, model))(
         inputs[0], *map(near, from_all(inputs[0], "x")[1:])
     )
@@ -318,29 +290,26 @@
         in_specs=[small] + [whole] * columns,
     )(place, weight_block, *map(near, from_all(weight_block, "x")[1:]))
     weight_line = weight_line.reshape(columns * w_cols, model)
-    weight_pieces = from_all(weight_line, "y")
+    weight_pieces = [weight_line]
+    for step in range(1, lines):
+        weight_pieces.append(shifted(weight_line, "y", step))
     kept = (tokens // 2 + 7) // 8 * 8
     sequence = near(arrived.reshape(length, 2 * LANES))
     wide, tile = pltpu.VMEM((length, LANES), jnp.float32), pltpu.VMEM((length, TILE), jnp.float32)
-    row = shaped(1, length, dtype=jnp.float32)
-    value_grad, peak, share = pl.pallas_call(
-        value_kernel,
-        out_shape=(shaped(planes, kept, LANES), row, row),
-        scratch_shapes=[pltpu.VMEM((length, LANES), jnp.bfloat16), wide, wide, tile],
-    )(sequence, gate_prefix[0])
-    value_back = exchanged(value_grad, "sp")
-    pair_grad = pl.pallas_call(
-        pair_kernel,
-        out_shape=shaped(length, LANES),
+    pair_grad, value_grad = pl.pallas_call(
+        attention_kernel,
+        out_shape=(shaped(length, LANES), shaped(planes, kept, LANES)),
         scratch_shapes=[
             pltpu.VMEM((length, LANES), jnp.bfloat16),
             pltpu.VMEM((HEAD_DIM, length), jnp.bfloat16),
             wide,
             wide,
+            wide,
             tile,
             tile,
         ],
-    )(sequence, gate_prefix[0], peak, share)
+    )(sequence, gate_prefix[0])
+    value_back = exchanged(value_grad, "sp")
     pair_back = exchanged(pair_grad.reshape(planes, tokens, LANES), "sp")
     block = shaped(columns, tokens, LANES)
     mine, away = pl.pallas_call(

time: 245 us -> 245 us (level)
  the two profiles are of different devices: /device:TPU:9 before, /device:TPU:1 now
where the time goes in v7:
time: 245 us; the launch traced here: 243 us
  starting transfers between devices  108 us (44%)
  waiting for transfers between devices  72.4 us (30%)
  Pallas kernels  33.4 us (14%)
  blocking collectives  23.3 us (10%)
  local copies, waits for them, and re-layouts  3.07 us (1%)
    ppermute x18, starting transfers between devices, shifted(): lax.ppermute(x, axis, [(place, (place + step) % count) for place in range...  68.9 us
    ppermute x18, waiting for transfers between devices, shifted(): lax.ppermute(x, axis, [(place, (place + step) % count) for place in range...  50.4 us
    all_to_all x4, starting transfers between devices, exchanged(): return lax.all_to_all(x, axis, split_axis=0, concat_axis=0, tiled=True)  39.1 us
    all_to_all x1, blocking collectives, exchanged(): return lax.all_to_all(x, axis, split_axis=0, concat_axis=0, tiled=True)  23.3 us
    all_to_all x4, waiting for transfers between devices, exchanged(): return lax.all_to_all(x, axis, split_axis=0, concat_axis=0, tiled=True)  22.1 us
    pallas_call x1, Pallas kernels, shards(): pl.pallas_call(attention_kernel, out_shape=(shaped(length, LANES), shaped...  12.6 us
  transfers between devices with their start and end apart: 22, of which 14 were waited for; matrix products, arithmetic and copies ran while one was open for 1% of the time, Pallas kernels for 12%

profile of v7, /device:TPU:1, one launch (start us, length us, event | category | flops | bytes accessed | tf_op | source)
XLA Modules:
  0.0 243.3 jit_solution(5976298089946608236)
XLA Ops:
  3.3 15.9 %all-to-all-start = ((bf16[16,136,256]{2,1,0:T(8,128)(2,1)}), bf16[16,136,256]{2,1,0:T(8,128)(2,1)S(1)}, u32[]{:S(2)}, u32[]{:S(2)}) async-start(bf16[16,136,256]{2,1,0:T(8,128)(2,1)} %shard_map.102), calls=%async_computation | async-start | bytes 2228224 | tf_op jit(solution)/shard_map/all_to_all | solution.py:241
  19.2 4.4 %collective-permute-start.10 = (bf16[136,2048]{1,0:T(8,128)(2,1)S(1)}, bf16[136,2048]{1,0:T(8,128)(2,1)S(1)}, u32[]{:S(2)}, u32[]{:S(2)}) collective-permute-start(bf16[136,2048]{1,0:T(8,128)(2,1)S(1)} %bitcast.41), channel_id=1, source_target_pairs={{0,6},{2,0},{4,2},{6,4},{1,7},{3,1},{5,3},{7,5},{8,14},{10,8},{12,... | collective-permute-start | bytes 1671176 | tf_op jit(solution)/shard_map/ppermute | solution.py:246
  25.5 3.6 %collective-permute-start.9 = (bf16[136,2048]{1,0:T(8,128)(2,1)S(1)}, bf16[136,2048]{1,0:T(8,128)(2,1)S(1)}, u32[]{:S(2)}, u32[]{:S(2)}) collective-permute-start(bf16[136,2048]{1,0:T(8,128)(2,1)S(1)} %bitcast.43), channel_id=1, source_target_pairs={{0,4},{2,6},{4,0},{6,2},{1,5},{3,7},{5,1},{7,3},{8,12},{10,14},{12... | collective-permute-start | bytes 1671176 | tf_op jit(solution)/shard_map/ppermute | solution.py:246
  29.2 6.2 %collective-permute-done.10.refs_3_ = bf16[136,2048]{1,0:T(8,128)(2,1)S(1)} collective-permute-done((bf16[136,2048]{1,0:T(8,128)(2,1)S(1)}, bf16[136,2048]{1,0:T(8,128)(2,1)S(1)}, u32[]{:S(2)}, u32[]{:S(2)}) %collective-permute-start.10) | collective-permute-done | bytes 557088 | tf_op jit(solution)/shard_map/ppermute | solution.py:246
  35.4 5.2 %collective-permute-done.8.refs_1_ = bf16[136,2048]{1,0:T(8,128)(2,1)S(1)} collective-permute-done((bf16[136,2048]{1,0:T(8,128)(2,1)S(1)}, bf16[136,2048]{1,0:T(8,128)(2,1)S(1)}, u32[]{:S(2)}, u32[]{:S(2)}) %collective-permute-start.8) | collective-permute-done | bytes 557088 | tf_op jit(solution)/shard_map/ppermute | solution.py:246
  40.6 10.1 %collective-permute-done.9.refs_2_ = bf16[136,2048]{1,0:T(8,128)(2,1)S(1)} collective-permute-done((bf16[136,2048]{1,0:T(8,128)(2,1)S(1)}, bf16[136,2048]{1,0:T(8,128)(2,1)S(1)}, u32[]{:S(2)}, u32[]{:S(2)}) %collective-permute-start.9) | collective-permute-done | bytes 557088 | tf_op jit(solution)/shard_map/ppermute | solution.py:246
  53.3 4.9 %collective-permute-start.11 = (bf16[4,136,2048]{2,1,0:T(8,128)(2,1)}, bf16[4,136,2048]{2,1,0:T(8,128)(2,1)}, u32[]{:S(2)}, u32[]{:S(2)}) collective-permute-start(bf16[4,136,2048]{2,1,0:T(8,128)(2,1)} %shard_map.111.own_ref), channel_id=1, source_target_pairs={{0,1},{1,0},{2,3},{3,2},{4,5},{5,4},{6,7},{7,6},{8,9},{9,8},{10,11... | collective-permute-start | bytes 6684680 | tf_op jit(solution)/shard_map/ppermute | solution.py:246
  58.2 8.4 %all-to-all-done = bf16[16,136,256]{2,1,0:T(8,128)(2,1)S(1)} async-done(((bf16[16,136,256]{2,1,0:T(8,128)(2,1)}), bf16[16,136,256]{2,1,0:T(8,128)(2,1)S(1)}, u32[]{:S(2)}, u32[]{:S(2)}) %all-to-all-start) | async-done | bytes 1114144 | tf_op jit(solution)/shard_map/all_to_all | solution.py:241
  68.9 12.6 %shard_map.103 = (bf16[2176,128]{1,0:T(8,128)(2,1)}, bf16[16,72,128]{2,1,0:T(8,128)(2,1)}) custom-call(bf16[2176,256]{1,0:T(8,128)(2,1)S(1)} %bitcast.34, f32[1,2176]{1,0:T(1,128)} %bitcast.52), custom_call_target="tpu_custom_call" | custom-call | tf_op jit(solution)/shard_map/pallas_call | solution.py:299
  81.4 13.5 %all-to-all-start.2 = ((bf16[16,72,128]{2,1,0:T(8,128)(2,1)}), bf16[16,72,128]{2,1,0:T(8,128)(2,1)S(1)}, u32[]{:S(2)}, u32[]{:S(2)}) async-start(bf16[16,72,128]{2,1,0:T(8,128)(2,1)} %get-tuple-element.19), calls=%async_computation.2 | async-start | bytes 589824 | tf_op jit(solution)/shard_map/all_to_all | solution.py:241
  95.6 13.7 %all-to-all-done.2.x_ref = bf16[16,72,128]{2,1,0:T(8,128)(2,1)S(1)} async-done(((bf16[16,72,128]{2,1,0:T(8,128)(2,1)}), bf16[16,72,128]{2,1,0:T(8,128)(2,1)S(1)}, u32[]{:S(2)}, u32[]{:S(2)}) %all-to-all-start.2) | async-done | bytes 294944 | tf_op jit(solution)/shard_map/all_to_all | solution.py:241
  110.9 8.1 %collective-permute-start = (bf16[4,136,128]{2,1,0:T(8,128)(2,1)}, bf16[4,136,128]{2,1,0:T(8,128)(2,1)S(1)}, u32[]{:S(2)}, u32[]{:S(2)}) collective-permute-start(bf16[4,136,128]{2,1,0:T(8,128)(2,1)} %get-tuple-element.21), channel_id=1, source_target_pairs={{0,1},{1,0},{2,3},{3,2},{4,5},{5,4},{6,7},{7,6},{8,9},{9,8},{10,11... | collective-permute-start | bytes 417800 | tf_op jit(solution)/shard_map/ppermute | solution.py:246
  120.4 5.7 %all-to-all-start.3 = ((bf16[16,32,128]{2,1,0:T(8,128)(2,1)}), bf16[16,32,128]{2,1,0:T(8,128)(2,1)S(1)}, u32[]{:S(2)}, u32[]{:S(2)}) async-start(bf16[16,32,128]{2,1,0:T(8,128)(2,1)} %shard_map.106), calls=%async_computation.3 | async-start | bytes 262144 | tf_op jit(solution)/shard_map/all_to_all | solution.py:241
  130.0 4.4 %collective-permute-start.13 = (bf16[2,136,128]{2,1,0:T(8,128)(2,1)S(1)}, bf16[2,136,128]{2,1,0:T(8,128)(2,1)S(1)}, u32[]{:S(2)}, u32[]{:S(2)}) collective-permute-start(bf16[2,136,128]{2,1,0:T(8,128)(2,1)S(1)} %get-tuple-element.31), channel_id=1, source_target_pairs={{0,4},{2,6},{4,0},{6,2},{1,5},{3,7},{5,1},{7,3},{8,12},{10,14},{12... | collective-permute-start | bytes 208904 | tf_op jit(solution)/shard_map/ppermute | solution.py:246
  134.4 3.2 %collective-permute-start.14 = (bf16[2,136,128]{2,1,0:T(8,128)(2,1)S(1)}, bf16[2,136,128]{2,1,0:T(8,128)(2,1)S(1)}, u32[]{:S(2)}, u32[]{:S(2)}) collective-permute-start(bf16[2,136,128]{2,1,0:T(8,128)(2,1)S(1)} %get-tuple-element.28), channel_id=1, source_target_pairs={{0,6},{2,0},{4,2},{6,4},{1,7},{3,1},{5,3},{7,5},{8,14},{10,8},{12,... | collective-permute-start | bytes 208904 | tf_op jit(solution)/shard_map/ppermute | solution.py:246
  145.7 4.5 %collective-permute-start.16 = (bf16[32,2048]{1,0:T(8,128)(2,1)S(1)}, bf16[32,2048]{1,0:T(8,128)(2,1)S(1)}, u32[]{:S(2)}, u32[]{:S(2)}) collective-permute-start(bf16[32,2048]{1,0:T(8,128)(2,1)S(1)} %get-tuple-element.26), channel_id=1, source_target_pairs={{0,16},{8,24},{16,0},{24,8},{1,17},{9,25},{17,1},{25,9},{2,18},{10... | collective-permute-start | bytes 393224 | tf_op jit(solution)/shard_map/ppermute | solution.py:246
  156.0 23.3 %all_to_all.25 = bf16[16,32,128]{2,1,0:T(8,128)(2,1)S(1)} all-to-all(bf16[16,32,128]{2,1,0:T(8,128)(2,1)S(1)} %bitcast_bitcast_fusion), channel_id=1, replica_groups=mesh['sp'=16,'y'=4,'x'=4,'core'=2] {'sp'}, dimensions={0} | all-to-all | bytes 262144 | tf_op jit(solution)/shard_map/all_to_all | solution.py:241
  179.3 4.0 %all-to-all-start.1 = ((bf16[16,136,128]{2,1,0:T(8,128)(2,1)}), bf16[16,136,128]{2,1,0:T(8,128)(2,1)S(1)}, u32[]{:S(2)}, u32[]{:S(2)}) async-start(bf16[16,136,128]{2,1,0:T(8,128)(2,1)} %bitcast.44), calls=%async_computation.1 | async-start | bytes 1114112 | tf_op jit(solution)/shard_map/all_to_all | solution.py:241
  186.0 5.4 %collective-permute-start.2 = (bf16[32,2048]{1,0:T(8,128)(2,1)}, bf16[32,2048]{1,0:T(8,128)(2,1)S(1)}, u32[]{:S(2)}, u32[]{:S(2)}) collective-permute-start(bf16[32,2048]{1,0:T(8,128)(2,1)} %shard_map.107.refs_0_), channel_id=1, source_target_pairs={{0,4},{2,6},{4,0},{6,2},{1,5},{3,7},{5,1},{7,3},{8,12},{10,14},{12... | collective-permute-start | bytes 393224 | tf_op jit(solution)/shard_map/ppermute | solution.py:246
  201.3 5.5 %collective-permute-start.5 = (bf16[128,2048]{1,0:T(8,128)(2,1)}, bf16[128,2048]{1,0:T(8,128)(2,1)S(1)}, u32[]{:S(2)}, u32[]{:S(2)}) collective-permute-start(bf16[128,2048]{1,0:T(8,128)(2,1)} %bitcast.37), channel_id=1, source_target_pairs={{0,16},{8,24},{16,0},{24,8},{1,17},{9,25},{17,1},{25,9},{2,18},{10... | collective-permute-start | bytes 1572872 | tf_op jit(solution)/shard_map/ppermute | solution.py:246
  211.0 10.7 %collective-permute-done.5.refs_2_ = bf16[128,2048]{1,0:T(8,128)(2,1)S(1)} collective-permute-done((bf16[128,2048]{1,0:T(8,128)(2,1)}, bf16[128,2048]{1,0:T(8,128)(2,1)S(1)}, u32[]{:S(2)}, u32[]{:S(2)}) %collective-permute-start.5) | collective-permute-done | bytes 524320 | tf_op jit(solution)/shard_map/ppermute | solution.py:246
  221.7 5.0 %collective-permute-done.6.refs_3_ = bf16[128,2048]{1,0:T(8,128)(2,1)S(1)} collective-permute-done((bf16[128,2048]{1,0:T(8,128)(2,1)}, bf16[128,2048]{1,0:T(8,128)(2,1)S(1)}, u32[]{:S(2)}, u32[]{:S(2)}) %collective-permute-start.6) | collective-permute-done | bytes 524320 | tf_op jit(solution)/shard_map/ppermute | solution.py:246
  227.5 4.2 %shard_map.109 = (f32[136,2048]{1,0:T(8,128)}, bf16[136,2048]{1,0:T(8,128)(2,1)}) custom-call(s32[3]{0:T(128)} %pad_add_fusion.place_ref, bf16[4,136,128]{2,1,0:T(8,128)(2,1)} %get-tuple-element.20.first_ref, bf16[4,136,128]{2,1,0:T(8,128)(2,1)S(1)} %collective-permute-done.second_ref, bf16[128,2048]{1,0:T(8,128)(2,1)} %bitcast.39, ...), custom_call_target="tpu_custom_call" | custom-call | tf_op jit(solution)/shard_map/pallas_call | solution.py:336
  231.7 6.1 %collective-permute-start.7 = (bf16[136,2048]{1,0:T(8,128)(2,1)}, bf16[136,2048]{1,0:T(8,128)(2,1)S(1)}, u32[]{:S(2)}, u32[]{:S(2)}) collective-permute-start(bf16[136,2048]{1,0:T(8,128)(2,1)} %get-tuple-element.23), channel_id=1, source_target_pairs={{0,1},{1,0},{2,3},{3,2},{4,5},{5,4},{6,7},{7,6},{8,9},{9,8},{10,11... | collective-permute-start | bytes 1671176 | tf_op jit(solution)/shard_map/ppermute | solution.py:246
  (52 shorter events, 53.9 us)
Async XLA Ops:
  3.3 63.3 %all-to-all-start = ((bf16[16,136,256]{2,1,0:T(8,128)(2,1)}), bf16[16,136,256]{2,1,0:T(8,128)(2,1)S(1)}, u32[]{:S(2)}, u32[]{:S(2)}) async-start(bf16[16,136,256]{2,1,0:T(8,128)(2,1)} %shard_map.102), calls=%async_computation | async-start | bytes 2228224 | tf_op jit(solution)/shard_map/all_to_all | solution.py:241
  19.2 16.2 %collective-permute-start.10 = (bf16[136,2048]{1,0:T(8,128)(2,1)S(1)}, bf16[136,2048]{1,0:T(8,128)(2,1)S(1)}, u32[]{:S(2)}, u32[]{:S(2)}) collective-permute-start(bf16[136,2048]{1,0:T(8,128)(2,1)S(1)} %bitcast.41), channel_id=1, source_target_pairs={{0,6},{2,0},{4,2},{6,4},{1,7},{3,1},{5,3},{7,5},{8,14},{10,8},{12,... | collective-permute-start | bytes 1671176 | tf_op jit(solution)/shard_map/ppermute | solution.py:246
  23.6 17.0 %collective-permute-start.8 = (bf16[136,2048]{1,0:T(8,128)(2,1)S(1)}, bf16[136,2048]{1,0:T(8,128)(2,1)S(1)}, u32[]{:S(2)}, u32[]{:S(2)}) collective-permute-start(bf16[136,2048]{1,0:T(8,128)(2,1)S(1)} %bitcast.42), channel_id=1, source_target_pairs={{0,2},{2,4},{4,6},{6,0},{1,3},{3,5},{5,7},{7,1},{8,10},{10,12},{12... | collective-permute-start | bytes 1671176 | tf_op jit(solution)/shard_map/ppermute | solution.py:246
  25.5 25.2 %collective-permute-start.9 = (bf16[136,2048]{1,0:T(8,128)(2,1)S(1)}, bf16[136,2048]{1,0:T(8,128)(2,1)S(1)}, u32[]{:S(2)}, u32[]{:S(2)}) collective-permute-start(bf16[136,2048]{1,0:T(8,128)(2,1)S(1)} %bitcast.43), channel_id=1, source_target_pairs={{0,4},{2,6},{4,0},{6,2},{1,5},{3,7},{5,1},{7,3},{8,12},{10,14},{12... | collective-permute-start | bytes 1671176 | tf_op jit(solution)/shard_map/ppermute | solution.py:246
  53.3 84.4 %collective-permute-start.11 = (bf16[4,136,2048]{2,1,0:T(8,128)(2,1)}, bf16[4,136,2048]{2,1,0:T(8,128)(2,1)}, u32[]{:S(2)}, u32[]{:S(2)}) collective-permute-start(bf16[4,136,2048]{2,1,0:T(8,128)(2,1)} %shard_map.111.own_ref), channel_id=1, source_target_pairs={{0,1},{1,0},{2,3},{3,2},{4,5},{5,4},{6,7},{7,6},{8,9},{9,8},{10,11... | collective-permute-start | bytes 6684680 | tf_op jit(solution)/shard_map/ppermute | solution.py:246
  68.9 70.9 %copy-start = (bf16[4,136,2048]{2,1,0:T(8,128)(2,1)S(1)}, bf16[4,136,2048]{2,1,0:T(8,128)(2,1)}, u32[]{:S(2)}) copy-start(bf16[4,136,2048]{2,1,0:T(8,128)(2,1)} %shard_map.111.own_ref) | copy-start | bytes 6684676
  81.4 27.8 %all-to-all-start.2 = ((bf16[16,72,128]{2,1,0:T(8,128)(2,1)}), bf16[16,72,128]{2,1,0:T(8,128)(2,1)S(1)}, u32[]{:S(2)}, u32[]{:S(2)}) async-start(bf16[16,72,128]{2,1,0:T(8,128)(2,1)} %get-tuple-element.19), calls=%async_computation.2 | async-start | bytes 589824 | tf_op jit(solution)/shard_map/all_to_all | solution.py:241
  95.6 44.2 %copy-start.3 = (s32[3]{0:T(128)S(1)}, s32[3]{0:T(128)}, u32[]{:S(2)}) copy-start(s32[3]{0:T(128)} %pad_add_fusion.place_ref) | copy-start | bytes 40
  110.9 15.2 %collective-permute-start = (bf16[4,136,128]{2,1,0:T(8,128)(2,1)}, bf16[4,136,128]{2,1,0:T(8,128)(2,1)S(1)}, u32[]{:S(2)}, u32[]{:S(2)}) collective-permute-start(bf16[4,136,128]{2,1,0:T(8,128)(2,1)} %get-tuple-element.21), channel_id=1, source_target_pairs={{0,1},{1,0},{2,3},{3,2},{4,5},{5,4},{6,7},{7,6},{8,9},{9,8},{10,11... | collective-permute-start | bytes 417800 | tf_op jit(solution)/shard_map/ppermute | solution.py:246
  120.4 35.6 %all-to-all-start.3 = ((bf16[16,32,128]{2,1,0:T(8,128)(2,1)}), bf16[16,32,128]{2,1,0:T(8,128)(2,1)S(1)}, u32[]{:S(2)}, u32[]{:S(2)}) async-start(bf16[16,32,128]{2,1,0:T(8,128)(2,1)} %shard_map.106), calls=%async_computation.3 | async-start | bytes 262144 | tf_op jit(solution)/shard_map/all_to_all | solution.py:241
  126.9 10.7 %collective-permute-start.12 = (bf16[2,136,128]{2,1,0:T(8,128)(2,1)S(1)}, bf16[2,136,128]{2,1,0:T(8,128)(2,1)S(1)}, u32[]{:S(2)}, u32[]{:S(2)}) collective-permute-start(bf16[2,136,128]{2,1,0:T(8,128)(2,1)S(1)} %get-tuple-element.30), channel_id=1, source_target_pairs={{0,2},{2,4},{4,6},{6,0},{1,3},{3,5},{5,7},{7,1},{8,10},{10,12},{12... | collective-permute-start | bytes 208904 | tf_op jit(solution)/shard_map/ppermute | solution.py:246
  130.0 7.6 %collective-permute-start.13 = (bf16[2,136,128]{2,1,0:T(8,128)(2,1)S(1)}, bf16[2,136,128]{2,1,0:T(8,128)(2,1)S(1)}, u32[]{:S(2)}, u32[]{:S(2)}) collective-permute-start(bf16[2,136,128]{2,1,0:T(8,128)(2,1)S(1)} %get-tuple-element.31), channel_id=1, source_target_pairs={{0,4},{2,6},{4,0},{6,2},{1,5},{3,7},{5,1},{7,3},{8,12},{10,14},{12... | collective-permute-start | bytes 208904 | tf_op jit(solution)/shard_map/ppermute | solution.py:246
  134.4 5.3 %collective-permute-start.14 = (bf16[2,136,128]{2,1,0:T(8,128)(2,1)S(1)}, bf16[2,136,128]{2,1,0:T(8,128)(2,1)S(1)}, u32[]{:S(2)}, u32[]{:S(2)}) collective-permute-start(bf16[2,136,128]{2,1,0:T(8,128)(2,1)S(1)} %get-tuple-element.28), channel_id=1, source_target_pairs={{0,6},{2,0},{4,2},{6,4},{1,7},{3,1},{5,3},{7,5},{8,14},{10,8},{12,... | collective-permute-start | bytes 208904 | tf_op jit(solution)/shard_map/ppermute | solution.py:246
  142.5 10.7 %collective-permute-start.15 = (bf16[32,2048]{1,0:T(8,128)(2,1)S(1)}, bf16[32,2048]{1,0:T(8,128)(2,1)S(1)}, u32[]{:S(2)}, u32[]{:S(2)}) collective-permute-start(bf16[32,2048]{1,0:T(8,128)(2,1)S(1)} %get-tuple-element.25), channel_id=1, source_target_pairs={{0,8},{8,16},{16,24},{24,0},{1,9},{9,17},{17,25},{25,1},{2,10},{10... | collective-permute-start | bytes 393224 | tf_op jit(solution)/shard_map/ppermute | solution.py:246
  145.7 8.9 %collective-permute-start.16 = (bf16[32,2048]{1,0:T(8,128)(2,1)S(1)}, bf16[32,2048]{1,0:T(8,128)(2,1)S(1)}, u32[]{:S(2)}, u32[]{:S(2)}) collective-permute-start(bf16[32,2048]{1,0:T(8,128)(2,1)S(1)} %get-tuple-element.26), channel_id=1, source_target_pairs={{0,16},{8,24},{16,0},{24,8},{1,17},{9,25},{17,1},{25,9},{2,18},{10... | collective-permute-start | bytes 393224 | tf_op jit(solution)/shard_map/ppermute | solution.py:246
  150.2 5.7 %collective-permute-start.17 = (bf16[32,2048]{1,0:T(8,128)(2,1)S(1)}, bf16[32,2048]{1,0:T(8,128)(2,1)S(1)}, u32[]{:S(2)}, u32[]{:S(2)}) collective-permute-start(bf16[32,2048]{1,0:T(8,128)(2,1)S(1)} %get-tuple-element.27), channel_id=1, source_target_pairs={{0,24},{8,0},{16,8},{24,16},{1,25},{9,1},{17,9},{25,17},{2,26},{10... | collective-permute-start | bytes 393224 | tf_op jit(solution)/shard_map/ppermute | solution.py:246
  179.3 63.0 %all-to-all-start.1 = ((bf16[16,136,128]{2,1,0:T(8,128)(2,1)}), bf16[16,136,128]{2,1,0:T(8,128)(2,1)S(1)}, u32[]{:S(2)}, u32[]{:S(2)}) async-start(bf16[16,136,128]{2,1,0:T(8,128)(2,1)} %bitcast.44), calls=%async_computation.1 | async-start | bytes 1114112 | tf_op jit(solution)/shard_map/all_to_all | solution.py:241
  184.1 9.3 %collective-permute-start.1 = (bf16[32,2048]{1,0:T(8,128)(2,1)}, bf16[32,2048]{1,0:T(8,128)(2,1)S(1)}, u32[]{:S(2)}, u32[]{:S(2)}) collective-permute-start(bf16[32,2048]{1,0:T(8,128)(2,1)} %shard_map.107.refs_0_), channel_id=1, source_target_pairs={{0,2},{2,4},{4,6},{6,0},{1,3},{3,5},{5,7},{7,1},{8,10},{10,12},{12... | collective-permute-start | bytes 393224 | tf_op jit(solution)/shard_map/ppermute | solution.py:246
  186.0 8.8 %collective-permute-start.2 = (bf16[32,2048]{1,0:T(8,128)(2,1)}, bf16[32,2048]{1,0:T(8,128)(2,1)S(1)}, u32[]{:S(2)}, u32[]{:S(2)}) collective-permute-start(bf16[32,2048]{1,0:T(8,128)(2,1)} %shard_map.107.refs_0_), channel_id=1, source_target_pairs={{0,4},{2,6},{4,0},{6,2},{1,5},{3,7},{5,1},{7,3},{8,12},{10,14},{12... | collective-permute-start | bytes 393224 | tf_op jit(solution)/shard_map/ppermute | solution.py:246
  191.4 6.2 %collective-permute-start.3 = (bf16[32,2048]{1,0:T(8,128)(2,1)}, bf16[32,2048]{1,0:T(8,128)(2,1)S(1)}, u32[]{:S(2)}, u32[]{:S(2)}) collective-permute-start(bf16[32,2048]{1,0:T(8,128)(2,1)} %shard_map.107.refs_0_), channel_id=1, source_target_pairs={{0,6},{2,0},{4,2},{6,4},{1,7},{3,1},{5,3},{7,5},{8,14},{10,8},{12,... | collective-permute-start | bytes 393224 | tf_op jit(solution)/shard_map/ppermute | solution.py:246
  199.4 11.6 %collective-permute-start.4 = (bf16[128,2048]{1,0:T(8,128)(2,1)}, bf16[128,2048]{1,0:T(8,128)(2,1)S(1)}, u32[]{:S(2)}, u32[]{:S(2)}) collective-permute-start(bf16[128,2048]{1,0:T(8,128)(2,1)} %bitcast.36), channel_id=1, source_target_pairs={{0,8},{8,16},{16,24},{24,0},{1,9},{9,17},{17,25},{25,1},{2,10},{10... | collective-permute-start | bytes 1572872 | tf_op jit(solution)/shard_map/ppermute | solution.py:246
  201.3 20.4 %collective-permute-start.5 = (bf16[128,2048]{1,0:T(8,128)(2,1)}, bf16[128,2048]{1,0:T(8,128)(2,1)S(1)}, u32[]{:S(2)}, u32[]{:S(2)}) collective-permute-start(bf16[128,2048]{1,0:T(8,128)(2,1)} %bitcast.37), channel_id=1, source_target_pairs={{0,16},{8,24},{16,0},{24,8},{1,17},{9,25},{17,1},{25,9},{2,18},{10... | collective-permute-start | bytes 1572872 | tf_op jit(solution)/shard_map/ppermute | solution.py:246
  206.8 19.9 %collective-permute-start.6 = (bf16[128,2048]{1,0:T(8,128)(2,1)}, bf16[128,2048]{1,0:T(8,128)(2,1)S(1)}, u32[]{:S(2)}, u32[]{:S(2)}) collective-permute-start(bf16[128,2048]{1,0:T(8,128)(2,1)} %bitcast.38), channel_id=1, source_target_pairs={{0,24},{8,0},{16,8},{24,16},{1,25},{9,1},{17,9},{25,17},{2,26},{10... | collective-permute-start | bytes 1572872 | tf_op jit(solution)/shard_map/ppermute | solution.py:246
  231.7 7.8 %collective-permute-start.7 = (bf16[136,2048]{1,0:T(8,128)(2,1)}, bf16[136,2048]{1,0:T(8,128)(2,1)S(1)}, u32[]{:S(2)}, u32[]{:S(2)}) collective-permute-start(bf16[136,2048]{1,0:T(8,128)(2,1)} %get-tuple-element.23), channel_id=1, source_target_pairs={{0,1},{1,0},{2,3},{3,2},{4,5},{5,4},{6,7},{7,6},{8,9},{9,8},{10,11... | collective-permute-start | bytes 1671176 | tf_op jit(solution)/shard_map/ppermute | solution.py:246
  (6 other events, 39.6 us)

commit v8 on v4

--- a/solution.py
+++ b/solution.py
@@ -274,6 +274,13 @@
 def shifted(x, axis, step):
     count = lax.axis_size(axis)
     return lax.ppermute(x, axis, [(place, (place + step) % count) for place in range(count)])
+
+
+def numbered(blocks, axis):
+    sent = []
+    for step in range(1, lax.axis_size(axis)):
+        sent.append(shifted(blocks[step], axis, step))
+    return sent
 
 
 def from_all(x, axis):
@@ -348,7 +355,7 @@
     )(place, near(value_back))
     brought = shifted(away, "core", 1)
     both = jnp.stack([mine, brought], axis=1)
-    pieces = [both[0]] + [shifted(both[step], "x", step) for step in range(1, columns)]
+    pieces = [both[0]] + numbered(both, "x")
     partial = pl.pallas_call(
         product_kernel,
         compiler_params=pltpu.CompilerParams(vmem_limit_bytes=VMEM_BYTES),
@@ -356,7 +363,7 @@
         in_specs=[small] + [whole] * (2 + columns),
         scratch_shapes=[pltpu.VMEM((lines, w_cols, model), jnp.bfloat16)],
     )(place, near(own_rows), near(other_rows), *map(near, pieces))
-    partial = [partial[0]] + [shifted(partial[step], "y", step) for step in range(1, lines)]
+    partial = [partial[0]] + numbered(partial, "y")
     partial = sum(part.astype(jnp.float32) for part in partial).astype(jnp.bfloat16)
     partial = jnp.moveaxis(partial.reshape(w_cols, planes, model // planes), 1, 0)
     partial = exchanged(partial, "sp")

time: 245 us -> 245 us (level)
  no operation moved by 1% of the time
where the time goes in v8:
time: 245 us; the launch traced here: 244 us
  starting transfers between devices  118 us (48%)
  waiting for transfers between devices  82.2 us (34%)
  Pallas kernels  36.3 us (15%)
  local copies, waits for them, and re-layouts  3.11 us (1%)
  other arithmetic  2.81 us (1%)
    ppermute x18, starting transfers between devices, shifted(): lax.ppermute(x, axis, [(place, (place + step) % count) for place in range...  64.3 us
    ppermute x18, waiting for transfers between devices, shifted(): lax.ppermute(x, axis, [(place, (place + step) % count) for place in range...  55.5 us
    all_to_all x5, starting transfers between devices, exchanged(): return lax.all_to_all(x, axis, split_axis=0, concat_axis=0, tiled=True)  53.9 us
    all_to_all x5, waiting for transfers between devices, exchanged(): return lax.all_to_all(x, axis, split_axis=0, concat_axis=0, tiled=True)  26.7 us
    pallas_call x1, Pallas kernels, shards(): pl.pallas_call(pair_kernel, out_shape=shaped(length, LANES), scratch_shap...  9.13 us
    pallas_call x1, Pallas kernels, shards(): pl.pallas_call(value_kernel, out_shape=(shaped(planes, kept, LANES), row,...  7.74 us
  transfers between devices with their start and end apart: 23, of which 15 were waited for; matrix products, arithmetic and copies ran while one was open for 1% of the time, Pallas kernels for 13%

profile of v8, /device:TPU:9, one launch (start us, length us, event | category | flops | bytes accessed | tf_op | source)
XLA Modules:
  0.0 243.6 jit_solution(14647131847184100833)
XLA Ops:
  3.3 15.0 %all-to-all-start = ((bf16[16,136,256]{2,1,0:T(8,128)(2,1)}), bf16[16,136,256]{2,1,0:T(8,128)(2,1)S(1)}, u32[]{:S(2)}, u32[]{:S(2)}) async-start(bf16[16,136,256]{2,1,0:T(8,128)(2,1)} %shard_map.102), calls=%async_computation | async-start | bytes 2228224 | tf_op jit(solution)/shard_map/all_to_all | solution.py:271
  21.5 4.4 %collective-permute-start.9 = (bf16[136,2048]{1,0:T(8,128)(2,1)S(1)}, bf16[136,2048]{1,0:T(8,128)(2,1)S(1)}, u32[]{:S(2)}, u32[]{:S(2)}) collective-permute-start(bf16[136,2048]{1,0:T(8,128)(2,1)S(1)} %bitcast.44), channel_id=1, source_target_pairs={{0,4},{2,6},{4,0},{6,2},{1,5},{3,7},{5,1},{7,3},{8,12},{10,14},{12... | collective-permute-start | bytes 1671176 | tf_op jit(solution)/shard_map/ppermute | solution.py:276
  29.0 5.8 %collective-permute-done.8.refs_1_ = bf16[136,2048]{1,0:T(8,128)(2,1)S(1)} collective-permute-done((bf16[136,2048]{1,0:T(8,128)(2,1)S(1)}, bf16[136,2048]{1,0:T(8,128)(2,1)S(1)}, u32[]{:S(2)}, u32[]{:S(2)}) %collective-permute-start.8) | collective-permute-done | bytes 557088 | tf_op jit(solution)/shard_map/ppermute | solution.py:276
  34.7 12.9 %collective-permute-done.9.refs_2_ = bf16[136,2048]{1,0:T(8,128)(2,1)S(1)} collective-permute-done((bf16[136,2048]{1,0:T(8,128)(2,1)S(1)}, bf16[136,2048]{1,0:T(8,128)(2,1)S(1)}, u32[]{:S(2)}, u32[]{:S(2)}) %collective-permute-start.9) | collective-permute-done | bytes 557088 | tf_op jit(solution)/shard_map/ppermute | solution.py:276
  52.1 3.6 %collective-permute-start.11 = (bf16[4,136,2048]{2,1,0:T(8,128)(2,1)}, bf16[4,136,2048]{2,1,0:T(8,128)(2,1)}, u32[]{:S(2)}, u32[]{:S(2)}) collective-permute-start(bf16[4,136,2048]{2,1,0:T(8,128)(2,1)} %shard_map.111.own_ref), channel_id=1, source_target_pairs={{0,1},{1,0},{2,3},{3,2},{4,5},{5,4},{6,7},{7,6},{8,9},{9,8},{10,11... | collective-permute-start | bytes 6684680 | tf_op jit(solution)/shard_map/ppermute | solution.py:276
  55.6 10.1 %all-to-all-done = bf16[16,136,256]{2,1,0:T(8,128)(2,1)S(1)} async-done(((bf16[16,136,256]{2,1,0:T(8,128)(2,1)}), bf16[16,136,256]{2,1,0:T(8,128)(2,1)S(1)}, u32[]{:S(2)}, u32[]{:S(2)}) %all-to-all-start) | async-done | bytes 1114144 | tf_op jit(solution)/shard_map/all_to_all | solution.py:271
  65.8 7.7 %shard_map.103 = (bf16[16,72,128]{2,1,0:T(8,128)(2,1)}, f32[1,2176]{1,0:T(1,128)}, f32[1,2176]{1,0:T(1,128)}) custom-call(bf16[2176,256]{1,0:T(8,128)(2,1)S(1)} %bitcast.34, f32[1,2176]{1,0:T(1,128)} %bitcast.52), custom_call_target="tpu_custom_call" | custom-call | tf_op jit(solution)/shard_map/pallas_call | solution.py:333
  73.5 13.5 %all-to-all-start.2 = ((bf16[16,72,128]{2,1,0:T(8,128)(2,1)}), bf16[16,72,128]{2,1,0:T(8,128)(2,1)S(1)}, u32[]{:S(2)}, u32[]{:S(2)}) async-start(bf16[16,72,128]{2,1,0:T(8,128)(2,1)} %get-tuple-element.21), calls=%async_computation.2 | async-start | bytes 589824 | tf_op jit(solution)/shard_map/all_to_all | solution.py:271
  87.6 13.7 %all-to-all-done.2.x_ref = bf16[16,72,128]{2,1,0:T(8,128)(2,1)S(1)} async-done(((bf16[16,72,128]{2,1,0:T(8,128)(2,1)}), bf16[16,72,128]{2,1,0:T(8,128)(2,1)S(1)}, u32[]{:S(2)}, u32[]{:S(2)}) %all-to-all-start.2) | async-done | bytes 294944 | tf_op jit(solution)/shard_map/all_to_all | solution.py:271
  103.0 8.1 %collective-permute-start = (bf16[4,136,128]{2,1,0:T(8,128)(2,1)}, bf16[4,136,128]{2,1,0:T(8,128)(2,1)S(1)}, u32[]{:S(2)}, u32[]{:S(2)}) collective-permute-start(bf16[4,136,128]{2,1,0:T(8,128)(2,1)} %get-tuple-element.23), channel_id=1, source_target_pairs={{0,1},{1,0},{2,3},{3,2},{4,5},{5,4},{6,7},{7,6},{8,9},{9,8},{10,11... | collective-permute-start | bytes 417800 | tf_op jit(solution)/shard_map/ppermute | solution.py:276
  111.8 5.7 %all-to-all-start.3 = ((bf16[16,32,128]{2,1,0:T(8,128)(2,1)}), bf16[16,32,128]{2,1,0:T(8,128)(2,1)S(1)}, u32[]{:S(2)}, u32[]{:S(2)}) async-start(bf16[16,32,128]{2,1,0:T(8,128)(2,1)} %broadcast_in_dim.14), calls=%async_computation.3 | async-start | bytes 262144 | tf_op jit(solution)/shard_map/all_to_all | solution.py:271
  121.5 4.4 %collective-permute-start.13 = (bf16[2,136,128]{2,1,0:T(8,128)(2,1)S(1)}, bf16[2,136,128]{2,1,0:T(8,128)(2,1)S(1)}, u32[]{:S(2)}, u32[]{:S(2)}) collective-permute-start(bf16[2,136,128]{2,1,0:T(8,128)(2,1)S(1)} %get-tuple-element.33), channel_id=1, source_target_pairs={{0,4},{2,6},{4,0},{6,2},{1,5},{3,7},{5,1},{7,3},{8,12},{10,14},{12... | collective-permute-start | bytes 208904 | tf_op jit(solution)/shard_map/ppermute | solution.py:276
  137.6 4.2 %collective-permute-start.16 = (bf16[32,2048]{1,0:T(8,128)(2,1)S(1)}, bf16[32,2048]{1,0:T(8,128)(2,1)S(1)}, u32[]{:S(2)}, u32[]{:S(2)}) collective-permute-start(bf16[32,2048]{1,0:T(8,128)(2,1)S(1)} %get-tuple-element.28), channel_id=1, source_target_pairs={{0,16},{8,24},{16,0},{24,8},{1,17},{9,25},{17,1},{25,9},{2,18},{10... | collective-permute-start | bytes 393224 | tf_op jit(solution)/shard_map/ppermute | solution.py:276
  141.8 3.5 %collective-permute-start.15 = (bf16[32,2048]{1,0:T(8,128)(2,1)S(1)}, bf16[32,2048]{1,0:T(8,128)(2,1)S(1)}, u32[]{:S(2)}, u32[]{:S(2)}) collective-permute-start(bf16[32,2048]{1,0:T(8,128)(2,1)S(1)} %get-tuple-element.27), channel_id=1, source_target_pairs={{0,8},{8,16},{16,24},{24,0},{1,9},{9,17},{17,25},{25,1},{2,10},{10... | collective-permute-start | bytes 393224 | tf_op jit(solution)/shard_map/ppermute | solution.py:276
  149.5 11.0 %all-to-all-start.4 = ((bf16[16,32,128]{2,1,0:T(8,128)(2,1)}), bf16[16,32,128]{2,1,0:T(8,128)(2,1)S(1)}, u32[]{:S(2)}, u32[]{:S(2)}) async-start(bf16[16,32,128]{2,1,0:T(8,128)(2,1)} %bitcast_bitcast_fusion), calls=%async_computation.4 | async-start | bytes 262144 | tf_op jit(solution)/shard_map/all_to_all | solution.py:271
  160.5 9.1 %shard_map.104 = bf16[2176,128]{1,0:T(8,128)(2,1)} custom-call(bf16[2176,256]{1,0:T(8,128)(2,1)S(1)} %bitcast.35, f32[1,2176]{1,0:T(1,128)} %bitcast.53, f32[1,2176]{1,0:T(1,128)} %get-tuple-element.17.peak_ref, f32[1,2176]{1,0:T(1,128)} %get-tuple-element.18.share_ref), custom_call_target="tpu_custom_call" | custom-call | tf_op jit(solution)/shard_map/pallas_call | solution.py:339
  172.5 8.6 %all-to-all-start.1 = ((bf16[16,136,128]{2,1,0:T(8,128)(2,1)}), bf16[16,136,128]{2,1,0:T(8,128)(2,1)S(1)}, u32[]{:S(2)}, u32[]{:S(2)}) async-start(bf16[16,136,128]{2,1,0:T(8,128)(2,1)} %bitcast.37), calls=%async_computation.1 | async-start | bytes 1114112 | tf_op jit(solution)/shard_map/all_to_all | solution.py:271
  184.0 5.2 %collective-permute-start.2 = (bf16[32,2048]{1,0:T(8,128)(2,1)}, bf16[32,2048]{1,0:T(8,128)(2,1)S(1)}, u32[]{:S(2)}, u32[]{:S(2)}) collective-permute-start(bf16[32,2048]{1,0:T(8,128)(2,1)} %shard_map.107.refs_0_), channel_id=1, source_target_pairs={{0,4},{2,6},{4,0},{6,2},{1,5},{3,7},{5,1},{7,3},{8,12},{10,14},{12... | collective-permute-start | bytes 393224 | tf_op jit(solution)/shard_map/ppermute | solution.py:276
  191.7 4.3 %collective-permute-done.3.refs_3_ = bf16[32,2048]{1,0:T(8,128)(2,1)S(1)} collective-permute-done((bf16[32,2048]{1,0:T(8,128)(2,1)}, bf16[32,2048]{1,0:T(8,128)(2,1)S(1)}, u32[]{:S(2)}, u32[]{:S(2)}) %collective-permute-start.3) | collective-permute-done | bytes 131104 | tf_op jit(solution)/shard_map/ppermute | solution.py:276
  197.8 4.1 %collective-permute-start.4 = (bf16[128,2048]{1,0:T(8,128)(2,1)}, bf16[128,2048]{1,0:T(8,128)(2,1)S(1)}, u32[]{:S(2)}, u32[]{:S(2)}) collective-permute-start(bf16[128,2048]{1,0:T(8,128)(2,1)} %bitcast.38), channel_id=1, source_target_pairs={{0,8},{8,16},{16,24},{24,0},{1,9},{9,17},{17,25},{25,1},{2,10},{10... | collective-permute-start | bytes 1572872 | tf_op jit(solution)/shard_map/ppermute | solution.py:276
  207.5 3.4 %collective-permute-done.4.refs_1_ = bf16[128,2048]{1,0:T(8,128)(2,1)S(1)} collective-permute-done((bf16[128,2048]{1,0:T(8,128)(2,1)}, bf16[128,2048]{1,0:T(8,128)(2,1)S(1)}, u32[]{:S(2)}, u32[]{:S(2)}) %collective-permute-start.4) | collective-permute-done | bytes 524320 | tf_op jit(solution)/shard_map/ppermute | solution.py:276
  210.9 4.0 %collective-permute-done.5.refs_2_ = bf16[128,2048]{1,0:T(8,128)(2,1)S(1)} collective-permute-done((bf16[128,2048]{1,0:T(8,128)(2,1)}, bf16[128,2048]{1,0:T(8,128)(2,1)S(1)}, u32[]{:S(2)}, u32[]{:S(2)}) %collective-permute-start.5) | collective-permute-done | bytes 524320 | tf_op jit(solution)/shard_map/ppermute | solution.py:276
  214.8 15.3 %collective-permute-done.6.refs_3_ = bf16[128,2048]{1,0:T(8,128)(2,1)S(1)} collective-permute-done((bf16[128,2048]{1,0:T(8,128)(2,1)}, bf16[128,2048]{1,0:T(8,128)(2,1)S(1)}, u32[]{:S(2)}, u32[]{:S(2)}) %collective-permute-start.6) | collective-permute-done | bytes 524320 | tf_op jit(solution)/shard_map/ppermute | solution.py:276
  231.0 4.2 %shard_map.109 = (f32[136,2048]{1,0:T(8,128)}, bf16[136,2048]{1,0:T(8,128)(2,1)}) custom-call(s32[3]{0:T(128)} %pad_add_fusion.place_ref, bf16[4,136,128]{2,1,0:T(8,128)(2,1)} %get-tuple-element.22.first_ref, bf16[4,136,128]{2,1,0:T(8,128)(2,1)S(1)} %collective-permute-done.second_ref, bf16[128,2048]{1,0:T(8,128)(2,1)} %bitcast.41, ...), custom_call_target="tpu_custom_call" | custom-call | tf_op jit(solution)/shard_map/pallas_call | solution.py:374
  (52 shorter events, 60.9 us)
Async XLA Ops:
  3.3 62.4 %all-to-all-start = ((bf16[16,136,256]{2,1,0:T(8,128)(2,1)}), bf16[16,136,256]{2,1,0:T(8,128)(2,1)S(1)}, u32[]{:S(2)}, u32[]{:S(2)}) async-start(bf16[16,136,256]{2,1,0:T(8,128)(2,1)} %shard_map.102), calls=%async_computation | async-start | bytes 2228224 | tf_op jit(solution)/shard_map/all_to_all | solution.py:271
  18.4 16.3 %collective-permute-start.8 = (bf16[136,2048]{1,0:T(8,128)(2,1)S(1)}, bf16[136,2048]{1,0:T(8,128)(2,1)S(1)}, u32[]{:S(2)}, u32[]{:S(2)}) collective-permute-start(bf16[136,2048]{1,0:T(8,128)(2,1)S(1)} %bitcast.43), channel_id=1, source_target_pairs={{0,2},{2,4},{4,6},{6,0},{1,3},{3,5},{5,7},{7,1},{8,10},{10,12},{12... | collective-permute-start | bytes 1671176 | tf_op jit(solution)/shard_map/ppermute | solution.py:276
  21.5 26.1 %collective-permute-start.9 = (bf16[136,2048]{1,0:T(8,128)(2,1)S(1)}, bf16[136,2048]{1,0:T(8,128)(2,1)S(1)}, u32[]{:S(2)}, u32[]{:S(2)}) collective-permute-start(bf16[136,2048]{1,0:T(8,128)(2,1)S(1)} %bitcast.44), channel_id=1, source_target_pairs={{0,4},{2,6},{4,0},{6,2},{1,5},{3,7},{5,1},{7,3},{8,12},{10,14},{12... | collective-permute-start | bytes 1671176 | tf_op jit(solution)/shard_map/ppermute | solution.py:276
  25.9 23.6 %collective-permute-start.10 = (bf16[136,2048]{1,0:T(8,128)(2,1)S(1)}, bf16[136,2048]{1,0:T(8,128)(2,1)S(1)}, u32[]{:S(2)}, u32[]{:S(2)}) collective-permute-start(bf16[136,2048]{1,0:T(8,128)(2,1)S(1)} %bitcast.45), channel_id=1, source_target_pairs={{0,6},{2,0},{4,2},{6,4},{1,7},{3,1},{5,3},{7,5},{8,14},{10,8},{12,... | collective-permute-start | bytes 1671176 | tf_op jit(solution)/shard_map/ppermute | solution.py:276
  52.1 59.0 %copy-start.6 = (bf16[128,32]{0,1:T(8,128)(2,1)S(1)}, bf16[128,32]{0,1:T(8,128)(2,1)}, u32[]{:S(2)}) copy-start(bf16[128,32]{0,1:T(8,128)(2,1)} %param.13) | copy-start | bytes 24580
  52.1 76.9 %collective-permute-start.11 = (bf16[4,136,2048]{2,1,0:T(8,128)(2,1)}, bf16[4,136,2048]{2,1,0:T(8,128)(2,1)}, u32[]{:S(2)}, u32[]{:S(2)}) collective-permute-start(bf16[4,136,2048]{2,1,0:T(8,128)(2,1)} %shard_map.111.own_ref), channel_id=1, source_target_pairs={{0,1},{1,0},{2,3},{3,2},{4,5},{5,4},{6,7},{7,6},{8,9},{9,8},{10,11... | collective-permute-start | bytes 6684680 | tf_op jit(solution)/shard_map/ppermute | solution.py:276
  73.5 27.8 %all-to-all-start.2 = ((bf16[16,72,128]{2,1,0:T(8,128)(2,1)}), bf16[16,72,128]{2,1,0:T(8,128)(2,1)S(1)}, u32[]{:S(2)}, u32[]{:S(2)}) async-start(bf16[16,72,128]{2,1,0:T(8,128)(2,1)} %get-tuple-element.21), calls=%async_computation.2 | async-start | bytes 589824 | tf_op jit(solution)/shard_map/all_to_all | solution.py:271
  103.0 14.5 %collective-permute-start = (bf16[4,136,128]{2,1,0:T(8,128)(2,1)}, bf16[4,136,128]{2,1,0:T(8,128)(2,1)S(1)}, u32[]{:S(2)}, u32[]{:S(2)}) collective-permute-start(bf16[4,136,128]{2,1,0:T(8,128)(2,1)} %get-tuple-element.23), channel_id=1, source_target_pairs={{0,1},{1,0},{2,3},{3,2},{4,5},{5,4},{6,7},{7,6},{8,9},{9,8},{10,11... | collective-permute-start | bytes 417800 | tf_op jit(solution)/shard_map/ppermute | solution.py:276
  111.8 37.7 %all-to-all-start.3 = ((bf16[16,32,128]{2,1,0:T(8,128)(2,1)}), bf16[16,32,128]{2,1,0:T(8,128)(2,1)S(1)}, u32[]{:S(2)}, u32[]{:S(2)}) async-start(bf16[16,32,128]{2,1,0:T(8,128)(2,1)} %broadcast_in_dim.14), calls=%async_computation.3 | async-start | bytes 262144 | tf_op jit(solution)/shard_map/all_to_all | solution.py:271
  118.3 10.6 %collective-permute-start.12 = (bf16[2,136,128]{2,1,0:T(8,128)(2,1)S(1)}, bf16[2,136,128]{2,1,0:T(8,128)(2,1)S(1)}, u32[]{:S(2)}, u32[]{:S(2)}) collective-permute-start(bf16[2,136,128]{2,1,0:T(8,128)(2,1)S(1)} %get-tuple-element.32), channel_id=1, source_target_pairs={{0,2},{2,4},{4,6},{6,0},{1,3},{3,5},{5,7},{7,1},{8,10},{10,12},{12... | collective-permute-start | bytes 208904 | tf_op jit(solution)/shard_map/ppermute | solution.py:276
  121.5 7.5 %collective-permute-start.13 = (bf16[2,136,128]{2,1,0:T(8,128)(2,1)S(1)}, bf16[2,136,128]{2,1,0:T(8,128)(2,1)S(1)}, u32[]{:S(2)}, u32[]{:S(2)}) collective-permute-start(bf16[2,136,128]{2,1,0:T(8,128)(2,1)S(1)} %get-tuple-element.33), channel_id=1, source_target_pairs={{0,4},{2,6},{4,0},{6,2},{1,5},{3,7},{5,1},{7,3},{8,12},{10,14},{12... | collective-permute-start | bytes 208904 | tf_op jit(solution)/shard_map/ppermute | solution.py:276
  125.8 5.3 %collective-permute-start.14 = (bf16[2,136,128]{2,1,0:T(8,128)(2,1)S(1)}, bf16[2,136,128]{2,1,0:T(8,128)(2,1)S(1)}, u32[]{:S(2)}, u32[]{:S(2)}) collective-permute-start(bf16[2,136,128]{2,1,0:T(8,128)(2,1)S(1)} %get-tuple-element.30), channel_id=1, source_target_pairs={{0,6},{2,0},{4,2},{6,4},{1,7},{3,1},{5,3},{7,5},{8,14},{10,8},{12,... | collective-permute-start | bytes 208904 | tf_op jit(solution)/shard_map/ppermute | solution.py:276
  135.5 9.8 %collective-permute-start.17 = (bf16[32,2048]{1,0:T(8,128)(2,1)S(1)}, bf16[32,2048]{1,0:T(8,128)(2,1)S(1)}, u32[]{:S(2)}, u32[]{:S(2)}) collective-permute-start(bf16[32,2048]{1,0:T(8,128)(2,1)S(1)} %get-tuple-element.29), channel_id=1, source_target_pairs={{0,24},{8,0},{16,8},{24,16},{1,25},{9,1},{17,9},{25,17},{2,26},{10... | collective-permute-start | bytes 393224 | tf_op jit(solution)/shard_map/ppermute | solution.py:276
  137.6 8.2 %collective-permute-start.16 = (bf16[32,2048]{1,0:T(8,128)(2,1)S(1)}, bf16[32,2048]{1,0:T(8,128)(2,1)S(1)}, u32[]{:S(2)}, u32[]{:S(2)}) collective-permute-start(bf16[32,2048]{1,0:T(8,128)(2,1)S(1)} %get-tuple-element.28), channel_id=1, source_target_pairs={{0,16},{8,24},{16,0},{24,8},{1,17},{9,25},{17,1},{25,9},{2,18},{10... | collective-permute-start | bytes 393224 | tf_op jit(solution)/shard_map/ppermute | solution.py:276
  141.8 7.0 %collective-permute-start.15 = (bf16[32,2048]{1,0:T(8,128)(2,1)S(1)}, bf16[32,2048]{1,0:T(8,128)(2,1)S(1)}, u32[]{:S(2)}, u32[]{:S(2)}) collective-permute-start(bf16[32,2048]{1,0:T(8,128)(2,1)S(1)} %get-tuple-element.27), channel_id=1, source_target_pairs={{0,8},{8,16},{16,24},{24,0},{1,9},{9,17},{17,25},{25,1},{2,10},{10... | collective-permute-start | bytes 393224 | tf_op jit(solution)/shard_map/ppermute | solution.py:276
  149.5 23.0 %all-to-all-start.4 = ((bf16[16,32,128]{2,1,0:T(8,128)(2,1)}), bf16[16,32,128]{2,1,0:T(8,128)(2,1)S(1)}, u32[]{:S(2)}, u32[]{:S(2)}) async-start(bf16[16,32,128]{2,1,0:T(8,128)(2,1)} %bitcast_bitcast_fusion), calls=%async_computation.4 | async-start | bytes 262144 | tf_op jit(solution)/shard_map/all_to_all | solution.py:271
  172.5 70.0 %all-to-all-start.1 = ((bf16[16,136,128]{2,1,0:T(8,128)(2,1)}), bf16[16,136,128]{2,1,0:T(8,128)(2,1)S(1)}, u32[]{:S(2)}, u32[]{:S(2)}) async-start(bf16[16,136,128]{2,1,0:T(8,128)(2,1)} %bitcast.37), calls=%async_computation.1 | async-start | bytes 1114112 | tf_op jit(solution)/shard_map/all_to_all | solution.py:271
  181.8 9.3 %collective-permute-start.1 = (bf16[32,2048]{1,0:T(8,128)(2,1)}, bf16[32,2048]{1,0:T(8,128)(2,1)S(1)}, u32[]{:S(2)}, u32[]{:S(2)}) collective-permute-start(bf16[32,2048]{1,0:T(8,128)(2,1)} %shard_map.107.refs_0_), channel_id=1, source_target_pairs={{0,2},{2,4},{4,6},{6,0},{1,3},{3,5},{5,7},{7,1},{8,10},{10,12},{12... | collective-permute-start | bytes 393224 | tf_op jit(solution)/shard_map/ppermute | solution.py:276
  184.0 7.7 %collective-permute-start.2 = (bf16[32,2048]{1,0:T(8,128)(2,1)}, bf16[32,2048]{1,0:T(8,128)(2,1)S(1)}, u32[]{:S(2)}, u32[]{:S(2)}) collective-permute-start(bf16[32,2048]{1,0:T(8,128)(2,1)} %shard_map.107.refs_0_), channel_id=1, source_target_pairs={{0,4},{2,6},{4,0},{6,2},{1,5},{3,7},{5,1},{7,3},{8,12},{10,14},{12... | collective-permute-start | bytes 393224 | tf_op jit(solution)/shard_map/ppermute | solution.py:276
  189.2 6.8 %collective-permute-start.3 = (bf16[32,2048]{1,0:T(8,128)(2,1)}, bf16[32,2048]{1,0:T(8,128)(2,1)S(1)}, u32[]{:S(2)}, u32[]{:S(2)}) collective-permute-start(bf16[32,2048]{1,0:T(8,128)(2,1)} %shard_map.107.refs_0_), channel_id=1, source_target_pairs={{0,6},{2,0},{4,2},{6,4},{1,7},{3,1},{5,3},{7,5},{8,14},{10,8},{12,... | collective-permute-start | bytes 393224 | tf_op jit(solution)/shard_map/ppermute | solution.py:276
  197.8 13.1 %collective-permute-start.4 = (bf16[128,2048]{1,0:T(8,128)(2,1)}, bf16[128,2048]{1,0:T(8,128)(2,1)S(1)}, u32[]{:S(2)}, u32[]{:S(2)}) collective-permute-start(bf16[128,2048]{1,0:T(8,128)(2,1)} %bitcast.38), channel_id=1, source_target_pairs={{0,8},{8,16},{16,24},{24,0},{1,9},{9,17},{17,25},{25,1},{2,10},{10... | collective-permute-start | bytes 1572872 | tf_op jit(solution)/shard_map/ppermute | solution.py:276
  201.9 13.0 %collective-permute-start.5 = (bf16[128,2048]{1,0:T(8,128)(2,1)}, bf16[128,2048]{1,0:T(8,128)(2,1)S(1)}, u32[]{:S(2)}, u32[]{:S(2)}) collective-permute-start(bf16[128,2048]{1,0:T(8,128)(2,1)} %bitcast.39), channel_id=1, source_target_pairs={{0,16},{8,24},{16,0},{24,8},{1,17},{9,25},{17,1},{25,9},{2,18},{10... | collective-permute-start | bytes 1572872 | tf_op jit(solution)/shard_map/ppermute | solution.py:276
  204.4 25.8 %collective-permute-start.6 = (bf16[128,2048]{1,0:T(8,128)(2,1)}, bf16[128,2048]{1,0:T(8,128)(2,1)S(1)}, u32[]{:S(2)}, u32[]{:S(2)}) collective-permute-start(bf16[128,2048]{1,0:T(8,128)(2,1)} %bitcast.40), channel_id=1, source_target_pairs={{0,24},{8,0},{16,8},{24,16},{1,25},{9,1},{17,9},{25,17},{2,26},{10... | collective-permute-start | bytes 1572872 | tf_op jit(solution)/shard_map/ppermute | solution.py:276
  235.2 4.6 %collective-permute-start.7 = (bf16[136,2048]{1,0:T(8,128)(2,1)}, bf16[136,2048]{1,0:T(8,128)(2,1)S(1)}, u32[]{:S(2)}, u32[]{:S(2)}) collective-permute-start(bf16[136,2048]{1,0:T(8,128)(2,1)} %get-tuple-element.25), channel_id=1, source_target_pairs={{0,1},{1,0},{2,3},{3,2},{4,5},{5,4},{6,7},{7,6},{8,9},{9,8},{10,11... | collective-permute-start | bytes 1671176 | tf_op jit(solution)/shard_map/ppermute | solution.py:276
  (6 other events, 95.7 us)
